TPU v7x, 32 devices: a whole 2x2x4 slice. The times are simulated.
32 devices in a mesh: ep: 8 (over z, x), tp: 4 (over y, core).
Axes of the slice: x: 2, y: 2, z: 4, core: 2. Of those that a mesh axis runs over, the one named last changes fastest.
Arguments:
- queries: bfloat16 [1024, 4096], P('ep', 'tp'), may hold values from -112 to 112
- key_rows: bfloat16 [1024, 4096], P('ep', 'tp'), may hold values from -8.1 to 8.1
- values: bfloat16 [1024, 4096], P('ep', 'tp'), may hold values from -6 to 6
- lambdas: float32 [16], P('tp'), may hold values from 0.3 to 0.8
- head_gain: float32 [256], replicated, may hold values from 0.1 to 1.9
- tokens: bfloat16 [512, 4096], P('ep'), may hold values from -6 to 6
- moe_gain: float32 [4096], replicated, may hold values from 0.1 to 1.9
- routes: int32 [512, 2], P('ep'), may hold values from 0 to 7, all different within a row; in each aligned block of 64 rows (0 to 63, 64 to 127, ...) at most 32 rows name the same one
- route_scores: float32 [512, 2], P('ep'), may hold values from -6 to 6
- w_gate: bfloat16 [8, 4096, 2048], P('ep', None, 'tp'), may hold values from -0.09375 to 0.09375
- w_up: bfloat16 [8, 4096, 2048], P('ep', None, 'tp'), may hold values from -0.09375 to 0.09375
- w_down: bfloat16 [8, 2048, 4096], P('ep', 'tp'), may hold values from -0.125 to 0.125
Outputs:
- attended: bfloat16 [1024, 4096], P('ep', 'tp')
- expert_out: bfloat16 [512, 4096], P('ep', 'tp')
Inputs may be any that keep to these rules, and one draw needn't show every extreme that they name: `routes`: each row names 2 different experts. Among the rows of one index of ep at most 32 name the same expert, and some index reaches 32 in every draw.
All inputs are finite; a program needn't handle non-finite values.
Results may differ from a plain program's by a relative error of at most 0.018.
Values may be sent and summed in bfloat16 or wider, within the bound.
No kernel may reach another device: no remote copies, remote signals or barrier semaphores. Data moves between devices by JAX's collectives and lax.ppermute only.
A program may use at most 64 MiB of HBM per device.

v0:
```python
import jax
import jax.numpy as jnp
from jax import lax
from jax.sharding import PartitionSpec as P

QKD = 128
VD = 256
TOP = 2


neg_big = -1e30
head_eps = 1e-05
moe_eps = 1e-06
head_scale = 0.8


def slot_table(routes, experts, capacity):
    flat_routes = routes.reshape(-1)
    onehot = (flat_routes[:, None] == jnp.arange(experts, dtype=jnp.int32)[None, :]).astype(
        jnp.int32
    )
    before = jnp.cumsum(onehot, axis=0) - onehot
    position = jnp.sum(before * onehot, axis=1)
    return (flat_routes * capacity + position).reshape(routes.shape)


def fold_block(state, query_group, query_pos, key_heads, value_heads, key_pos):
    maxima, denominators, accumulated = state
    scores = jnp.einsum(
        "qhmd,khmd->hmqk", query_group, key_heads, preferred_element_type=jnp.float32
    ) * QKD ** (-0.5)
    visible = key_pos[None, :] <= query_pos[:, None]
    scores = jnp.where(visible, scores, neg_big)
    new_max = jnp.maximum(maxima, jnp.max(scores, axis=-1))
    weights = jnp.where(visible, jnp.exp(scores - new_max[..., None]), 0.0)
    accumulated = jnp.einsum(
        "hmqk,khd->hmqd", weights, value_heads, precision=lax.Precision.HIGHEST
    )
    denominators = jnp.sum(weights, axis=-1)
    return (new_max, denominators, accumulated)


def local(
    queries,
    key_rows,
    values,
    lambdas,
    head_gain,
    tokens,
    moe_gain,
    routes,
    route_scores,
    w_gate,
    w_up,
    w_down,
):
    rows_a = queries.shape[0]
    half_rows = rows_a // 2
    head_local = lambdas.shape[0]
    ep_count = lax.axis_size("ep")
    ep_index = lax.axis_index("ep")
    early_queries = queries[:half_rows]
    later_queries = queries[half_rows:]
    early_pos = ep_index * rows_a + jnp.arange(half_rows, dtype=jnp.int32)
    later_pos = ep_index * rows_a + half_rows + jnp.arange(half_rows, dtype=jnp.int32)
    query_groups = (
        early_queries.reshape(half_rows, head_local, 2, QKD),
        later_queries.reshape(half_rows, head_local, 2, QKD),
    )
    position_groups = (early_pos, later_pos)
    start_state = (
        jnp.full((head_local, 2, half_rows), neg_big, jnp.float32),
        jnp.zeros((head_local, 2, half_rows), jnp.float32),
        jnp.zeros((head_local, 2, half_rows, VD), jnp.float32),
    )
    totals = (start_state, start_state)
    row_start = jnp.int32(0)
    key_block = lax.all_gather(key_rows, "ep", axis=0, tiled=True)
    value_block = lax.all_gather(values, "ep", axis=0, tiled=True)
    key_count = key_block.shape[0]
    key_heads = key_block.reshape(key_count, head_local, 2, QKD)
    value_heads = value_block.reshape(key_count, head_local, VD).astype(jnp.float32)
    key_pos = jnp.arange(key_count, dtype=jnp.int32)
    updated = []
    for attend_group_index in range(2):
        state = totals[attend_group_index]
        query_group = query_groups[attend_group_index]
        query_pos = position_groups[attend_group_index]
        state = lax.cond(
            row_start <= query_pos[-1],
            lambda held: fold_block(held, query_group, query_pos, key_heads, value_heads, key_pos),
            lambda held: held,
            state,
        )
        updated.append(state)
    folded = (updated[0], updated[1])
    attended_groups = []
    for group_index in range(2):
        maxima, denominators, accumulated = folded[group_index]
        mixed_out = (
            accumulated[:, 0] / denominators[:, 0, :, None]
            - lambdas[:, None, None] * accumulated[:, 1] / denominators[:, 1, :, None]
        )
        scaled = mixed_out * lax.rsqrt(
            jnp.mean(mixed_out * mixed_out, axis=-1, keepdims=True) + head_eps
        )
        scaled = scaled * head_gain * head_scale
        attended_groups.append(
            scaled.transpose(1, 0, 2).reshape(half_rows, head_local * VD).astype(jnp.bfloat16)
        )
    later_out = attended_groups[1]
    attended = jnp.concatenate([attended_groups[0], later_out], axis=0)
    rows_b = tokens.shape[0]
    capacity = 2 * TOP * rows_b // ep_count
    token_f32 = tokens.astype(jnp.float32)
    normed = (
        token_f32
        * lax.rsqrt(jnp.mean(token_f32 * token_f32, axis=-1, keepdims=True) + moe_eps)
        * moe_gain
    ).astype(jnp.bfloat16)
    gate_weights = jax.nn.softmax(route_scores, axis=-1)
    slot_of = slot_table(routes, ep_count, capacity)
    row_ids = jnp.broadcast_to(jnp.arange(rows_b, dtype=jnp.int32)[:, None], slot_of.shape)
    row_of_slot = (
        jnp.zeros((ep_count * capacity,), jnp.int32)
        .at[slot_of.reshape(-1)]
        .set(row_ids.reshape(-1))
    )
    gate_local = w_gate[0]
    up_local = w_up[0]
    down_local = w_down[0]
    outgoing = normed[row_of_slot]
    arrived = lax.all_to_all(outgoing, "ep", split_axis=0, concat_axis=0, tiled=True)
    gate_act = jnp.dot(arrived, gate_local, preferred_element_type=jnp.float32)
    up_act = jnp.dot(arrived, up_local, preferred_element_type=jnp.float32)
    hidden = (jax.nn.silu(gate_act) * up_act).astype(jnp.bfloat16)
    summed = lax.psum_scatter(
        lax.dot_general(
            down_local, hidden, (((0,), (1,)), ((), ())), preferred_element_type=jnp.float32
        ).astype(jnp.bfloat16),
        "tp",
        scatter_dimension=0,
        tiled=True,
    )
    returned = lax.all_to_all(summed, "ep", split_axis=1, concat_axis=1, tiled=True)
    slot_ids = jnp.arange(ep_count * capacity, dtype=jnp.int32)
    combined = jnp.zeros((rows_b, returned.shape[0]), jnp.float32)
    for choice_index in range(TOP):
        picker = (slot_of[:, choice_index, None] == slot_ids[None, :]).astype(jnp.bfloat16)
        picked = lax.dot_general(
            picker, returned, (((1,), (1,)), ((), ())), preferred_element_type=jnp.float32
        )
        combined = combined + gate_weights[:, choice_index, None] * picked
    expert_out = combined.astype(jnp.bfloat16)
    return (attended, expert_out)


def solution(mesh):
    return jax.shard_map(
        local,
        mesh=mesh,
        in_specs=(
            P("ep", "tp"),
            P("ep", "tp"),
            P("ep", "tp"),
            P("tp"),
            P(),
            P("ep", None),
            P(),
            P("ep", None),
            P("ep", None),
            P("ep", None, "tp"),
            P("ep", None, "tp"),
            P("ep", "tp", None),
        ),
        out_specs=(P("ep", "tp"), P("ep", "tp")),
        check_vma=False,
    )
```

profile of v0, /device:TPU:0, one launch (start us, length us, event | category | flops | bytes accessed | tf_op | source)
XLA Modules:
  0.0 190.7 jit_solution(13893074613434656306)
XLA Ops:
  8.0 0.0 copy-start.2
  8.0 0.0 all-gather.5.cloned.1.call-start
  8.1 1.9 copy.24
  9.9 0.0 all-gather.5.cloned.1.call-update
  9.9 0.8 copy.34
  10.7 0.1 eq.45
  10.8 0.1 fusion.62
  10.9 0.2 reduce_window_sum.11
  11.1 0.2 select_reduce_fusion
  11.3 0.1 reduce_sum.71
  11.5 0.1 mul.157
  11.6 0.1 reshape.129
  11.8 1.0 scatter_custom_fusion
  12.8 1.2 fusion.42
  14.0 0.0 copy-done.2
  14.0 0.9 fusion.44
  15.0 3.2 %gather_fusion = bf16[256,4096]{1,0:T(8,128)(2,1)} fusion(bf16[64,4096]{1,0:T(8,128)(2,1)S(1)} %fusion.44, s32[1024]{0:T(1024)S(1)} %pad_clamp_fusion), kind=kCustom, calls=%fused_computation | custom fusion | bytes 4195328 | tf_op jit(solution)/shard_map/gather | solution.py:132
  18.2 0.0 copy-start.3
  18.2 7.4 %all-to-all-start = ((bf16[8,32,4096]{2,1,0:T(8,128)(2,1)}), bf16[8,32,4096]{2,1,0:T(8,128)(2,1)S(1)}, u32[]{:S(2)}, u32[]{:S(2)}) async-start(bf16[8,32,4096]{2,1,0:T(8,128)(2,1)} %bitcast.20), calls=%async_computation | async-start | bytes 4194304 | tf_op jit(solution)/shard_map/all_to_all | solution.py:133
  25.6 0.0 all-gather.3.cloned.1.call-start
  25.6 0.0 copy-done.3
  25.6 0.8 copy.23
  26.5 0.0 all-gather.3.cloned.1.call-update
  26.5 0.0 reduce-scatter.2.cloned.1.call-start
  26.5 69.8 %all-to-all-done = bf16[8,32,4096]{2,1,0:T(8,128)(2,1)S(1)} async-done(((bf16[8,32,4096]{2,1,0:T(8,128)(2,1)}), bf16[8,32,4096]{2,1,0:T(8,128)(2,1)S(1)}, u32[]{:S(2)}, u32[]{:S(2)}) %all-to-all-start) | async-done | bytes 2097184 | tf_op jit(solution)/shard_map/all_to_all | solution.py:133
  96.3 3.5 %fusion.32 = f32[256,512]{1,0:T(8,128)S(1)} fusion(bf16[256,4096]{1,0:T(8,128)(2,1)S(1)} %bitcast.99, bf16[1,4096,512]{2,1,0:T(8,128)(2,1)} %param.25), kind=kOutput, calls=%fused_computation.43 | convolution fusion | flops 1073741824 | bytes 6815744 | tf_op jit(solution)/shard_map/dot_general | solution.py:134
  99.8 7.4 %fusion.28 = bf16[4096,256]{0,1:T(8,128)(2,1)} fusion(bf16[1,512,4096]{2,1,0:T(8,128)(2,1)} %param.27, bf16[256,4096]{1,0:T(8,128)(2,1)S(1)} %bitcast.100, bf16[1,4096,512]{2,1,0:T(8,128)(2,1)} %param.26, f32[256,512]{1,0:T(8,128)S(1)} %fusion.32), kind=kOutput, calls=%fused_computation.39 | convolution fusion | flops 2149318656 | bytes 13107200 | tf_op jit(solution)/shard_map/dot_general | solution.py:138
  107.2 0.0 copy-start.5
  107.2 0.0 reduce-scatter.2.cloned.1.call-update
  107.2 0.6 slice.55
  108.5 0.6 slice.50
  109.7 0.0 copy-done.5
  109.8 0.2 slice_reduce_fusion
  110.0 0.0 all-gather.5.cloned.1.call-done
  110.0 0.0 copy-start.4
  110.0 4.1 %convert.3 = f32[1024,4,256]{0,2,1:T(8,128)} convert(bf16[1024,4,256]{0,2,1:T(8,128)(2,1)} %bitcast.98) | non-fusion elementwise | flops 1048576 | bytes 6291456 | tf_op jit(solution)/shard_map/convert_element_type | solution.py:82
  114.1 33.2 %all-gather.3.cloned.1.call-done = bf16[1024,1024]{0,1:T(8,128)(2,1)} async-done(((bf16[128,1024]{0,1:T(8,128)(2,1)}), bf16[1024,1024]{0,1:T(8,128)(2,1)}) %all-gather.3.cloned.1.call-update) | async-done | bytes 2097168 | tf_op jit(solution)/shard_map/all_gather | solution.py:78
  147.3 0.0 copy-done.4
  147.3 8.6 %conditional.3 = (f32[4,2,64]{2,1,0:T(2,128)S(1)}, f32[4,2,64,256]{3,2,1,0:T(8,128)S(1)}) conditional(s32[]{:T(128)} %bitcast.10, () %tuple.26, (s32[1024]{0:T(1024)S(1)}, s32[64]{0:T(128)S(1)}, bf16[128,1024]{1,0:T(8,128)(2,1)S(1)}, bf16[1024,4,2,128]{0,3,2,1:T(8,128)(2,1)}, f32[1024,4,256]{0,2,1:T(8,128)}) %tuple.56), branch_computations={%region_5.6_spmd, %region_6.9_spmd} | conditional | flops 1751186944 | bytes 30818604 | solution.py:89
  147.3 0.1 broadcast_compare_fusion.1
  147.4 0.1 reshape.109
  147.5 0.0 copy-start
  147.5 2.4 %fusion.16 = (f32[4,2,64]{2,1,0:T(2,128)S(1)}, f32[4,2,64,1024]{3,2,1,0:T(8,128)S(1)}) fusion(pred[64,1024]{1,0:T(8,128)(4,1)S(1)} %broadcast_compare_fusion.1, bf16[1024,4,2,128]{0,3,2,1:T(8,128)(2,1)} %get-tuple-element.52, bf16[64,4,2,128]{3,2,1,0:T(2,128)(2,1)S(1)} %reshape.109), kind=kOutput, calls=%fused_computation.24 | convolution fusion | flops 135790080 | bytes 4392960 | tf_op jit(solution)/shard_map/cond/branch_1_fun/qhmd,khmd->hmqk/dot_general | solution.py:29
  150.0 0.4 copy-done
  150.3 4.8 %fusion.14 = f32[4,2,64,256]{3,2,1,0:T(8,128)S(1)} fusion(f32[1024,4,256]{0,2,1:T(8,128)S(1)} %copy-done, f32[4,2,64,1024]{3,2,1,0:T(8,128)S(1)} %get-tuple-element.63, f32[4,2,64]{2,1,0:T(2,128)S(1)} %broadcast_maximum_fusion.1, pred[64,1024]{1,0:T(8,128)(4,1)S(1)} %broadcast_compare_fusion.1), kind=kOutput, calls=%fused_computation.20 | convolution fusion | flops 1612709888 | bytes 6883328 | tf_op jit(solution)/shard_map/cond/branch_1_fun/hmqk,khd->hmqd/dot_general | solution.py:36
  155.2 0.7 fusion.17
  155.9 8.8 %conditional.2 = (f32[4,2,64]{2,1,0:T(2,128)S(1)}, f32[4,2,64,256]{3,2,1,0:T(8,128)S(1)}) conditional(s32[]{:T(128)} %bitcast.2, () %tuple.24, (s32[1024]{0:T(1024)S(1)}, s32[64]{0:T(128)S(1)}, bf16[128,1024]{1,0:T(8,128)(2,1)S(1)}, bf16[1024,4,2,128]{0,3,2,1:T(8,128)(2,1)}, f32[1024,4,256]{0,2,1:T(8,128)}) %tuple.57), branch_computations={%region_0.0_spmd, %region_1.4_spmd} | conditional | flops 1751186944 | bytes 30818604 | solution.py:89
  156.1 0.1 broadcast_compare_fusion
  156.2 0.1 reshape.108
  156.3 0.0 copy-start.1
  156.3 2.4 %fusion.2 = (f32[4,2,64]{2,1,0:T(2,128)S(1)}, f32[4,2,64,1024]{3,2,1,0:T(8,128)S(1)}) fusion(pred[64,1024]{1,0:T(8,128)(4,1)S(1)} %broadcast_compare_fusion, bf16[1024,4,2,128]{0,3,2,1:T(8,128)(2,1)} %get-tuple-element.47, bf16[64,4,2,128]{3,2,1,0:T(2,128)(2,1)S(1)} %reshape.108), kind=kOutput, calls=%fused_computation.6 | convolution fusion | flops 135790080 | bytes 4392960 | tf_op jit(solution)/shard_map/cond/branch_1_fun/qhmd,khmd->hmqk/dot_general | solution.py:29
  158.7 0.4 copy-done.1
  159.1 4.8 %fusion = f32[4,2,64,256]{3,2,1,0:T(8,128)S(1)} fusion(f32[1024,4,256]{0,2,1:T(8,128)S(1)} %copy-done.1, f32[4,2,64,1024]{3,2,1,0:T(8,128)S(1)} %get-tuple-element.61, f32[4,2,64]{2,1,0:T(2,128)S(1)} %broadcast_maximum_fusion, pred[64,1024]{1,0:T(8,128)(4,1)S(1)} %broadcast_compare_fusion), kind=kOutput, calls=%fused_computation.2 | convolution fusion | flops 1612709888 | bytes 6883328 | tf_op jit(solution)/shard_map/cond/branch_1_fun/hmqk,khd->hmqd/dot_general | solution.py:36
  164.0 0.7 fusion.3
  164.7 0.0 reduce-scatter.2.cloned.1.call-done
  164.7 3.5 %all-to-all-start.1 = ((bf16[1024,8,32]{0,2,1:T(8,128)(2,1)}), bf16[1024,8,32]{0,2,1:T(8,128)(2,1)S(1)}, u32[]{:S(2)}, u32[]{:S(2)}) async-start(bf16[1024,8,32]{0,2,1:T(8,128)(2,1)} %bitcast.101), calls=%async_computation.2 | async-start | bytes 1048576 | tf_op jit(solution)/shard_map/all_to_all | solution.py:145
  168.2 0.0 copy-done.7
  168.3 0.4 multiply_reduce_fusion.1
  168.6 0.0 copy-done.6
  168.6 0.1 fusion.60
  168.8 0.7 pad_maximum_fusion
  169.5 12.6 %all-to-all-done.1 = bf16[1024,8,32]{0,2,1:T(8,128)(2,1)S(1)} async-done(((bf16[1024,8,32]{0,2,1:T(8,128)(2,1)}), bf16[1024,8,32]{0,2,1:T(8,128)(2,1)S(1)}, u32[]{:S(2)}, u32[]{:S(2)}) %all-to-all-start.1) | async-done | bytes 524320 | tf_op jit(solution)/shard_map/all_to_all | solution.py:145
  182.1 0.2 convolution_multiply_fusion.1
  182.4 0.9 fusion.41
  (25 shorter events, 0.2 us)
Async XLA Ops:
  8.0 6.0 %copy-start.2 = (bf16[64,4096]{1,0:T(8,128)(2,1)S(1)}, bf16[64,4096]{1,0:T(8,128)(2,1)}, u32[]{:S(2)}) copy-start(bf16[64,4096]{1,0:T(8,128)(2,1)} %param.21) | copy-start | bytes 1572868
  8.0 102.0 %all-gather.5.cloned.1.call-start = ((), (), s32[]{:S(2)}) async-start(), calls=%async_computation.4 | async-start | bytes 2359296 | tf_op jit(solution)/shard_map/all_gather | solution.py:79
  18.2 7.5 %copy-start.3 = (bf16[128,1024]{1,0:T(8,128)(2,1)S(1)}, bf16[128,1024]{1,0:T(8,128)(2,1)}, u32[]{:S(2)}) copy-start(bf16[128,1024]{1,0:T(8,128)(2,1)} %param.17) | copy-start | bytes 786436
  18.2 78.2 %all-to-all-start = ((bf16[8,32,4096]{2,1,0:T(8,128)(2,1)}), bf16[8,32,4096]{2,1,0:T(8,128)(2,1)S(1)}, u32[]{:S(2)}, u32[]{:S(2)}) async-start(bf16[8,32,4096]{2,1,0:T(8,128)(2,1)} %bitcast.20), calls=%async_computation | async-start | bytes 4194304 | tf_op jit(solution)/shard_map/all_to_all | solution.py:133
  25.6 121.7 %all-gather.3.cloned.1.call-start = ((), (), s32[]{:S(2)}) async-start(), calls=%async_computation.3 | async-start | bytes 2359296 | tf_op jit(solution)/shard_map/all_gather | solution.py:78
  26.5 138.2 %reduce-scatter.2.cloned.1.call-start = ((), (), s32[]{:S(2)}) async-start(), calls=%async_computation.5 | async-start | bytes 2621440 | tf_op jit(solution)/shard_map/reduce_scatter | solution.py:137
  107.2 2.5 %copy-start.5 = (f32[64,2]{0,1:T(2,128)S(1)}, f32[64,2]{0,1:T(2,128)}, u32[]{:S(2)}) copy-start(f32[64,2]{0,1:T(2,128)} %param.24) | copy-start | bytes 1540
  110.0 37.3 %copy-start.4 = (bf16[128,1024]{1,0:T(8,128)(2,1)S(1)}, bf16[128,1024]{1,0:T(8,128)(2,1)}, u32[]{:S(2)}) copy-start(bf16[128,1024]{1,0:T(8,128)(2,1)} %param.16) | copy-start | bytes 786436
  147.5 2.8 %copy-start = (f32[1024,4,256]{0,2,1:T(8,128)S(1)}, f32[1024,4,256]{0,2,1:T(8,128)}, u32[]{:S(2)}) copy-start(f32[1024,4,256]{0,2,1:T(8,128)} %get-tuple-element.53) | copy-start | bytes 12582916 | tf_op jit(solution)/shard_map/cond
  155.9 12.4 %copy-start.7 = (f32[4]{0:T(128)S(1)}, f32[4]{0:T(128)}, u32[]{:S(2)}) copy-start(f32[4]{0:T(128)} %param.19) | copy-start | bytes 52
  156.3 2.8 %copy-start.1 = (f32[1024,4,256]{0,2,1:T(8,128)S(1)}, f32[1024,4,256]{0,2,1:T(8,128)}, u32[]{:S(2)}) copy-start(f32[1024,4,256]{0,2,1:T(8,128)} %get-tuple-element.48) | copy-start | bytes 12582916 | tf_op jit(solution)/shard_map/cond
  164.7 4.0 %copy-start.6 = (f32[256]{0:T(256)S(1)}, f32[256]{0:T(256)}, u32[]{:S(2)}) copy-start(f32[256]{0:T(256)} %param.20) | copy-start | bytes 3076
  164.7 17.4 %all-to-all-start.1 = ((bf16[1024,8,32]{0,2,1:T(8,128)(2,1)}), bf16[1024,8,32]{0,2,1:T(8,128)(2,1)S(1)}, u32[]{:S(2)}, u32[]{:S(2)}) async-start(bf16[1024,8,32]{0,2,1:T(8,128)(2,1)} %bitcast.101), calls=%async_computation.2 | async-start | bytes 1048576 | tf_op jit(solution)/shard_map/all_to_all | solution.py:145
Sparse Core Ops, SparseCore 0:
  10.9 83.9 all-gather.4
  97.5 49.7 all-gather.2
Sparse Core Ops, SparseCore 1:
  107.3 30.1 reduce-scatter.1
where the time goes:
time: 191 us
  waiting for transfers between devices  116 us (61%)
  matrix products  26.5 us (14%)
  between operations  17.1 us (9%)
  starting transfers between devices  11 us (6%)
  local copies, waits for them, and re-layouts  10.5 us (5%)
  other arithmetic  9.63 us (5%)
    all_to_all x1, waiting for transfers between devices, local(): lax.all_to_all(outgoing, 'ep', split_axis=0, concat_axis=0, tiled=True)  69.8 us
    all_gather x1, waiting for transfers between devices, local(): key_block = lax.all_gather(key_rows, 'ep', axis=0, tiled=True)  33.2 us
    all_to_all x1, waiting for transfers between devices, local(): lax.all_to_all(summed, 'ep', split_axis=1, concat_axis=1, tiled=True)  12.6 us
    dot_general x2, matrix products, fold_block(): jnp.einsum('hmqk,khd->hmqd', weights, value_heads, precision=lax.Precisio...  9.67 us
    all_to_all x1, starting transfers between devices, local(): lax.all_to_all(outgoing, 'ep', split_axis=0, concat_axis=0, tiled=True)  7.41 us
    dot_general x1, matrix products, local(): lax.dot_general(down_local, hidden, (((0,), (1,)), ((), ())), preferred_e...  7.37 us
    dot_general x2, matrix products, fold_block(): jnp.einsum('qhmd,khmd->hmqk', query_group, key_heads, preferred_element_t...  4.85 us
    convert_element_type x1, other arithmetic, local(): value_block.reshape(key_count, head_local, VD).astype(jnp.float32)  4.08 us
  transfers between devices with their start and end apart: 5, of which 3 were waited for; matrix products, arithmetic and copies ran while one was open for 22% of the time, Pallas kernels for 0%

commit v1 on v0

v1 whole, which is shorter than its diff:
```python
import functools

import jax
import jax.numpy as jnp
from jax import lax
from jax.experimental import pallas as pl
from jax.experimental.pallas import tpu as pltpu
from jax.sharding import PartitionSpec as P


QKD = 128
VD = 256
TOP = 2


neg_big = -1e30
head_eps = 1e-05
moe_eps = 1e-06
head_scale = 0.8

VMEM = pl.BlockSpec(memory_space=pltpu.VMEM)
SMEM = pl.BlockSpec(memory_space=pltpu.SMEM)
HBM = pl.BlockSpec(memory_space=pltpu.HBM)


def struct(shape, dtype=jnp.bfloat16):
    return jax.ShapeDtypeStruct(shape, dtype)


def params(mib=8):
    return pltpu.CompilerParams(vmem_limit_bytes=mib * 1024 * 1024)


def dot(a, b, contract=((1,), (0,))):
    return lax.dot_general(a, b, (contract, ((), ())), preferred_element_type=jnp.float32)


def where_am_i(nx):
    ep = lax.axis_index("ep")
    return lax.div(ep, nx), lax.rem(ep, nx), lax.axis_index("tp")


def slot_hits(nz, nx, cap, routes):
    z, x, _ = where_am_i(nx)
    blocks, rows = nz * nx, routes.shape[1]
    block = lax.broadcasted_iota(jnp.int32, (blocks, rows), 0)
    wanted = (lax.div(block, nx) ^ z) * nx + (lax.rem(block, nx) ^ x)
    first, second = routes[0:1, :] == wanted, routes[1:2, :] == wanted
    hit = jnp.where(first | second, 1.0, 0.0)
    row_from = lax.broadcasted_iota(jnp.int32, (rows, rows), 0)
    row_to = lax.broadcasted_iota(jnp.int32, (rows, rows), 1)
    before = jnp.where(row_from < row_to, 1.0, 0.0).astype(jnp.bfloat16)
    place = jnp.where(hit > 0.5, dot(hit.astype(jnp.bfloat16), before), -1.0)
    slot = lax.broadcasted_iota(jnp.int32, (blocks, cap, rows), 1).astype(jnp.float32)
    return place[:, None, :] == slot, first


def prep_kernel(nz, nx, cap, width, wide, tokens_ref, gain_ref, routes_ref, *refs):
    blocks = nz * nx
    tokens_s, gain_s, sems = refs[-3:]
    copies = [
        pltpu.make_async_copy(tokens_ref, tokens_s, sems.at[0]),
        pltpu.make_async_copy(gain_ref, gain_s, sems.at[1]),
    ]
    slices = []
    if wide:
        z = where_am_i(nx)[0]
        sources, refs = refs[:3], refs[3:]
        count = sources[0].shape[0]
        for k in range(nz):
            columns = pl.ds(pl.multiple_of((z ^ k) * wide, wide), wide)
            for i, source in enumerate(sources):
                target = refs[blocks + k].at[pl.ds(i * count, count), :]
                sem = sems.at[2 + 3 * k + i]
                slices.append(pltpu.make_async_copy(source.at[:, columns], target, sem))
    out_refs = refs[:blocks]
    for copy in copies + slices:
        copy.start()
    rows = tokens_ref.shape[0]
    picker, _ = slot_hits(nz, nx, cap, routes_ref[...])
    picker = jnp.where(picker, 1.0, 0.0).reshape(blocks * cap, rows).astype(jnp.bfloat16)
    for copy in copies:
        copy.wait()
    tokens = tokens_s[...].astype(jnp.float32)
    scale = lax.rsqrt(jnp.mean(tokens * tokens, axis=-1, keepdims=True) + moe_eps)
    columns = pl.ds(pl.multiple_of(lax.axis_index("tp") * width, width), width)
    normed = tokens_s[:, columns].astype(jnp.float32) * scale * gain_s[:, columns]
    picked = dot(picker, normed.astype(jnp.bfloat16)).astype(jnp.bfloat16)
    for j in range(blocks):
        out_refs[j][...] = picked[j * cap : (j + 1) * cap]
    for copy in slices:
        copy.wait()


def gates_kernel(nz, nx, cap, routes_ref, scores_ref, high_ref, low_ref):
    rows = routes_ref.shape[1]
    scores = scores_ref[...]
    scores = jnp.exp(scores - jnp.max(scores, axis=0, keepdims=True))
    gates = scores / jnp.sum(scores, axis=0, keepdims=True)
    taken, first = slot_hits(nz, nx, cap, routes_ref[...])
    weight = jnp.where(first, gates[0:1, :], gates[1:2, :])
    weight = jnp.where(taken, weight[:, None, :], 0.0).reshape(nz * nx * cap, rows)
    high = weight.astype(jnp.bfloat16)
    high_ref[...] = high
    low_ref[...] = (weight - high.astype(jnp.float32)).astype(jnp.bfloat16)


def blend_kernel(nz, cap, n_sums, *refs):
    sum_refs, refs = refs[:n_sums], refs[n_sums:]
    attend_refs, near_ref, out_refs = refs[: nz - 1], refs[nz - 1], refs[nz:]
    total = sum_refs[0][...].astype(jnp.float32)
    for ref in sum_refs[1:]:
        total = total + ref[...].astype(jnp.float32)
    total = total.astype(jnp.bfloat16)
    near_ref[...] = total[:cap]
    for k in range(1, nz):
        out_ref = out_refs[k - 1]
        count, wide = attend_refs[k - 1].shape
        out_ref[:count, :] = attend_refs[k - 1][...]
        for c in range(total.shape[1] // wide):
            out_ref[count + c * cap : count + (c + 1) * cap, :] = total[
                k * cap : (k + 1) * cap, c * wide : (c + 1) * wide
            ]


def finish_kernel(nz, nx, cap, wide, high_ref, low_ref, *refs):
    blocks, refs = refs[: nz * nx], refs[nz * nx :]
    *refs, held, out_s, sems = refs
    copies = []
    if wide:
        own_ref, out_ref, attended_ref = refs
        z = where_am_i(nx)[0]
        count = own_ref.shape[0]
        for k in range(nz):
            source = blocks[k * nx].at[pl.ds(0, count), :] if k else own_ref
            columns = pl.ds(pl.multiple_of((z ^ k) * wide, wide), wide)
            copies.append(pltpu.make_async_copy(source, attended_ref.at[:, columns], sems.at[k]))
    else:
        (out_ref,) = refs
    for copy in copies:
        copy.start()
    for j, ref in enumerate(blocks):
        slots = slice(j * cap, (j + 1) * cap)
        if wide and j >= nx and j % nx == 0:
            for c in range(held.shape[1] // wide):
                first = count + c * cap
                held[slots, c * wide : (c + 1) * wide] = ref[first : first + cap, :]
        else:
            held[slots, :] = ref[...]
    returned = held[...]
    rows = ((0,), (0,))
    out_s[...] = (
        dot(high_ref[...], returned, rows) + dot(low_ref[...], returned, rows)
    ).astype(jnp.bfloat16)
    copies.append(pltpu.make_async_copy(out_s, out_ref, sems.at[nz]))
    copies[-1].start()
    for copy in copies:
        copy.wait()


def fence_kernel(in_ref, out_ref):
    out_ref[...] = in_ref[...]


def early_kernel(groups, tp_n, *refs):
    row_refs = refs[: 2 * groups]
    gate_ref, up_ref, down_ref = refs[2 * groups : 2 * groups + 3]
    gate_out, up_out, gate_late, up_late, down_late = refs[2 * groups + 3 : 2 * groups + 8]
    gate_s, up_s, sems = refs[2 * groups + 8 :]
    width = row_refs[0].shape[1]
    tp = lax.axis_index("tp")

    def block(q):
        return pl.ds(pl.multiple_of((tp ^ q) * width, width), width)

    early, late = [], []
    for q in range(tp_n):
        for which, (source, held, later) in enumerate(
            ((gate_ref, gate_s, gate_late), (up_ref, up_s, up_late))
        ):
            target = held.at[q] if q < 2 else later.at[q - 2]
            copy = pltpu.make_async_copy(source.at[block(q), :], target, sems.at[which, q])
            (early if q < 2 else late).append(copy)
    for q in range(tp_n):
        late.append(
            pltpu.make_async_copy(down_ref.at[:, block(q)], down_late.at[q], sems.at[2, q])
        )
    for copy in early + late:
        copy.start()
    gate, up = 0.0, 0.0
    for q in range(2):
        rows = [row_refs[q * groups + g][...] for g in range(groups)]
        rows = jnp.concatenate(rows, axis=0)
        early[2 * q].wait()
        gate = gate + dot(rows, gate_s[q])
        early[2 * q + 1].wait()
        up = up + dot(rows, up_s[q])
    gate_out[...] = gate
    up_out[...] = up
    for copy in late:
        copy.wait()


def late_kernel(groups, tp_n, *refs):
    n_in = (tp_n - 2) * groups
    row_refs = refs[:n_in]
    gate_in, up_in, gate_ref, up_ref, down_ref = refs[n_in : n_in + 5]
    out_refs = refs[n_in + 5 :]
    gate, up = gate_in[...], up_in[...]
    for q in range(tp_n - 2):
        rows = [row_refs[q * groups + g][...] for g in range(groups)]
        rows = jnp.concatenate(rows, axis=0)
        gate = gate + dot(rows, gate_ref[q])
        up = up + dot(rows, up_ref[q])
    hidden = (gate * jax.nn.sigmoid(gate) * up).astype(jnp.bfloat16)
    size = hidden.shape[0] // groups
    for q in range(tp_n):
        result = dot(hidden, down_ref[q]).astype(jnp.bfloat16)
        for g in range(groups):
            out_refs[q * groups + g][...] = result[g * size : (g + 1) * size]


def attend_kernel(nz, nx, heads, place_ref, lambda_ref, gain_ref, *refs):
    pack_refs = refs[:nz]
    near_refs = refs[nz : nz + nx - 1]
    rest_refs = refs[nz + nx - 1 : nz + 2 * (nx - 1)]
    out_refs = refs[nz + 2 * (nx - 1) : 2 * nz + 2 * (nx - 1)]
    query_s, key_s, value_s, out_s = refs[2 * nz + 2 * (nx - 1) :]
    z, x = place_ref[0], place_ref[1]
    rows = pack_refs[0].shape[0] // 3

    def at(block):
        return pl.ds(pl.multiple_of(block * rows, rows), rows)

    for k in range(nz):
        query_s[at(z ^ k), :] = pack_refs[k][2 * rows :, :]
        for m in range(nx):
            if m == 0:
                source, first = pack_refs[k], 0
            elif k == 0:
                source, first = near_refs[m - 1], 0
            else:
                source, first = rest_refs[m - 1], (k - 1) * 2 * rows
            block = at((z ^ k) * nx + (x ^ m))
            key_s[block, :] = source[first : first + rows, :]
            value_s[block, :] = source[first + rows : first + 2 * rows, :]
    for head in range(heads):
        weight = lambda_ref[z * heads + head]
        for group in range(nz):
            count = (group + 1) * nx * rows
            query_pos = (group * nx + x) * rows + lax.broadcasted_iota(jnp.int32, (rows, count), 0)
            visible = lax.broadcasted_iota(jnp.int32, (rows, count), 1) <= query_pos
            maps = []
            for index in range(2):
                lanes = slice(head * VD + index * QKD, head * VD + (index + 1) * QKD)
                scores = dot(
                    query_s[group * rows : (group + 1) * rows, lanes],
                    key_s[:count, lanes],
                    ((1,), (1,)),
                )
                scores = jnp.where(visible, scores * QKD ** (-0.5), neg_big)
                weights = jnp.exp(scores - jnp.max(scores, axis=-1, keepdims=True))
                maps.append((weights, jnp.sum(weights, axis=-1, keepdims=True)))
            mixing = maps[0][0] * (1.0 / maps[0][1]) - maps[1][0] * (weight / maps[1][1])
            lanes = slice(head * VD, (head + 1) * VD)
            high = mixing.astype(jnp.bfloat16)
            low = (mixing - high.astype(jnp.float32)).astype(jnp.bfloat16)
            held = value_s[:count, lanes]
            mixed = dot(high, held) + dot(low, held)
            scaled = mixed * lax.rsqrt(jnp.mean(mixed * mixed, axis=-1, keepdims=True) + head_eps)
            scaled = scaled * gain_ref[...] * head_scale
            out_s[group * rows : (group + 1) * rows, lanes] = scaled.astype(jnp.bfloat16)
    for k in range(nz):
        out_refs[k][...] = out_s[at(z ^ k), :]


def fold_block(query_group, query_pos, key_heads, value_heads, key_pos):
    scores = jnp.einsum(
        "qhmd,khmd->hmqk", query_group, key_heads, preferred_element_type=jnp.float32
    ) * QKD ** (-0.5)
    visible = key_pos[None, :] <= query_pos[:, None]
    scores = jnp.where(visible, scores, neg_big)
    weights = jnp.where(visible, jnp.exp(scores - jnp.max(scores, axis=-1, keepdims=True)), 0.0)
    accumulated = jnp.einsum(
        "hmqk,khd->hmqd", weights, value_heads, precision=lax.Precision.HIGHEST
    )
    return jnp.sum(weights, axis=-1), accumulated


def gathered_attention(queries, key_rows, values, lambdas, head_gain):
    rows = queries.shape[0]
    heads = lambdas.shape[0]
    half = rows // 2
    keys = lax.all_gather(key_rows, "ep", axis=0, tiled=True)
    held = lax.all_gather(values, "ep", axis=0, tiled=True)
    count = keys.shape[0]
    keys = keys.reshape(count, heads, 2, QKD)
    held = held.reshape(count, heads, VD).astype(jnp.float32)
    key_pos = jnp.arange(count, dtype=jnp.int32)
    groups = []
    for g in range(2):
        pos = lax.axis_index("ep") * rows + g * half + jnp.arange(half, dtype=jnp.int32)
        group = queries[g * half : (g + 1) * half].reshape(half, heads, 2, QKD)
        total, mixed = fold_block(group, pos, keys, held, key_pos)
        mixed = mixed / total[..., None]
        mixed = mixed[:, 0] - lambdas[:, None, None] * mixed[:, 1]
        scaled = mixed * lax.rsqrt(jnp.mean(mixed * mixed, axis=-1, keepdims=True) + head_eps)
        scaled = scaled * head_gain * head_scale
        groups.append(scaled.transpose(1, 0, 2).reshape(half, heads * VD).astype(jnp.bfloat16))
    return jnp.concatenate(groups, axis=0)


def local(
    sizes,
    queries,
    key_rows,
    values,
    lambdas,
    head_gain,
    tokens,
    moe_gain,
    routes,
    route_scores,
    w_gate,
    w_up,
    w_down,
):
    nz, nx, tp_n = sizes
    ep_n = nz * nx
    ep = lax.axis_index("ep")
    place = jnp.stack([ep // nx, ep % nx]).astype(jnp.int32)
    rows_b, model = tokens.shape
    cap = 2 * TOP * rows_b // ep_n
    width = model // tp_n
    units = w_gate.shape[2]

    def shift(v, axis, mask):
        if mask == 0:
            return v
        n = ep_n if axis == "ep" else tp_n
        return lax.ppermute(v, axis, [(i, i ^ mask) for i in range(n)])

    def kernel(body, ins, outs, in_specs=None, out_specs=None, scratch=(), mib=8):
        if in_specs:
            ins = [
                pltpu.with_memory_space_constraint(v, pltpu.HBM) if spec is HBM else v
                for v, spec in zip(ins, in_specs)
            ]
        return pl.pallas_call(
            body,
            out_shape=outs,
            in_specs=in_specs or [VMEM] * len(ins),
            out_specs=out_specs or jax.tree.map(lambda _: VMEM, outs),
            scratch_shapes=scratch,
            compiler_params=params(mib),
        )(*ins)

    heads, odd = divmod(lambdas.shape[0], nz)
    wide = 0 if odd or width % (heads * VD) else heads * VD
    rows_a = queries.shape[0]
    slices = (key_rows, values, queries) if wide else ()
    sends = kernel(
        functools.partial(prep_kernel, nz, nx, cap, width, wide),
        (tokens, moe_gain.reshape(1, model), routes.T, *slices),
        [struct((cap, width))] * ep_n + [struct((3 * rows_a, wide))] * (nz if wide else 0),
        in_specs=[HBM, HBM, VMEM] + [HBM] * len(slices),
        scratch=[
            pltpu.VMEM((rows_b, model), jnp.bfloat16),
            pltpu.VMEM((1, model), jnp.float32),
            pltpu.SemaphoreType.DMA((2 + 3 * nz,)),
        ],
    )
    sends, packs = sends[:ep_n], sends[ep_n:]
    order = list(range(1, nx)) + [0]
    parts = {}
    for m in order:
        arrived = [shift(sends[k * nx + m], "ep", k * nx + m) for k in range(nz)]
        parts[0, m] = jnp.concatenate(arrived, axis=0)

    packs = [shift(pack, "ep", k * nx) for k, pack in enumerate(packs)]

    for q in range(0, tp_n, 2):
        for m in order:
            parts[q, m] = shift(parts[0, m], "tp", q)
            parts[q + 1, m] = shift(parts[q, m], "tp", 1)

    attended = None
    if wide:
        near = packs[0][: 2 * rows_a]
        rest = jnp.concatenate([pack[: 2 * rows_a] for pack in packs[1:]], axis=0)
        near = [shift(near, "ep", m) for m in range(1, nx)]
        rest = [shift(rest, "ep", m) for m in range(1, nx)]
        gain = kernel(fence_kernel, (head_gain.reshape(1, VD),), struct((1, VD), jnp.float32))
        outs = kernel(
            functools.partial(attend_kernel, nz, nx, heads),
            (place, lambdas, gain, *packs, *near, *rest),
            [struct((rows_a, wide))] * nz,
            in_specs=[SMEM, SMEM] + [VMEM] * (1 + nz + 2 * (nx - 1)),
            scratch=[
                pltpu.VMEM((nz * rows_a, wide), jnp.bfloat16),
                pltpu.VMEM((ep_n * rows_a, wide), jnp.bfloat16),
                pltpu.VMEM((ep_n * rows_a, wide), jnp.bfloat16),
                pltpu.VMEM((nz * rows_a, wide), jnp.bfloat16),
            ],
            mib=16,
        )
    else:
        attended = gathered_attention(queries, key_rows, values, lambdas, head_gain)

    slots = ep_n * cap
    gate, up, *late = kernel(
        functools.partial(early_kernel, nx, tp_n),
        (*[parts[q, m] for q in range(2) for m in order], w_gate[0], w_up[0], w_down[0]),
        [
            struct((slots, units), jnp.float32),
            struct((slots, units), jnp.float32),
            struct((tp_n - 2, width, units)),
            struct((tp_n - 2, width, units)),
            struct((tp_n, units, width)),
        ],
        in_specs=[VMEM] * (2 * nx) + [HBM] * 3,
        scratch=[
            pltpu.VMEM((2, width, units), jnp.bfloat16),
            pltpu.VMEM((2, width, units), jnp.bfloat16),
            pltpu.SemaphoreType.DMA((3, tp_n)),
        ],
        mib=20,
    )
    results = kernel(
        functools.partial(late_kernel, nx, tp_n),
        (*[parts[q, m] for q in range(2, tp_n) for m in order], gate, up, *late),
        [struct((slots // nx, width))] * (tp_n * nx),
        mib=20,
    )

    returned = {}
    for g, m in enumerate(order):
        pieces = []
        for q in list(range(2, tp_n, 2)) + [0]:
            own = results[q * nx + g]
            other = shift(results[(q + 1) * nx + g], "tp", 1)
            if q:
                piece = own.astype(jnp.float32) + other.astype(jnp.float32)
                pieces.append(shift(piece.astype(jnp.bfloat16), "tp", q))
            else:
                pieces += [own, other]
        if wide and m == 0:
            returned[0, 0], *mixed = kernel(
                functools.partial(blend_kernel, nz, cap, len(pieces)),
                (*pieces, *outs[1:]),
                [struct((cap, width))]
                + [struct((rows_a + cap * width // wide, wide))] * (nz - 1),
            )
            for k in range(1, nz):
                returned[k, 0] = shift(mixed[k - 1], "ep", k * nx)
        else:
            total = sum(piece.astype(jnp.float32) for piece in pieces).astype(jnp.bfloat16)
            for k in range(nz):
                block = total[k * cap : (k + 1) * cap]
                returned[k, m] = shift(block, "ep", k * nx + m)

    high, low = kernel(
        functools.partial(gates_kernel, nz, nx, cap),
        (routes.T, route_scores.T),
        [struct((slots, rows_b))] * 2,
    )
    shapes = [struct((rows_b, width))] + [struct((rows_a, nz * wide))] * (wide > 0)
    out, *held = kernel(
        functools.partial(finish_kernel, nz, nx, cap, wide),
        (
            high,
            low,
            *[returned[k, m] for k in range(nz) for m in range(nx)],
            *(outs[:1] if wide else ()),
        ),
        shapes,
        out_specs=[HBM] * len(shapes),
        scratch=[
            pltpu.VMEM((slots, width), jnp.bfloat16),
            pltpu.VMEM((rows_b, width), jnp.bfloat16),
            pltpu.SemaphoreType.DMA((nz + 1,)),
        ],
    )
    return held[0] if wide else attended, out


def solution(mesh):
    ep_n, tp_n = mesh.shape["ep"], mesh.shape["tp"]
    nx = 1
    while (2 * nx) * (2 * nx) <= ep_n:
        nx *= 2
    sizes = (ep_n // nx, nx, tp_n)

    def body(*arrays):
        return local(sizes, *arrays)

    return jax.shard_map(
        body,
        mesh=mesh,
        in_specs=(
            P("ep", "tp"),
            P("ep", "tp"),
            P("ep", "tp"),
            P("tp"),
            P(),
            P("ep", None),
            P(),
            P("ep", None),
            P("ep", None),
            P("ep", None, "tp"),
            P("ep", None, "tp"),
            P("ep", "tp", None),
        ),
        out_specs=(P("ep", "tp"), P("ep", "tp")),
        check_vma=False,
    )
```

time: 191 us -> 101 us (0.53)
  waiting for transfers between devices: 116 us -> 38.7 us
  starting transfers between devices: 11 us -> 44.8 us
  matrix products: 26.5 us -> 0 us
  between operations: 17.1 us -> 0.9 us
  Pallas kernels: 0 us -> 13.3 us
  local copies, waits for them, and re-layouts: 10.5 us -> 0.81 us
  other arithmetic: 9.63 us -> 2.05 us
    all_to_all x2 -> x0, waiting for transfers between devices: 82.3 us -> none  [the longest x1 69.8 us: local(): lax.all_to_all(outgoing, 'ep', split_axis=0, concat_axis=0, tiled=True)]
    ppermute x0 -> x31, starting transfers between devices: none -> 44.8 us  [shift(): return lax.ppermute(v, axis, [(i, i ^ mask) for i in range(n)])]
    ppermute x0 -> x31, waiting for transfers between devices: none -> 38.7 us  [shift(): return lax.ppermute(v, axis, [(i, i ^ mask) for i in range(n)])]
    all_gather x2 -> x0, waiting for transfers between devices: 33.2 us -> none  [the longest x1 33.2 us: local(): key_block = lax.all_gather(key_rows, 'ep', axis=0, tiled=True)]
    dot_general x8 -> x0, matrix products: 26.5 us -> none  [the longest x2 9.67 us: fold_block(): jnp.einsum('hmqk,khd->hmqd', weights, value_heads, precision=lax.Precisio...]
    pallas_call x0 -> x8, Pallas kernels: none -> 13.3 us  [kernel(): pl.pallas_call(body, out_shape=outs, in_specs=in_specs or [VMEM] * len(in...]
    all_to_all x2 -> x0, starting transfers between devices: 10.9 us -> none  [the longest x1 7.41 us: local(): lax.all_to_all(outgoing, 'ep', split_axis=0, concat_axis=0, tiled=True)]
    convert_element_type x3, other arithmetic: 5.08 us -> 1.21 us  [the longest x2 1.08 us: local(): pieces.append(shift(piece.astype(jnp.bfloat16), 'tp', q))]
  transfers between devices with their start and end apart: 5 -> 31, of which waited for: 3 -> 9; matrix products, arithmetic and copies ran while one was open for 22% -> 2% of each run, Pallas kernels for 0% -> 11%
where the time goes in v1:
time: 101 us
  starting transfers between devices  44.8 us (44%)
  waiting for transfers between devices  38.7 us (38%)
  Pallas kernels  13.3 us (13%)
  other arithmetic  2.05 us (2%)
    ppermute x31, starting transfers between devices, shift(): return lax.ppermute(v, axis, [(i, i ^ mask) for i in range(n)])  44.8 us
    ppermute x31, waiting for transfers between devices, shift(): return lax.ppermute(v, axis, [(i, i ^ mask) for i in range(n)])  38.7 us
    pallas_call x8, Pallas kernels, kernel(): pl.pallas_call(body, out_shape=outs, in_specs=in_specs or [VMEM] * len(in...  13.3 us
  transfers between devices with their start and end apart: 31, of which 9 were waited for; matrix products, arithmetic and copies ran while one was open for 2% of the time, Pallas kernels for 11%

profile of v1, /device:TPU:0, one launch (start us, length us, event | category | flops | bytes accessed | tf_op | source)
XLA Modules:
  0.0 100.6 jit_solution(9110003986372901847)
XLA Ops:
  0.6 0.0 copy-start
  0.6 0.7 copy-done
  1.3 1.7 %shard_map.132 = (bf16[32,1024]{1,0:T(8,128)(2,1)S(1)}, bf16[32,1024]{1,0:T(8,128)(2,1)S(1)}, bf16[32,1024]{1,0:T(8,128)(2,1)S(1)}, bf16[32,1024]{1,0:T(8,128)(2...) custom-call(bf16[64,4096]{1,0:T(8,128)(2,1)} %tokens_ref.1, ...), custom_call_target="tpu_custom_call" | custom-call | tf_op jit(solution)/shard_map/pallas_call | solution.py:349
  3.0 3.0 %collective-permute-start = (bf16[32,1024]{1,0:T(8,128)(2,1)S(1)}, bf16[32,1024]{1,0:T(8,128)(2,1)S(1)}, u32[]{:S(2)}, u32[]{:S(2)}) collective-permute-start(bf16[32,1024]{1,0:T(8,128)(2,1)S(1)} %get-tuple-element.41), channel_id=1, source_target_pairs={{0,4},{4,0},{8,12},{12,8},{16,20},{20,16},{24,28},{28,24},{1,5},{5... | collective-permute-start | bytes 196616 | tf_op jit(solution)/shard_map/ppermute | solution.py:341
  6.0 1.5 %collective-permute-start.1 = (bf16[32,1024]{1,0:T(8,128)(2,1)S(1)}, bf16[32,1024]{1,0:T(8,128)(2,1)S(1)}, u32[]{:S(2)}, u32[]{:S(2)}) collective-permute-start(bf16[32,1024]{1,0:T(8,128)(2,1)S(1)} %get-tuple-element.42), channel_id=1, source_target_pairs={{0,12},{4,8},{8,4},{12,0},{16,28},{20,24},{24,20},{28,16},{1,13},{... | collective-permute-start | bytes 196616 | tf_op jit(solution)/shard_map/ppermute | solution.py:341
  7.6 3.5 %collective-permute-start.2 = (bf16[32,1024]{1,0:T(8,128)(2,1)S(1)}, bf16[32,1024]{1,0:T(8,128)(2,1)S(1)}, u32[]{:S(2)}, u32[]{:S(2)}) collective-permute-start(bf16[32,1024]{1,0:T(8,128)(2,1)S(1)} %get-tuple-element.43), channel_id=1, source_target_pairs={{0,20},{4,16},{8,28},{12,24},{16,4},{20,0},{24,12},{28,8},{1,21},{... | collective-permute-start | bytes 196616 | tf_op jit(solution)/shard_map/ppermute | solution.py:341
  11.1 0.9 collective-permute-start.5
  12.0 4.1 %collective-permute-done.5 = bf16[32,1024]{1,0:T(8,128)(2,1)S(1)} collective-permute-done((bf16[32,1024]{1,0:T(8,128)(2,1)S(1)}, bf16[32,1024]{1,0:T(8,128)(2,1)S(1)}, u32[]{:S(2)}, u32[]{:S(2)}) %collective-permute-start.5) | collective-permute-done | bytes 65568 | tf_op jit(solution)/shard_map/ppermute | solution.py:341
  16.1 2.3 %collective-permute-start.6 = (bf16[32,1024]{1,0:T(8,128)(2,1)S(1)}, bf16[32,1024]{1,0:T(8,128)(2,1)S(1)}, u32[]{:S(2)}, u32[]{:S(2)}) collective-permute-start(bf16[32,1024]{1,0:T(8,128)(2,1)S(1)} %get-tuple-element.47), channel_id=1, source_target_pairs={{0,16},{4,20},{8,24},{12,28},{16,0},{20,4},{24,8},{28,12},{1,17},{... | collective-permute-start | bytes 196616 | tf_op jit(solution)/shard_map/ppermute | solution.py:341
  18.4 3.6 %collective-permute-done.6 = bf16[32,1024]{1,0:T(8,128)(2,1)S(1)} collective-permute-done((bf16[32,1024]{1,0:T(8,128)(2,1)S(1)}, bf16[32,1024]{1,0:T(8,128)(2,1)S(1)}, u32[]{:S(2)}, u32[]{:S(2)}) %collective-permute-start.6) | collective-permute-done | bytes 65568 | tf_op jit(solution)/shard_map/ppermute | solution.py:341
  22.0 3.9 %collective-permute-start.7 = (bf16[32,1024]{1,0:T(8,128)(2,1)S(1)}, bf16[32,1024]{1,0:T(8,128)(2,1)S(1)}, u32[]{:S(2)}, u32[]{:S(2)}) collective-permute-start(bf16[32,1024]{1,0:T(8,128)(2,1)S(1)} %get-tuple-element.48), channel_id=1, source_target_pairs={{0,24},{4,28},{8,16},{12,20},{16,8},{20,12},{24,0},{28,4},{1,25},{... | collective-permute-start | bytes 196616 | tf_op jit(solution)/shard_map/ppermute | solution.py:341
  25.8 2.2 %collective-permute-done.7 = bf16[32,1024]{1,0:T(8,128)(2,1)S(1)} collective-permute-done((bf16[32,1024]{1,0:T(8,128)(2,1)S(1)}, bf16[32,1024]{1,0:T(8,128)(2,1)S(1)}, u32[]{:S(2)}, u32[]{:S(2)}) %collective-permute-start.7) | collective-permute-done | bytes 65568 | tf_op jit(solution)/shard_map/ppermute | solution.py:341
  28.1 1.5 %collective-permute-start.8 = (bf16[128,1024]{1,0:T(8,128)(2,1)S(1)}, bf16[128,1024]{1,0:T(8,128)(2,1)S(1)}, u32[]{:S(2)}, u32[]{:S(2)}) collective-permute-start(bf16[128,1024]{1,0:T(8,128)(2,1)S(1)} %constant_dynamic-update-slice_fusion.4.refs_1_), channel_id=1, source_target_pairs={{0,2},{1,3},{2,0},{3,1},{4,6},{5,7},{6,4},{7,5},{8,10},{9,11},{10,... | collective-permute-start | bytes 786440 | tf_op jit(solution)/shard_map/ppermute | solution.py:341
  29.6 0.0 collective-permute-done
  29.6 0.0 collective-permute-done.1
  29.6 0.0 collective-permute-done.2
  29.7 0.6 collective-permute-start.4
  30.3 0.5 collective-permute-start.11
  30.8 3.7 %collective-permute-done.8.refs_1_ = bf16[128,1024]{1,0:T(8,128)(2,1)S(1)} collective-permute-done((bf16[128,1024]{1,0:T(8,128)(2,1)S(1)}, bf16[128,1024]{1,0:T(8,128)(2,1)S(1)}, u32[]{:S(2)}, u32[]{:S(2)}) %collective-permute-start.8) | collective-permute-done | bytes 262176 | tf_op jit(solution)/shard_map/ppermute | solution.py:341
  34.5 0.0 collective-permute-start.10
  34.5 2.8 %collective-permute-done.4.refs_0_ = bf16[128,1024]{1,0:T(8,128)(2,1)S(1)} collective-permute-done((bf16[128,1024]{1,0:T(8,128)(2,1)S(1)}, bf16[128,1024]{1,0:T(8,128)(2,1)S(1)}, u32[]{:S(2)}, u32[]{:S(2)}) %collective-permute-start.4) | collective-permute-done | bytes 262176 | tf_op jit(solution)/shard_map/ppermute | solution.py:341
  37.3 0.0 collective-permute-start.16
  37.3 0.0 collective-permute-done.12.refs_3_
  37.3 4.3 %collective-permute-start.17 = (bf16[384,256]{1,0:T(8,128)(2,1)S(1)}, bf16[384,256]{1,0:T(8,128)(2,1)S(1)}, u32[]{:S(2)}, u32[]{:S(2)}) collective-permute-start(bf16[384,256]{1,0:T(8,128)(2,1)S(1)} %get-tuple-element.60), channel_id=1, source_target_pairs={{0,16},{4,20},{8,24},{12,28},{16,0},{20,4},{24,8},{28,12},{1,17},{... | collective-permute-start | bytes 589832 | tf_op jit(solution)/shard_map/ppermute | solution.py:341
  41.7 0.0 collective-permute-done.11.refs_2_
  41.7 0.1 collective-permute-start.18
  41.7 4.7 %shard_map.133 = (f32[256,512]{1,0:T(8,128)S(1)}, f32[256,512]{1,0:T(8,128)S(1)}, bf16[2,1024,512]{2,1,0:T(8,128)(2,1)S(1)}, bf16[2,1024,512]{2,1,0:T(8,128)(2,1)S(1)}, bf16[4,512,1024]{2,1,0:T(8,128)(2,1)S(1)}) custom-call(bf16[128,1024]{1,0:T(8,128)(2,1)S(1)} %constant_dynamic-update-slice_fusion.refs_0_, ...), custom_call_target="tpu_custom_call" | custom-call | tf_op jit(solution)/shard_map/pallas_call | solution.py:349
  46.5 0.0 copy-start.2
  46.5 0.0 copy-start.4
  46.5 2.4 %shard_map.134 = (bf16[128,1024]{1,0:T(8,128)(2,1)S(1)}, bf16[128,1024]{1,0:T(8,128)(2,1)S(1)}, bf16[128,1024]{1,0:T(8,128)(2,1)S(1)}, bf16[128,1024]{1,0:T(8,12...) custom-call(bf16[128,1024]{1,0:T(8,128)(2,1)S(1)} %collective-permut, ...), custom_call_target="tpu_custom_call" | custom-call | tf_op jit(solution)/shard_map/pallas_call | solution.py:349
  48.9 0.0 copy-start.1
  48.9 0.0 copy-start.3
  48.9 0.1 collective-permute-start.21
  49.0 0.0 collective-permute-done.16.refs_1_
  49.1 6.8 %collective-permute-done.17.refs_2_ = bf16[384,256]{1,0:T(8,128)(2,1)S(1)} collective-permute-done((bf16[384,256]{1,0:T(8,128)(2,1)S(1)}, bf16[384,256]{1,0:T(8,128)(2,1)S(1)}, u32[]{:S(2)}, u32[]{:S(2)}) %collective-permute-start.17) | collective-permute-done | bytes 196640 | tf_op jit(solution)/shard_map/ppermute | solution.py:341
  55.9 0.8 pad_maximum_fusion
  56.7 1.3 %collective-permute-start.20 = (bf16[768,256]{1,0:T(8,128)(2,1)}, bf16[768,256]{1,0:T(8,128)(2,1)S(1)}, u32[]{:S(2)}, u32[]{:S(2)}) collective-permute-start(bf16[768,256]{1,0:T(8,128)(2,1)} %pad_maximum_fusion), channel_id=1, source_target_pairs={{0,4},{4,0},{8,12},{12,8},{16,20},{20,16},{24,28},{28,24},{1,5},{5... | collective-permute-start | bytes 1179656 | tf_op jit(solution)/shard_map/ppermute | solution.py:341
  58.0 0.8 collective-permute-start.19
  58.8 0.0 collective-permute-start.13
  58.8 0.5 collective-permute-start.23
  59.3 1.0 %add_convert_fusion.1 = bf16[128,1024]{1,0:T(8,128)(2,1)S(1)} fusion(bf16[128,1024]{1,0:T(8,128)(2,1)} %collective-permute-done.21, bf16[128,1024]{1,0:T(8,128)(2,1)S(1)} %get-tuple-element.66), kind=kLoop, calls=%fused_computation.1 | loop fusion | flops 524288 | bytes 786432 | tf_op jit(solution)/shard_map/convert_element_type | solution.py:444
  60.3 1.6 %collective-permute-start.22 = (bf16[128,1024]{1,0:T(8,128)(2,1)S(1)}, bf16[128,1024]{1,0:T(8,128)(2,1)S(1)}, u32[]{:S(2)}, u32[]{:S(2)}) collective-permute-start(bf16[128,1024]{1,0:T(8,128)(2,1)S(1)} %add_convert_fusion.1), channel_id=1, source_target_pairs={{0,2},{1,3},{2,0},{3,1},{4,6},{5,7},{6,4},{7,5},{8,10},{9,11},{10,... | collective-permute-start | bytes 786440 | tf_op jit(solution)/shard_map/ppermute | solution.py:341
  61.9 0.1 pad_add_fusion.place_ref
  62.0 7.9 %collective-permute-done.19.refs_4_ = bf16[256,256]{1,0:T(8,128)(2,1)S(1)} collective-permute-done((bf16[256,256]{1,0:T(8,128)(2,1)S(1)}, bf16[256,256]{1,0:T(8,128)(2,1)S(1)}, u32[]{:S(2)}, u32[]{:S(2)}) %collective-permute-start.19) | collective-permute-done | bytes 131104 | tf_op jit(solution)/shard_map/ppermute | solution.py:341
  69.9 3.2 %shard_map.136 = (bf16[128,256]{1,0:T(8,128)(2,1)S(1)}, bf16[128,256]{1,0:T(8,128)(2,1)S(1)}, bf16[128,256]{1,0:T(8,128)(2,1)S(1)}, bf16[128,256]{1,0:T(8,128)(2,1)S(1)}) custom-call(s32[2]{0:T(128)S(1)} %pad_add_fusion.place_ref, f32[4]{0:T(128)S(1)} %copy-done.4, f32[1,256]{1,0:T(1,128)S(1)} %shard_map.135.gain_ref, ...), custom_call_target="tpu_custom_call" | custom-call | tf_op jit(solution)/shard_map/pallas_call | solution.py:349
  73.1 0.0 collective-permute-done.13
  73.1 0.1 add_convert_fusion.2
  73.2 1.6 %collective-permute-start.14 = (bf16[128,1024]{1,0:T(8,128)(2,1)S(1)}, bf16[128,1024]{1,0:T(8,128)(2,1)S(1)}, u32[]{:S(2)}, u32[]{:S(2)}) collective-permute-start(bf16[128,1024]{1,0:T(8,128)(2,1)S(1)} %add_convert_fusion.2), channel_id=1, source_target_pairs={{0,2},{1,3},{2,0},{3,1},{4,6},{5,7},{6,4},{7,5},{8,10},{9,11},{10,... | collective-permute-start | bytes 786440 | tf_op jit(solution)/shard_map/ppermute | solution.py:341
  74.8 0.0 collective-permute-done.23
  74.8 0.0 collective-permute-done.22
  74.8 0.1 add_convert_fusion
  74.9 3.1 %collective-permute-start.30 = (bf16[32,1024]{1,0:T(8,128)(2,1)S(1)}, bf16[32,1024]{1,0:T(8,128)(2,1)S(1)}, u32[]{:S(2)}, u32[]{:S(2)}) collective-permute-start(bf16[32,1024]{1,0:T(8,128)(2,1)S(1)} %get-tuple-element.76), channel_id=1, source_target_pairs={{0,28},{4,24},{8,20},{12,16},{16,12},{20,8},{24,4},{28,0},{1,29},{... | collective-permute-start | bytes 196616 | tf_op jit(solution)/shard_map/ppermute | solution.py:341
  78.1 4.1 %collective-permute-start.28 = (bf16[32,1024]{1,0:T(8,128)(2,1)S(1)}, bf16[32,1024]{1,0:T(8,128)(2,1)S(1)}, u32[]{:S(2)}, u32[]{:S(2)}) collective-permute-start(bf16[32,1024]{1,0:T(8,128)(2,1)S(1)} %get-tuple-element.77), channel_id=1, source_target_pairs={{0,20},{4,16},{8,28},{12,24},{16,4},{20,0},{24,12},{28,8},{1,21},{... | collective-permute-start | bytes 196616 | tf_op jit(solution)/shard_map/ppermute | solution.py:341
  82.1 0.1 shard_map.137
  82.2 4.7 %collective-permute-start.25 = (bf16[256,256]{1,0:T(8,128)(2,1)S(1)}, bf16[256,256]{1,0:T(8,128)(2,1)S(1)}, u32[]{:S(2)}, u32[]{:S(2)}) collective-permute-start(bf16[256,256]{1,0:T(8,128)(2,1)S(1)} %get-tuple-element.70), channel_id=1, source_target_pairs={{0,8},{4,12},{8,0},{12,4},{16,24},{20,28},{24,16},{28,20},{1,9},{5... | collective-permute-start | bytes 393224 | tf_op jit(solution)/shard_map/ppermute | solution.py:341
  86.9 0.9 collective-permute-start.27
  87.8 1.5 %collective-permute-start.29 = (bf16[256,256]{1,0:T(8,128)(2,1)S(1)}, bf16[256,256]{1,0:T(8,128)(2,1)S(1)}, u32[]{:S(2)}, u32[]{:S(2)}) collective-permute-start(bf16[256,256]{1,0:T(8,128)(2,1)S(1)} %get-tuple-element.72), channel_id=1, source_target_pairs={{0,24},{4,28},{8,16},{12,20},{16,8},{20,12},{24,0},{28,4},{1,25},{... | collective-permute-start | bytes 393224 | tf_op jit(solution)/shard_map/ppermute | solution.py:341
  89.3 0.0 collective-permute-done.30.refs_7_
  89.3 1.8 %collective-permute-start.26 = (bf16[32,1024]{1,0:T(8,128)(2,1)S(1)}, bf16[32,1024]{1,0:T(8,128)(2,1)S(1)}, u32[]{:S(2)}, u32[]{:S(2)}) collective-permute-start(bf16[32,1024]{1,0:T(8,128)(2,1)S(1)} %get-tuple-element.78), channel_id=1, source_target_pairs={{0,12},{4,8},{8,4},{12,0},{16,28},{20,24},{24,20},{28,16},{1,13},{... | collective-permute-start | bytes 196616 | tf_op jit(solution)/shard_map/ppermute | solution.py:341
  91.1 0.7 collective-permute-start.24
  91.9 0.2 shard_map.131
  92.0 4.5 %collective-permute-done.26.refs_3_ = bf16[32,1024]{1,0:T(8,128)(2,1)S(1)} collective-permute-done((bf16[32,1024]{1,0:T(8,128)(2,1)S(1)}, bf16[32,1024]{1,0:T(8,128)(2,1)S(1)}, u32[]{:S(2)}, u32[]{:S(2)}) %collective-permute-start.26) | collective-permute-done | bytes 65568 | tf_op jit(solution)/shard_map/ppermute | solution.py:341
  96.5 3.0 %collective-permute-done.27.refs_4_ = bf16[256,256]{1,0:T(8,128)(2,1)S(1)} collective-permute-done((bf16[256,256]{1,0:T(8,128)(2,1)S(1)}, bf16[256,256]{1,0:T(8,128)(2,1)S(1)}, u32[]{:S(2)}, u32[]{:S(2)}) %collective-permute-start.27) | collective-permute-done | bytes 131104 | tf_op jit(solution)/shard_map/ppermute | solution.py:341
  99.6 1.0 %shard_map.138 = (bf16[64,1024]{1,0:T(8,128)(2,1)}, bf16[128,1024]{1,0:T(8,128)(2,1)}) custom-call(bf16[256,64]{1,0:T(8,128)(2,1)S(1)} %get-tuple-element.39.high_ref, bf16[256,64]{1,0:T(8,128)(2,1)S(1)} %get-tuple-element.40.low_ref, bf16[32,1024]{1,0:T(8,128)(2,1)S(1)} %get-tuple-element.65.refs_0_, bf16[32,1024]{1,0:T(8,128)(2,1)S(1)} %collective-permute-done.24.refs_1_, ...), custom_call_target="tpu_custom_call" | custom-call | tf_op jit(solution)/shard_map/pallas_call | solution.py:349
  (34 shorter events, 0.2 us)
Async XLA Ops:
  0.6 0.7 copy-start
  3.0 26.6 %collective-permute-start = (bf16[32,1024]{1,0:T(8,128)(2,1)S(1)}, bf16[32,1024]{1,0:T(8,128)(2,1)S(1)}, u32[]{:S(2)}, u32[]{:S(2)}) collective-permute-start(bf16[32,1024]{1,0:T(8,128)(2,1)S(1)} %get-tuple-element.41), channel_id=1, source_target_pairs={{0,4},{4,0},{8,12},{12,8},{16,20},{20,16},{24,28},{28,24},{1,5},{5... | collective-permute-start | bytes 196616 | tf_op jit(solution)/shard_map/ppermute | solution.py:341
  6.0 23.6 %collective-permute-start.1 = (bf16[32,1024]{1,0:T(8,128)(2,1)S(1)}, bf16[32,1024]{1,0:T(8,128)(2,1)S(1)}, u32[]{:S(2)}, u32[]{:S(2)}) collective-permute-start(bf16[32,1024]{1,0:T(8,128)(2,1)S(1)} %get-tuple-element.42), channel_id=1, source_target_pairs={{0,12},{4,8},{8,4},{12,0},{16,28},{20,24},{24,20},{28,16},{1,13},{... | collective-permute-start | bytes 196616 | tf_op jit(solution)/shard_map/ppermute | solution.py:341
  7.6 22.1 %collective-permute-start.2 = (bf16[32,1024]{1,0:T(8,128)(2,1)S(1)}, bf16[32,1024]{1,0:T(8,128)(2,1)S(1)}, u32[]{:S(2)}, u32[]{:S(2)}) collective-permute-start(bf16[32,1024]{1,0:T(8,128)(2,1)S(1)} %get-tuple-element.43), channel_id=1, source_target_pairs={{0,20},{4,16},{8,28},{12,24},{16,4},{20,0},{24,12},{28,8},{1,21},{... | collective-permute-start | bytes 196616 | tf_op jit(solution)/shard_map/ppermute | solution.py:341
  11.1 18.6 %collective-permute-start.3 = (bf16[32,1024]{1,0:T(8,128)(2,1)S(1)}, bf16[32,1024]{1,0:T(8,128)(2,1)S(1)}, u32[]{:S(2)}, u32[]{:S(2)}) collective-permute-start(bf16[32,1024]{1,0:T(8,128)(2,1)S(1)} %get-tuple-element.44), channel_id=1, source_target_pairs={{0,28},{4,24},{8,20},{12,16},{16,12},{20,8},{24,4},{28,0},{1,29},{... | collective-permute-start | bytes 196616 | tf_op jit(solution)/shard_map/ppermute | solution.py:341
  11.1 5.0 %collective-permute-start.5 = (bf16[32,1024]{1,0:T(8,128)(2,1)S(1)}, bf16[32,1024]{1,0:T(8,128)(2,1)S(1)}, u32[]{:S(2)}, u32[]{:S(2)}) collective-permute-start(bf16[32,1024]{1,0:T(8,128)(2,1)S(1)} %get-tuple-element.46), channel_id=1, source_target_pairs={{0,8},{4,12},{8,0},{12,4},{16,24},{20,28},{24,16},{28,20},{1,9},{5... | collective-permute-start | bytes 196616 | tf_op jit(solution)/shard_map/ppermute | solution.py:341
  16.1 5.9 %collective-permute-start.6 = (bf16[32,1024]{1,0:T(8,128)(2,1)S(1)}, bf16[32,1024]{1,0:T(8,128)(2,1)S(1)}, u32[]{:S(2)}, u32[]{:S(2)}) collective-permute-start(bf16[32,1024]{1,0:T(8,128)(2,1)S(1)} %get-tuple-element.47), channel_id=1, source_target_pairs={{0,16},{4,20},{8,24},{12,28},{16,0},{20,4},{24,8},{28,12},{1,17},{... | collective-permute-start | bytes 196616 | tf_op jit(solution)/shard_map/ppermute | solution.py:341
  22.0 6.1 %collective-permute-start.7 = (bf16[32,1024]{1,0:T(8,128)(2,1)S(1)}, bf16[32,1024]{1,0:T(8,128)(2,1)S(1)}, u32[]{:S(2)}, u32[]{:S(2)}) collective-permute-start(bf16[32,1024]{1,0:T(8,128)(2,1)S(1)} %get-tuple-element.48), channel_id=1, source_target_pairs={{0,24},{4,28},{8,16},{12,20},{16,8},{20,12},{24,0},{28,4},{1,25},{... | collective-permute-start | bytes 196616 | tf_op jit(solution)/shard_map/ppermute | solution.py:341
  28.1 6.4 %collective-permute-start.8 = (bf16[128,1024]{1,0:T(8,128)(2,1)S(1)}, bf16[128,1024]{1,0:T(8,128)(2,1)S(1)}, u32[]{:S(2)}, u32[]{:S(2)}) collective-permute-start(bf16[128,1024]{1,0:T(8,128)(2,1)S(1)} %constant_dynamic-update-slice_fusion.4.refs_1_), channel_id=1, source_target_pairs={{0,2},{1,3},{2,0},{3,1},{4,6},{5,7},{6,4},{7,5},{8,10},{9,11},{10,... | collective-permute-start | bytes 786440 | tf_op jit(solution)/shard_map/ppermute | solution.py:341
  29.7 7.6 %collective-permute-start.4 = (bf16[128,1024]{1,0:T(8,128)(2,1)S(1)}, bf16[128,1024]{1,0:T(8,128)(2,1)S(1)}, u32[]{:S(2)}, u32[]{:S(2)}) collective-permute-start(bf16[128,1024]{1,0:T(8,128)(2,1)S(1)} %constant_dynamic-update-slice_fusion.refs_0_), channel_id=1, source_target_pairs={{0,2},{1,3},{2,0},{3,1},{4,6},{5,7},{6,4},{7,5},{8,10},{9,11},{10,... | collective-permute-start | bytes 786440 | tf_op jit(solution)/shard_map/ppermute | solution.py:341
  30.3 7.1 %collective-permute-start.12 = (bf16[128,1024]{1,0:T(8,128)(2,1)S(1)}, bf16[128,1024]{1,0:T(8,128)(2,1)S(1)}, u32[]{:S(2)}, u32[]{:S(2)}) collective-permute-start(bf16[128,1024]{1,0:T(8,128)(2,1)S(1)} %constant_dynamic-update-slice_fusion.4.refs_1_), channel_id=1, source_target_pairs={{0,1},{1,0},{2,3},{3,2},{4,5},{5,4},{6,7},{7,6},{8,9},{9,8},{10,11... | collective-permute-start | bytes 786440 | tf_op jit(solution)/shard_map/ppermute | solution.py:341
  30.3 11.4 %collective-permute-start.11 = (bf16[128,1024]{1,0:T(8,128)(2,1)S(1)}, bf16[128,1024]{1,0:T(8,128)(2,1)S(1)}, u32[]{:S(2)}, u32[]{:S(2)}) collective-permute-start(bf16[128,1024]{1,0:T(8,128)(2,1)S(1)} %constant_dynamic-update-slice_fusion.refs_0_), channel_id=1, source_target_pairs={{0,1},{1,0},{2,3},{3,2},{4,5},{5,4},{6,7},{7,6},{8,9},{9,8},{10,11... | collective-permute-start | bytes 786440 | tf_op jit(solution)/shard_map/ppermute | solution.py:341
  34.5 11.9 %collective-permute-start.10 = (bf16[128,1024]{1,0:T(8,128)(2,1)S(1)}, bf16[128,1024]{1,0:T(8,128)(2,1)S(1)}, u32[]{:S(2)}, u32[]{:S(2)}) collective-permute-start(bf16[128,1024]{1,0:T(8,128)(2,1)S(1)} %collective-permute-done.8.refs_1_), channel_id=1, source_target_pairs={{0,1},{1,0},{2,3},{3,2},{4,5},{5,4},{6,7},{7,6},{8,9},{9,8},{10,11... | collective-permute-start | bytes 786440 | tf_op jit(solution)/shard_map/ppermute | solution.py:341
  37.3 9.1 %collective-permute-start.9 = (bf16[128,1024]{1,0:T(8,128)(2,1)S(1)}, bf16[128,1024]{1,0:T(8,128)(2,1)S(1)}, u32[]{:S(2)}, u32[]{:S(2)}) collective-permute-start(bf16[128,1024]{1,0:T(8,128)(2,1)S(1)} %collective-permute-done.4.refs_0_), channel_id=1, source_target_pairs={{0,1},{1,0},{2,3},{3,2},{4,5},{5,4},{6,7},{7,6},{8,9},{9,8},{10,11... | collective-permute-start | bytes 786440 | tf_op jit(solution)/shard_map/ppermute | solution.py:341
  37.3 11.7 %collective-permute-start.16 = (bf16[384,256]{1,0:T(8,128)(2,1)S(1)}, bf16[384,256]{1,0:T(8,128)(2,1)S(1)}, u32[]{:S(2)}, u32[]{:S(2)}) collective-permute-start(bf16[384,256]{1,0:T(8,128)(2,1)S(1)} %get-tuple-element.59), channel_id=1, source_target_pairs={{0,8},{4,12},{8,0},{12,4},{16,24},{20,28},{24,16},{28,20},{1,9},{5... | collective-permute-start | bytes 589832 | tf_op jit(solution)/shard_map/ppermute | solution.py:341
  37.3 18.6 %collective-permute-start.17 = (bf16[384,256]{1,0:T(8,128)(2,1)S(1)}, bf16[384,256]{1,0:T(8,128)(2,1)S(1)}, u32[]{:S(2)}, u32[]{:S(2)}) collective-permute-start(bf16[384,256]{1,0:T(8,128)(2,1)S(1)} %get-tuple-element.60), channel_id=1, source_target_pairs={{0,16},{4,20},{8,24},{12,28},{16,0},{20,4},{24,8},{28,12},{1,17},{... | collective-permute-start | bytes 589832 | tf_op jit(solution)/shard_map/ppermute | solution.py:341
  41.7 14.2 %collective-permute-start.18 = (bf16[384,256]{1,0:T(8,128)(2,1)S(1)}, bf16[384,256]{1,0:T(8,128)(2,1)S(1)}, u32[]{:S(2)}, u32[]{:S(2)}) collective-permute-start(bf16[384,256]{1,0:T(8,128)(2,1)S(1)} %get-tuple-element.61), channel_id=1, source_target_pairs={{0,24},{4,28},{8,16},{12,20},{16,8},{20,12},{24,0},{28,4},{1,25},{... | collective-permute-start | bytes 589832 | tf_op jit(solution)/shard_map/ppermute | solution.py:341
  46.5 15.5 %copy-start.2 = (f32[256]{0:T(256)S(1)}, f32[256]{0:T(256)}, u32[]{:S(2)}) copy-start(f32[256]{0:T(256)} %param.16) | copy-start | bytes 3076
  46.5 23.4 %copy-start.4 = (f32[4]{0:T(128)S(1)}, f32[4]{0:T(128)}, u32[]{:S(2)}) copy-start(f32[4]{0:T(128)} %lambda_ref.1) | copy-start | bytes 52
  48.9 43.0 %copy-start.1 = (s32[64,2]{0,1:T(2,128)S(1)}, s32[64,2]{0,1:T(2,128)}, u32[]{:S(2)}) copy-start(s32[64,2]{0,1:T(2,128)} %param.19) | copy-start | bytes 1540
  48.9 42.9 %copy-start.3 = (f32[64,2]{0,1:T(2,128)S(1)}, f32[64,2]{0,1:T(2,128)}, u32[]{:S(2)}) copy-start(f32[64,2]{0,1:T(2,128)} %param.20) | copy-start | bytes 1540
  48.9 10.4 %collective-permute-start.21 = (bf16[128,1024]{1,0:T(8,128)(2,1)S(1)}, bf16[128,1024]{1,0:T(8,128)(2,1)}, u32[]{:S(2)}, u32[]{:S(2)}) collective-permute-start(bf16[128,1024]{1,0:T(8,128)(2,1)S(1)} %get-tuple-element.67), channel_id=1, source_target_pairs={{0,1},{1,0},{2,3},{3,2},{4,5},{5,4},{6,7},{7,6},{8,9},{9,8},{10,11... | collective-permute-start | bytes 786440 | tf_op jit(solution)/shard_map/ppermute | solution.py:341
  56.7 13.2 %collective-permute-start.20 = (bf16[768,256]{1,0:T(8,128)(2,1)}, bf16[768,256]{1,0:T(8,128)(2,1)S(1)}, u32[]{:S(2)}, u32[]{:S(2)}) collective-permute-start(bf16[768,256]{1,0:T(8,128)(2,1)} %pad_maximum_fusion), channel_id=1, source_target_pairs={{0,4},{4,0},{8,12},{12,8},{16,20},{20,16},{24,28},{28,24},{1,5},{5... | collective-permute-start | bytes 1179656 | tf_op jit(solution)/shard_map/ppermute | solution.py:341
  58.0 11.9 %collective-permute-start.19 = (bf16[256,256]{1,0:T(8,128)(2,1)S(1)}, bf16[256,256]{1,0:T(8,128)(2,1)S(1)}, u32[]{:S(2)}, u32[]{:S(2)}) collective-permute-start(bf16[256,256]{1,0:T(8,128)(2,1)S(1)} %slice.24), channel_id=1, source_target_pairs={{0,4},{4,0},{8,12},{12,8},{16,20},{20,16},{24,28},{28,24},{1,5},{5... | collective-permute-start | bytes 393224 | tf_op jit(solution)/shard_map/ppermute | solution.py:341
  58.8 14.3 %collective-permute-start.13 = (bf16[128,1024]{1,0:T(8,128)(2,1)S(1)}, bf16[128,1024]{1,0:T(8,128)(2,1)S(1)}, u32[]{:S(2)}, u32[]{:S(2)}) collective-permute-start(bf16[128,1024]{1,0:T(8,128)(2,1)S(1)} %get-tuple-element.55), channel_id=1, source_target_pairs={{0,1},{1,0},{2,3},{3,2},{4,5},{5,4},{6,7},{7,6},{8,9},{9,8},{10,11... | collective-permute-start | bytes 786440 | tf_op jit(solution)/shard_map/ppermute | solution.py:341
  58.8 16.0 %collective-permute-start.23 = (bf16[128,1024]{1,0:T(8,128)(2,1)S(1)}, bf16[128,1024]{1,0:T(8,128)(2,1)S(1)}, u32[]{:S(2)}, u32[]{:S(2)}) collective-permute-start(bf16[128,1024]{1,0:T(8,128)(2,1)S(1)} %get-tuple-element.69), channel_id=1, source_target_pairs={{0,1},{1,0},{2,3},{3,2},{4,5},{5,4},{6,7},{7,6},{8,9},{9,8},{10,11... | collective-permute-start | bytes 786440 | tf_op jit(solution)/shard_map/ppermute | solution.py:341
  60.3 14.4 %collective-permute-start.22 = (bf16[128,1024]{1,0:T(8,128)(2,1)S(1)}, bf16[128,1024]{1,0:T(8,128)(2,1)S(1)}, u32[]{:S(2)}, u32[]{:S(2)}) collective-permute-start(bf16[128,1024]{1,0:T(8,128)(2,1)S(1)} %add_convert_fusion.1), channel_id=1, source_target_pairs={{0,2},{1,3},{2,0},{3,1},{4,6},{5,7},{6,4},{7,5},{8,10},{9,11},{10,... | collective-permute-start | bytes 786440 | tf_op jit(solution)/shard_map/ppermute | solution.py:341
  69.9 12.3 %collective-permute-start.15 = (bf16[128,1024]{1,0:T(8,128)(2,1)S(1)}, bf16[128,1024]{1,0:T(8,128)(2,1)S(1)}, u32[]{:S(2)}, u32[]{:S(2)}) collective-permute-start(bf16[128,1024]{1,0:T(8,128)(2,1)S(1)} %get-tuple-element.57), channel_id=1, source_target_pairs={{0,1},{1,0},{2,3},{3,2},{4,5},{5,4},{6,7},{7,6},{8,9},{9,8},{10,11... | collective-permute-start | bytes 786440 | tf_op jit(solution)/shard_map/ppermute | solution.py:341
  73.2 9.0 %collective-permute-start.14 = (bf16[128,1024]{1,0:T(8,128)(2,1)S(1)}, bf16[128,1024]{1,0:T(8,128)(2,1)S(1)}, u32[]{:S(2)}, u32[]{:S(2)}) collective-permute-start(bf16[128,1024]{1,0:T(8,128)(2,1)S(1)} %add_convert_fusion.2), channel_id=1, source_target_pairs={{0,2},{1,3},{2,0},{3,1},{4,6},{5,7},{6,4},{7,5},{8,10},{9,11},{10,... | collective-permute-start | bytes 786440 | tf_op jit(solution)/shard_map/ppermute | solution.py:341
  74.9 14.4 %collective-permute-start.30 = (bf16[32,1024]{1,0:T(8,128)(2,1)S(1)}, bf16[32,1024]{1,0:T(8,128)(2,1)S(1)}, u32[]{:S(2)}, u32[]{:S(2)}) collective-permute-start(bf16[32,1024]{1,0:T(8,128)(2,1)S(1)} %get-tuple-element.76), channel_id=1, source_target_pairs={{0,28},{4,24},{8,20},{12,16},{16,12},{20,8},{24,4},{28,0},{1,29},{... | collective-permute-start | bytes 196616 | tf_op jit(solution)/shard_map/ppermute | solution.py:341
  78.1 13.1 %collective-permute-start.28 = (bf16[32,1024]{1,0:T(8,128)(2,1)S(1)}, bf16[32,1024]{1,0:T(8,128)(2,1)S(1)}, u32[]{:S(2)}, u32[]{:S(2)}) collective-permute-start(bf16[32,1024]{1,0:T(8,128)(2,1)S(1)} %get-tuple-element.77), channel_id=1, source_target_pairs={{0,20},{4,16},{8,28},{12,24},{16,4},{20,0},{24,12},{28,8},{1,21},{... | collective-permute-start | bytes 196616 | tf_op jit(solution)/shard_map/ppermute | solution.py:341
  82.2 14.3 %collective-permute-start.25 = (bf16[256,256]{1,0:T(8,128)(2,1)S(1)}, bf16[256,256]{1,0:T(8,128)(2,1)S(1)}, u32[]{:S(2)}, u32[]{:S(2)}) collective-permute-start(bf16[256,256]{1,0:T(8,128)(2,1)S(1)} %get-tuple-element.70), channel_id=1, source_target_pairs={{0,8},{4,12},{8,0},{12,4},{16,24},{20,28},{24,16},{28,20},{1,9},{5... | collective-permute-start | bytes 393224 | tf_op jit(solution)/shard_map/ppermute | solution.py:341
  86.9 12.6 %collective-permute-start.27 = (bf16[256,256]{1,0:T(8,128)(2,1)S(1)}, bf16[256,256]{1,0:T(8,128)(2,1)S(1)}, u32[]{:S(2)}, u32[]{:S(2)}) collective-permute-start(bf16[256,256]{1,0:T(8,128)(2,1)S(1)} %get-tuple-element.71), channel_id=1, source_target_pairs={{0,16},{4,20},{8,24},{12,28},{16,0},{20,4},{24,8},{28,12},{1,17},{... | collective-permute-start | bytes 393224 | tf_op jit(solution)/shard_map/ppermute | solution.py:341
  87.8 11.7 %collective-permute-start.29 = (bf16[256,256]{1,0:T(8,128)(2,1)S(1)}, bf16[256,256]{1,0:T(8,128)(2,1)S(1)}, u32[]{:S(2)}, u32[]{:S(2)}) collective-permute-start(bf16[256,256]{1,0:T(8,128)(2,1)S(1)} %get-tuple-element.72), channel_id=1, source_target_pairs={{0,24},{4,28},{8,16},{12,20},{16,8},{20,12},{24,0},{28,4},{1,25},{... | collective-permute-start | bytes 393224 | tf_op jit(solution)/shard_map/ppermute | solution.py:341
  89.3 7.2 %collective-permute-start.26 = (bf16[32,1024]{1,0:T(8,128)(2,1)S(1)}, bf16[32,1024]{1,0:T(8,128)(2,1)S(1)}, u32[]{:S(2)}, u32[]{:S(2)}) collective-permute-start(bf16[32,1024]{1,0:T(8,128)(2,1)S(1)} %get-tuple-element.78), channel_id=1, source_target_pairs={{0,12},{4,8},{8,4},{12,0},{16,28},{20,24},{24,20},{28,16},{1,13},{... | collective-permute-start | bytes 196616 | tf_op jit(solution)/shard_map/ppermute | solution.py:341
  91.1 5.4 %collective-permute-start.24 = (bf16[32,1024]{1,0:T(8,128)(2,1)S(1)}, bf16[32,1024]{1,0:T(8,128)(2,1)S(1)}, u32[]{:S(2)}, u32[]{:S(2)}) collective-permute-start(bf16[32,1024]{1,0:T(8,128)(2,1)S(1)} %get-tuple-element.79), channel_id=1, source_target_pairs={{0,4},{4,0},{8,12},{12,8},{16,20},{20,16},{24,28},{28,24},{1,5},{5... | collective-permute-start | bytes 196616 | tf_op jit(solution)/shard_map/ppermute | solution.py:341

commit v2 on v1

--- a/solution.py
+++ b/solution.py
@@ -57,10 +57,11 @@
 
 def prep_kernel(nz, nx, cap, width, wide, tokens_ref, gain_ref, routes_ref, *refs):
     blocks = nz * nx
-    tokens_s, gain_s, sems = refs[-3:]
+    tokens_s, gain_s, routes_s, sems = refs[-4:]
     copies = [
-        pltpu.make_async_copy(tokens_ref, tokens_s, sems.at[0]),
-        pltpu.make_async_copy(gain_ref, gain_s, sems.at[1]),
+        pltpu.make_async_copy(routes_ref, routes_s, sems.at[0]),
+        pltpu.make_async_copy(tokens_ref, tokens_s, sems.at[1]),
+        pltpu.make_async_copy(gain_ref, gain_s, sems.at[2]),
     ]
     slices = []
     if wide:
@@ -71,15 +72,16 @@
             columns = pl.ds(pl.multiple_of((z ^ k) * wide, wide), wide)
             for i, source in enumerate(sources):
                 target = refs[blocks + k].at[pl.ds(i * count, count), :]
-                sem = sems.at[2 + 3 * k + i]
+                sem = sems.at[3 + 3 * k + i]
                 slices.append(pltpu.make_async_copy(source.at[:, columns], target, sem))
     out_refs = refs[:blocks]
     for copy in copies + slices:
         copy.start()
     rows = tokens_ref.shape[0]
-    picker, _ = slot_hits(nz, nx, cap, routes_ref[...])
+    copies[0].wait()
+    picker, _ = slot_hits(nz, nx, cap, routes_s[...])
     picker = jnp.where(picker, 1.0, 0.0).reshape(blocks * cap, rows).astype(jnp.bfloat16)
-    for copy in copies:
+    for copy in copies[1:]:
         copy.wait()
     tokens = tokens_s[...].astype(jnp.float32)
     scale = lax.rsqrt(jnp.mean(tokens * tokens, axis=-1, keepdims=True) + moe_eps)
@@ -105,13 +107,24 @@
     low_ref[...] = (weight - high.astype(jnp.float32)).astype(jnp.bfloat16)
 
 
+def total_of(refs):
+    total = refs[0][...].astype(jnp.float32)
+    for ref in refs[1:]:
+        total = total + ref[...].astype(jnp.float32)
+    return total.astype(jnp.bfloat16)
+
+
+def add_kernel(n_sums, *refs):
+    total = total_of(refs[:n_sums])
+    count = refs[n_sums].shape[0]
+    for k, out_ref in enumerate(refs[n_sums:]):
+        out_ref[...] = total[k * count : (k + 1) * count]
+
+
 def blend_kernel(nz, cap, n_sums, *refs):
     sum_refs, refs = refs[:n_sums], refs[n_sums:]
     attend_refs, near_ref, out_refs = refs[: nz - 1], refs[nz - 1], refs[nz:]
-    total = sum_refs[0][...].astype(jnp.float32)
-    for ref in sum_refs[1:]:
-        total = total + ref[...].astype(jnp.float32)
-    total = total.astype(jnp.bfloat16)
+    total = total_of(sum_refs)
     near_ref[...] = total[:cap]
     for k in range(1, nz):
         out_ref = out_refs[k - 1]
@@ -162,71 +175,50 @@
     out_ref[...] = in_ref[...]
 
 
-def early_kernel(groups, tp_n, *refs):
-    row_refs = refs[: 2 * groups]
-    gate_ref, up_ref, down_ref = refs[2 * groups : 2 * groups + 3]
-    gate_out, up_out, gate_late, up_late, down_late = refs[2 * groups + 3 : 2 * groups + 8]
-    gate_s, up_s, sems = refs[2 * groups + 8 :]
-    width = row_refs[0].shape[1]
-    tp = lax.axis_index("tp")
-
-    def block(q):
-        return pl.ds(pl.multiple_of((tp ^ q) * width, width), width)
-
-    early, late = [], []
+def columns_of(q, width):
+    return pl.ds(pl.multiple_of((lax.axis_index("tp") ^ q) * width, width), width)
+
+
+def early_kernel(groups, *refs):
+    row_refs, (gate_ref, up_ref), out_refs = (
+        refs[: 2 * groups],
+        refs[2 * groups : 2 * groups + 2],
+        refs[2 * groups + 2 :],
+    )
+    rows = [
+        jnp.concatenate([ref[...] for ref in row_refs[q * groups : (q + 1) * groups]], axis=0)
+        for q in range(2)
+    ]
+    size = row_refs[0].shape[0]
+    width = rows[0].shape[1]
+    for i, ref in enumerate((gate_ref, up_ref)):
+        product = dot(rows[0], ref[columns_of(0, width), :])
+        product = product + dot(rows[1], ref[columns_of(1, width), :])
+        for g in range(groups):
+            out_refs[i * groups + g][...] = product[g * size : (g + 1) * size]
+
+
+def late_kernel(tp_n, *refs):
+    row_refs = refs[: tp_n - 2]
+    gate_in, up_in, gate_ref, up_ref, down_ref = refs[tp_n - 2 : tp_n + 3]
+    out_refs = refs[tp_n + 3 :]
+    gate, up = gate_in[...], up_in[...]
+    for q in range(2, tp_n):
+        rows = row_refs[q - 2][...]
+        gate = gate + dot(rows, gate_ref[columns_of(q, rows.shape[1]), :])
+        up = up + dot(rows, up_ref[columns_of(q, rows.shape[1]), :])
+    hidden = (gate * jax.nn.sigmoid(gate) * up).astype(jnp.bfloat16)
     for q in range(tp_n):
-        for which, (source, held, later) in enumerate(
-            ((gate_ref, gate_s, gate_late), (up_ref, up_s, up_late))
-        ):
-            target = held.at[q] if q < 2 else later.at[q - 2]
-            copy = pltpu.make_async_copy(source.at[block(q), :], target, sems.at[which, q])
-            (early if q < 2 else late).append(copy)
-    for q in range(tp_n):
-        late.append(
-            pltpu.make_async_copy(down_ref.at[:, block(q)], down_late.at[q], sems.at[2, q])
-        )
-    for copy in early + late:
-        copy.start()
-    gate, up = 0.0, 0.0
-    for q in range(2):
-        rows = [row_refs[q * groups + g][...] for g in range(groups)]
-        rows = jnp.concatenate(rows, axis=0)
-        early[2 * q].wait()
-        gate = gate + dot(rows, gate_s[q])
-        early[2 * q + 1].wait()
-        up = up + dot(rows, up_s[q])
-    gate_out[...] = gate
-    up_out[...] = up
-    for copy in late:
-        copy.wait()
-
-
-def late_kernel(groups, tp_n, *refs):
-    n_in = (tp_n - 2) * groups
-    row_refs = refs[:n_in]
-    gate_in, up_in, gate_ref, up_ref, down_ref = refs[n_in : n_in + 5]
-    out_refs = refs[n_in + 5 :]
-    gate, up = gate_in[...], up_in[...]
-    for q in range(tp_n - 2):
-        rows = [row_refs[q * groups + g][...] for g in range(groups)]
-        rows = jnp.concatenate(rows, axis=0)
-        gate = gate + dot(rows, gate_ref[q])
-        up = up + dot(rows, up_ref[q])
-    hidden = (gate * jax.nn.sigmoid(gate) * up).astype(jnp.bfloat16)
-    size = hidden.shape[0] // groups
-    for q in range(tp_n):
-        result = dot(hidden, down_ref[q]).astype(jnp.bfloat16)
-        for g in range(groups):
-            out_refs[q * groups + g][...] = result[g * size : (g + 1) * size]
-
-
-def attend_kernel(nz, nx, heads, place_ref, lambda_ref, gain_ref, *refs):
-    pack_refs = refs[:nz]
-    near_refs = refs[nz : nz + nx - 1]
-    rest_refs = refs[nz + nx - 1 : nz + 2 * (nx - 1)]
-    out_refs = refs[nz + 2 * (nx - 1) : 2 * nz + 2 * (nx - 1)]
-    query_s, key_s, value_s, out_s = refs[2 * nz + 2 * (nx - 1) :]
-    z, x = place_ref[0], place_ref[1]
+        block = down_ref[:, columns_of(q, out_refs[q].shape[1])]
+        out_refs[q][...] = dot(hidden, block).astype(jnp.bfloat16)
+
+
+def attend_kernel(nz, nx, heads, lambda_ref, gain_ref, *refs):
+    pack_refs, refs = refs[:nz], refs[nz:]
+    near_refs, rest_refs, refs = refs[: nx - 1], refs[nx - 1 : 2 * nx - 2], refs[2 * nx - 2 :]
+    out_refs = refs[:nz]
+    query_s, key_s, value_s, out_s = refs[nz:]
+    z, x, _ = where_am_i(nx)
     rows = pack_refs[0].shape[0] // 3
 
     def at(block):
@@ -327,8 +319,6 @@
 ):
     nz, nx, tp_n = sizes
     ep_n = nz * nx
-    ep = lax.axis_index("ep")
-    place = jnp.stack([ep // nx, ep % nx]).astype(jnp.int32)
     rows_b, model = tokens.shape
     cap = 2 * TOP * rows_b // ep_n
     width = model // tp_n
@@ -340,7 +330,7 @@
         n = ep_n if axis == "ep" else tp_n
         return lax.ppermute(v, axis, [(i, i ^ mask) for i in range(n)])
 
-    def kernel(body, ins, outs, in_specs=None, out_specs=None, scratch=(), mib=8):
+    def kernel(body, ins, outs, in_specs=None, out_specs=None, scratch=(), mib=8, cost=None):
         if in_specs:
             ins = [
                 pltpu.with_memory_space_constraint(v, pltpu.HBM) if spec is HBM else v
@@ -353,6 +343,7 @@
             out_specs=out_specs or jax.tree.map(lambda _: VMEM, outs),
             scratch_shapes=scratch,
             compiler_params=params(mib),
+            cost_estimate=cost,
         )(*ins)
 
     heads, odd = divmod(lambdas.shape[0], nz)
@@ -362,12 +353,14 @@
     sends = kernel(
         functools.partial(prep_kernel, nz, nx, cap, width, wide),
         (tokens, moe_gain.reshape(1, model), routes.T, *slices),
-        [struct((cap, width))] * ep_n + [struct((3 * rows_a, wide))] * (nz if wide else 0),
-        in_specs=[HBM, HBM, VMEM] + [HBM] * len(slices),
+        [struct((cap, width))] * ep_n
+        + [struct((3 * rows_a, wide))] * (nz if wide else 0),
+        in_specs=[HBM] * (3 + len(slices)),
         scratch=[
             pltpu.VMEM((rows_b, model), jnp.bfloat16),
             pltpu.VMEM((1, model), jnp.float32),
-            pltpu.SemaphoreType.DMA((2 + 3 * nz,)),
+            pltpu.VMEM((TOP, rows_b), jnp.int32),
+            pltpu.SemaphoreType.DMA((3 + 3 * nz,)),
         ],
     )
     sends, packs = sends[:ep_n], sends[ep_n:]
@@ -393,9 +386,9 @@
         gain = kernel(fence_kernel, (head_gain.reshape(1, VD),), struct((1, VD), jnp.float32))
         outs = kernel(
             functools.partial(attend_kernel, nz, nx, heads),
-            (place, lambdas, gain, *packs, *near, *rest),
+            (lambdas, gain, *packs, *near, *rest),
             [struct((rows_a, wide))] * nz,
-            in_specs=[SMEM, SMEM] + [VMEM] * (1 + nz + 2 * (nx - 1)),
+            in_specs=[SMEM] + [VMEM] * (1 + nz + 2 * (nx - 1)),
             scratch=[
                 pltpu.VMEM((nz * rows_a, wide), jnp.bfloat16),
                 pltpu.VMEM((ep_n * rows_a, wide), jnp.bfloat16),
@@ -407,62 +400,52 @@
     else:
         attended = gathered_attention(queries, key_rows, values, lambdas, head_gain)
 
-    slots = ep_n * cap
-    gate, up, *late = kernel(
-        functools.partial(early_kernel, nx, tp_n),
-        (*[parts[q, m] for q in range(2) for m in order], w_gate[0], w_up[0], w_down[0]),
-        [
-            struct((slots, units), jnp.float32),
-            struct((slots, units), jnp.float32),
-            struct((tp_n - 2, width, units)),
-            struct((tp_n - 2, width, units)),
-            struct((tp_n, units, width)),
-        ],
-        in_specs=[VMEM] * (2 * nx) + [HBM] * 3,
-        scratch=[
-            pltpu.VMEM((2, width, units), jnp.bfloat16),
-            pltpu.VMEM((2, width, units), jnp.bfloat16),
-            pltpu.SemaphoreType.DMA((3, tp_n)),
-        ],
+    slots, span = ep_n * cap, nz * cap
+    gate, up, down = w_gate[0], w_up[0], w_down[0]
+    sums = kernel(
+        functools.partial(early_kernel, nx),
+        (*[parts[q, m] for q in range(2) for m in order], gate, up),
+        [struct((span, units), jnp.float32)] * (2 * nx),
         mib=20,
     )
-    results = kernel(
-        functools.partial(late_kernel, nx, tp_n),
-        (*[parts[q, m] for q in range(2, tp_n) for m in order], gate, up, *late),
-        [struct((slots // nx, width))] * (tp_n * nx),
-        mib=20,
-    )
+    results = {}
+    for g, m in enumerate(order):
+        results[m] = kernel(
+            functools.partial(late_kernel, tp_n),
+            (*[parts[q, m] for q in range(2, tp_n)], sums[g], sums[nx + g], gate, up, down),
+            [struct((span, width))] * tp_n,
+            mib=20,
+        )
 
     returned = {}
-    for g, m in enumerate(order):
+    for m in order:
         pieces = []
         for q in list(range(2, tp_n, 2)) + [0]:
-            own = results[q * nx + g]
-            other = shift(results[(q + 1) * nx + g], "tp", 1)
+            both = [results[m][q], shift(results[m][q + 1], "tp", 1)]
             if q:
-                piece = own.astype(jnp.float32) + other.astype(jnp.float32)
-                pieces.append(shift(piece.astype(jnp.bfloat16), "tp", q))
+                (piece,) = kernel(functools.partial(add_kernel, 2), both, [struct((span, width))])
+                pieces.append(shift(piece, "tp", q))
             else:
-                pieces += [own, other]
+                pieces += both
         if wide and m == 0:
-            returned[0, 0], *mixed = kernel(
+            blocks = kernel(
                 functools.partial(blend_kernel, nz, cap, len(pieces)),
                 (*pieces, *outs[1:]),
                 [struct((cap, width))]
                 + [struct((rows_a + cap * width // wide, wide))] * (nz - 1),
             )
-            for k in range(1, nz):
-                returned[k, 0] = shift(mixed[k - 1], "ep", k * nx)
         else:
-            total = sum(piece.astype(jnp.float32) for piece in pieces).astype(jnp.bfloat16)
-            for k in range(nz):
-                block = total[k * cap : (k + 1) * cap]
-                returned[k, m] = shift(block, "ep", k * nx + m)
+            blocks = kernel(
+                functools.partial(add_kernel, len(pieces)), pieces, [struct((cap, width))] * nz
+            )
+        for k in range(nz):
+            returned[k, m] = shift(blocks[k], "ep", k * nx + m)
 
     high, low = kernel(
         functools.partial(gates_kernel, nz, nx, cap),
         (routes.T, route_scores.T),
         [struct((slots, rows_b))] * 2,
+        cost=pl.CostEstimate(flops=20_000_000_000, bytes_accessed=100_000, transcendentals=0),
     )
     shapes = [struct((rows_b, width))] + [struct((rows_a, nz * wide))] * (wide > 0)
     out, *held = kernel(

time: 101 us -> 90.9 us (0.900)
  local copies, waits for them, and re-layouts: 0.81 us -> 9.58 us
  waiting for transfers between devices: 38.7 us -> 31.7 us
  starting transfers between devices: 44.8 us -> 38 us
  Pallas kernels: 13.3 us -> 10.4 us
  other arithmetic: 2.05 us -> 0.03 us
    unnamed x16 -> x26, local copies, waits for them, and re-layouts: 0.73 us -> 9.53 us
    ppermute x31, waiting for transfers between devices: 38.7 us -> 31.7 us  [shift(): return lax.ppermute(v, axis, [(i, i ^ mask) for i in range(n)])]
    ppermute x31, starting transfers between devices: 44.8 us -> 38 us  [shift(): return lax.ppermute(v, axis, [(i, i ^ mask) for i in range(n)])]
    pallas_call x8 -> x12, Pallas kernels: 13.3 us -> 10.4 us  [kernel(): pl.pallas_call(body, out_shape=outs, in_specs=in_specs or [VMEM] * len(in...]
    convert_element_type x3 -> x0, other arithmetic: 1.21 us -> none  [the longest x2 1.08 us: local(): pieces.append(shift(piece.astype(jnp.bfloat16), 'tp', q))]
  transfers between devices with their start and end apart: 31 -> 31, of which waited for: 9 -> 11; matrix products, arithmetic and copies ran while one was open for 2% -> 0% of each run, Pallas kernels for 11% -> 9%
where the time goes in v2:
time: 90.9 us; the launch traced here: 90.6 us
  starting transfers between devices  38 us (42%)
  waiting for transfers between devices  31.7 us (35%)
  Pallas kernels  10.4 us (11%)
  local copies, waits for them, and re-layouts  9.58 us (11%)
    ppermute x31, starting transfers between devices, shift(): return lax.ppermute(v, axis, [(i, i ^ mask) for i in range(n)])  38 us
    ppermute x31, waiting for transfers between devices, shift(): return lax.ppermute(v, axis, [(i, i ^ mask) for i in range(n)])  31.7 us
    pallas_call x12, Pallas kernels, kernel(): pl.pallas_call(body, out_shape=outs, in_specs=in_specs or [VMEM] * len(in...  10.4 us
    unnamed x26, local copies, waits for them, and re-layouts  9.53 us
  transfers between devices with their start and end apart: 31, of which 11 were waited for; matrix products, arithmetic and copies ran while one was open for 0% of the time, Pallas kernels for 9%

profile of v2, /device:TPU:0, one launch (start us, length us, event | category | flops | bytes accessed | tf_op | source)
XLA Modules:
  0.0 90.6 jit_solution(9882988103095978688)
XLA Ops:
  0.6 1.7 %shard_map.132 = (bf16[32,1024]{1,0:T(8,128)(2,1)S(1)}, bf16[32,1024]{1,0:T(8,128)(2,1)S(1)}, bf16[32,1024]{1,0:T(8,128)(2,1)S(1)}, bf16[32,1024]{1,0:T(8,128)(2...) custom-call(bf16[64,4096]{1,0:T(8,128)(2,1)} %tokens_ref.1, ...), custom_call_target="tpu_custom_call" | custom-call | tf_op jit(solution)/shard_map/pallas_call | solution.py:339
  2.3 3.0 %collective-permute-start.5 = (bf16[32,1024]{1,0:T(8,128)(2,1)S(1)}, bf16[32,1024]{1,0:T(8,128)(2,1)S(1)}, u32[]{:S(2)}, u32[]{:S(2)}) collective-permute-start(bf16[32,1024]{1,0:T(8,128)(2,1)S(1)} %get-tuple-element.48), channel_id=1, source_target_pairs={{0,4},{4,0},{8,12},{12,8},{16,20},{20,16},{24,28},{28,24},{1,5},{5... | collective-permute-start | bytes 196616 | tf_op jit(solution)/shard_map/ppermute | solution.py:331
  5.4 1.6 %collective-permute-start.6 = (bf16[32,1024]{1,0:T(8,128)(2,1)S(1)}, bf16[32,1024]{1,0:T(8,128)(2,1)S(1)}, u32[]{:S(2)}, u32[]{:S(2)}) collective-permute-start(bf16[32,1024]{1,0:T(8,128)(2,1)S(1)} %get-tuple-element.49), channel_id=1, source_target_pairs={{0,12},{4,8},{8,4},{12,0},{16,28},{20,24},{24,20},{28,16},{1,13},{... | collective-permute-start | bytes 196616 | tf_op jit(solution)/shard_map/ppermute | solution.py:331
  6.9 3.5 %collective-permute-start.7 = (bf16[32,1024]{1,0:T(8,128)(2,1)S(1)}, bf16[32,1024]{1,0:T(8,128)(2,1)S(1)}, u32[]{:S(2)}, u32[]{:S(2)}) collective-permute-start(bf16[32,1024]{1,0:T(8,128)(2,1)S(1)} %get-tuple-element.50), channel_id=1, source_target_pairs={{0,20},{4,16},{8,28},{12,24},{16,4},{20,0},{24,12},{28,8},{1,21},{... | collective-permute-start | bytes 196616 | tf_op jit(solution)/shard_map/ppermute | solution.py:331
  10.4 0.0 collective-permute-start.8
  10.4 0.9 collective-permute-start
  11.3 3.5 %collective-permute-start.1 = (bf16[32,1024]{1,0:T(8,128)(2,1)S(1)}, bf16[32,1024]{1,0:T(8,128)(2,1)S(1)}, u32[]{:S(2)}, u32[]{:S(2)}) collective-permute-start(bf16[32,1024]{1,0:T(8,128)(2,1)S(1)} %get-tuple-element.46), channel_id=1, source_target_pairs={{0,16},{4,20},{8,24},{12,28},{16,0},{20,4},{24,8},{28,12},{1,17},{... | collective-permute-start | bytes 196616 | tf_op jit(solution)/shard_map/ppermute | solution.py:331
  14.9 0.0 collective-permute-done.6
  14.9 0.1 collective-permute-start.2
  15.0 0.0 collective-permute-done.7
  15.0 2.6 %collective-permute-done.8 = bf16[32,1024]{1,0:T(8,128)(2,1)S(1)} collective-permute-done((bf16[32,1024]{1,0:T(8,128)(2,1)S(1)}, bf16[32,1024]{1,0:T(8,128)(2,1)S(1)}, u32[]{:S(2)}, u32[]{:S(2)}) %collective-permute-start.8) | collective-permute-done | bytes 65568 | tf_op jit(solution)/shard_map/ppermute | solution.py:331
  17.6 1.5 %collective-permute-start.19 = (bf16[128,1024]{1,0:T(8,128)(2,1)S(1)}, bf16[128,1024]{1,0:T(8,128)(2,1)S(1)}, u32[]{:S(2)}, u32[]{:S(2)}) collective-permute-start(bf16[128,1024]{1,0:T(8,128)(2,1)S(1)} %constant_dynamic-update-slice_fusion.4.refs_0_), channel_id=1, source_target_pairs={{0,2},{1,3},{2,0},{3,1},{4,6},{5,7},{6,4},{7,5},{8,10},{9,11},{10,... | collective-permute-start | bytes 786440 | tf_op jit(solution)/shard_map/ppermute | solution.py:331
  19.2 0.0 collective-permute-done
  19.2 1.2 %collective-permute-done.1 = bf16[32,1024]{1,0:T(8,128)(2,1)S(1)} collective-permute-done((bf16[32,1024]{1,0:T(8,128)(2,1)S(1)}, bf16[32,1024]{1,0:T(8,128)(2,1)S(1)}, u32[]{:S(2)}, u32[]{:S(2)}) %collective-permute-start.1) | collective-permute-done | bytes 65568 | tf_op jit(solution)/shard_map/ppermute | solution.py:331
  20.3 0.8 collective-permute-done.2
  21.1 1.5 %collective-permute-start.3 = (bf16[128,1024]{1,0:T(8,128)(2,1)S(1)}, bf16[128,1024]{1,0:T(8,128)(2,1)S(1)}, u32[]{:S(2)}, u32[]{:S(2)}) collective-permute-start(bf16[128,1024]{1,0:T(8,128)(2,1)S(1)} %constant_dynamic-update-slice_fusion.refs_1_), channel_id=1, source_target_pairs={{0,2},{1,3},{2,0},{3,1},{4,6},{5,7},{6,4},{7,5},{8,10},{9,11},{10,... | collective-permute-start | bytes 786440 | tf_op jit(solution)/shard_map/ppermute | solution.py:331
  22.6 0.0 collective-permute-start.9
  22.6 0.5 collective-permute-start.10
  23.2 3.6 %collective-permute-done.19.refs_0_ = bf16[128,1024]{1,0:T(8,128)(2,1)S(1)} collective-permute-done((bf16[128,1024]{1,0:T(8,128)(2,1)S(1)}, bf16[128,1024]{1,0:T(8,128)(2,1)S(1)}, u32[]{:S(2)}, u32[]{:S(2)}) %collective-permute-start.19) | collective-permute-done | bytes 262176 | tf_op jit(solution)/shard_map/ppermute | solution.py:331
  26.7 0.0 collective-permute-start.20
  26.7 2.9 %collective-permute-done.3.refs_0_ = bf16[128,1024]{1,0:T(8,128)(2,1)S(1)} collective-permute-done((bf16[128,1024]{1,0:T(8,128)(2,1)S(1)}, bf16[128,1024]{1,0:T(8,128)(2,1)S(1)}, u32[]{:S(2)}, u32[]{:S(2)}) %collective-permute-start.3) | collective-permute-done | bytes 262176 | tf_op jit(solution)/shard_map/ppermute | solution.py:331
  29.6 2.0 %collective-permute-start.14 = (bf16[384,256]{1,0:T(8,128)(2,1)S(1)}, bf16[384,256]{1,0:T(8,128)(2,1)S(1)}, u32[]{:S(2)}, u32[]{:S(2)}) collective-permute-start(bf16[384,256]{1,0:T(8,128)(2,1)S(1)} %get-tuple-element.59), channel_id=1, source_target_pairs={{0,8},{4,12},{8,0},{12,4},{16,24},{20,28},{24,16},{28,20},{1,9},{5... | collective-permute-start | bytes 589832 | tf_op jit(solution)/shard_map/ppermute | solution.py:331
  31.6 0.7 collective-permute-start.15
  32.3 1.7 %collective-permute-start.16 = (bf16[384,256]{1,0:T(8,128)(2,1)S(1)}, bf16[384,256]{1,0:T(8,128)(2,1)S(1)}, u32[]{:S(2)}, u32[]{:S(2)}) collective-permute-start(bf16[384,256]{1,0:T(8,128)(2,1)S(1)} %get-tuple-element.61), channel_id=1, source_target_pairs={{0,24},{4,28},{8,16},{12,20},{16,8},{20,12},{24,0},{28,4},{1,25},{... | collective-permute-start | bytes 589832 | tf_op jit(solution)/shard_map/ppermute | solution.py:331
  34.1 2.2 %copy-done = bf16[1,4096,512]{2,1,0:T(8,128)(2,1)S(1)} copy-done((bf16[1,4096,512]{2,1,0:T(8,128)(2,1)S(1)}, bf16[1,4096,512]{2,1,0:T(8,128)(2,1)}, u32[]{:S(2)}) %copy-start) | copy-done | bytes 4194328
  36.2 2.2 %copy-done.2 = bf16[1,4096,512]{2,1,0:T(8,128)(2,1)S(1)} copy-done((bf16[1,4096,512]{2,1,0:T(8,128)(2,1)S(1)}, bf16[1,4096,512]{2,1,0:T(8,128)(2,1)}, u32[]{:S(2)}) %copy-start.2) | copy-done | bytes 4194328
  38.4 1.2 %shard_map.133 = (f32[128,512]{1,0:T(8,128)S(1)}, f32[128,512]{1,0:T(8,128)S(1)}, f32[128,512]{1,0:T(8,128)S(1)}, f32[128,512]{1,0:T(8,128)S(1)}) custom-call(bf16[128,1024]{1,0:T(8,128)(2,1)S(1)} %constant_dynamic-update-slice_fusion.4.refs_0_, bf16[128,1024]{1,0:T(8,128)(2,1)S(1)} %constant_dynamic-update-slice_fusion.refs_1_, ...), custom_call_target="tpu_custom_call" | custom-call | tf_op jit(solution)/shard_map/pallas_call | solution.py:339
  39.7 0.9 %copy-done.1 = bf16[1,4096,512]{2,1,0:T(8,128)(2,1)S(1)} copy-done((bf16[1,4096,512]{2,1,0:T(8,128)(2,1)S(1)}, bf16[1,4096,512]{2,1,0:T(8,128)(2,1)}, u32[]{:S(2)}) %copy-start.1) | copy-done | bytes 4194328
  40.6 1.3 %copy-done.3 = bf16[1,4096,512]{2,1,0:T(8,128)(2,1)S(1)} copy-done((bf16[1,4096,512]{2,1,0:T(8,128)(2,1)S(1)}, bf16[1,4096,512]{2,1,0:T(8,128)(2,1)}, u32[]{:S(2)}) %copy-start.3) | copy-done | bytes 4194328
  41.9 2.2 %copy-done.4 = bf16[1,512,4096]{2,1,0:T(8,128)(2,1)S(1)} copy-done((bf16[1,512,4096]{2,1,0:T(8,128)(2,1)S(1)}, bf16[1,512,4096]{2,1,0:T(8,128)(2,1)}, u32[]{:S(2)}) %copy-start.4) | copy-done | bytes 4194328
  44.1 1.4 %shard_map.139 = (bf16[128,1024]{1,0:T(8,128)(2,1)S(1)}, bf16[128,1024]{1,0:T(8,128)(2,1)S(1)}, bf16[128,1024]{1,0:T(8,128)(2,1)S(1)}, bf16[128,1024]{1,0:T(8,128)(2,1)S(1)}) custom-call(bf16[128,1024]{1,0:T(8,128)(2,1)S(1)} %collective-permute-done.19.refs_0_, bf16[128,1024]{1,0:T(8,128)(2,1)S(1)} %collective-permute-done.20.refs_1_, ...), custom_call_target="tpu_custom_call" | custom-call | tf_op jit(solution)/shard_map/pallas_call | solution.py:339
  45.5 0.1 collective-permute-start.21
  45.6 0.7 copy-done.5
  46.3 1.4 %shard_map.134 = (bf16[128,1024]{1,0:T(8,128)(2,1)S(1)}, bf16[128,1024]{1,0:T(8,128)(2,1)S(1)}, bf16[128,1024]{1,0:T(8,128)(2,1)S(1)}, bf16[128,1024]{1,0:T(8,128)(2,1)S(1)}) custom-call(bf16[128,1024]{1,0:T(8,128)(2,1)S(1)} %collective-permute-done.3.refs_0_, bf16[128,1024]{1,0:T(8,128)(2,1)S(1)} %collective-permute-done.4.refs_1_, ...), custom_call_target="tpu_custom_call" | custom-call | tf_op jit(solution)/shard_map/pallas_call | solution.py:339
  47.7 0.0 copy-start.7
  47.7 0.0 copy-start.8
  47.7 0.0 copy-start.6
  47.7 0.0 copy-start.9
  47.7 0.1 collective-permute-start.11
  47.8 0.9 %collective-permute-done.15.refs_2_ = bf16[384,256]{1,0:T(8,128)(2,1)S(1)} collective-permute-done((bf16[384,256]{1,0:T(8,128)(2,1)S(1)}, bf16[384,256]{1,0:T(8,128)(2,1)S(1)}, u32[]{:S(2)}, u32[]{:S(2)}) %collective-permute-start.15) | collective-permute-done | bytes 196640 | tf_op jit(solution)/shard_map/ppermute | solution.py:331
  48.8 0.1 collective-permute-start.23
  48.9 1.5 %collective-permute-start.18 = (bf16[768,256]{1,0:T(8,128)(2,1)S(1)}, bf16[768,256]{1,0:T(8,128)(2,1)S(1)}, u32[]{:S(2)}, u32[]{:S(2)}) collective-permute-start(bf16[768,256]{1,0:T(8,128)(2,1)S(1)} %pad_maximum_fusion), channel_id=1, source_target_pairs={{0,4},{4,0},{8,12},{12,8},{16,20},{20,16},{24,28},{28,24},{1,5},{5... | collective-permute-start | bytes 1179656 | tf_op jit(solution)/shard_map/ppermute | solution.py:331
  50.5 0.1 shard_map.140
  50.5 1.6 %collective-permute-start.22 = (bf16[128,1024]{1,0:T(8,128)(2,1)S(1)}, bf16[128,1024]{1,0:T(8,128)(2,1)S(1)}, u32[]{:S(2)}, u32[]{:S(2)}) collective-permute-start(bf16[128,1024]{1,0:T(8,128)(2,1)S(1)} %shard_map.140), channel_id=1, source_target_pairs={{0,2},{1,3},{2,0},{3,1},{4,6},{5,7},{6,4},{7,5},{8,10},{9,11},{10,... | collective-permute-start | bytes 786440 | tf_op jit(solution)/shard_map/ppermute | solution.py:331
  52.1 0.1 shard_map.135
  52.2 0.6 collective-permute-start.12
  52.8 0.6 collective-permute-start.17
  53.4 6.4 %collective-permute-done.22.refs_0_ = bf16[128,1024]{1,0:T(8,128)(2,1)S(1)} collective-permute-done((bf16[128,1024]{1,0:T(8,128)(2,1)S(1)}, bf16[128,1024]{1,0:T(8,128)(2,1)S(1)}, u32[]{:S(2)}, u32[]{:S(2)}) %collective-permute-start.22) | collective-permute-done | bytes 262176 | tf_op jit(solution)/shard_map/ppermute | solution.py:331
  59.8 0.1 shard_map.141
  59.9 0.6 collective-permute-start.24
  60.5 3.3 %collective-permute-done.17.refs_4_ = bf16[256,256]{1,0:T(8,128)(2,1)S(1)} collective-permute-done((bf16[256,256]{1,0:T(8,128)(2,1)S(1)}, bf16[256,256]{1,0:T(8,128)(2,1)S(1)}, u32[]{:S(2)}, u32[]{:S(2)}) %collective-permute-start.17) | collective-permute-done | bytes 131104 | tf_op jit(solution)/shard_map/ppermute | solution.py:331
  63.8 4.9 %collective-permute-start.26 = (bf16[32,1024]{1,0:T(8,128)(2,1)S(1)}, bf16[32,1024]{1,0:T(8,128)(2,1)S(1)}, u32[]{:S(2)}, u32[]{:S(2)}) collective-permute-start(bf16[32,1024]{1,0:T(8,128)(2,1)S(1)} %get-tuple-element.74), channel_id=1, source_target_pairs={{0,12},{4,8},{8,4},{12,0},{16,28},{20,24},{24,20},{28,16},{1,13},{... | collective-permute-start | bytes 196616 | tf_op jit(solution)/shard_map/ppermute | solution.py:331
  68.7 3.2 %shard_map.137 = (bf16[128,256]{1,0:T(8,128)(2,1)S(1)}, bf16[128,256]{1,0:T(8,128)(2,1)S(1)}, bf16[128,256]{1,0:T(8,128)(2,1)S(1)}, bf16[128,256]{1,0:T(8,128)(2,1)S(1)}) custom-call(f32[4]{0:T(128)S(1)} %copy-done.8, f32[1,256]{1,0:T(1,128)S(1)} %shard_map.136.gain_ref, bf16[384,256]{1,0:T(8,128)(2,1)S(1)} %get-tuple-element.58.refs_0_, ...), custom_call_target="tpu_custom_call" | custom-call | tf_op jit(solution)/shard_map/pallas_call | solution.py:339
  71.9 1.4 %collective-permute-start.28 = (bf16[32,1024]{1,0:T(8,128)(2,1)S(1)}, bf16[32,1024]{1,0:T(8,128)(2,1)S(1)}, u32[]{:S(2)}, u32[]{:S(2)}) collective-permute-start(bf16[32,1024]{1,0:T(8,128)(2,1)S(1)} %get-tuple-element.76), channel_id=1, source_target_pairs={{0,20},{4,16},{8,28},{12,24},{16,4},{20,0},{24,12},{28,8},{1,21},{... | collective-permute-start | bytes 196616 | tf_op jit(solution)/shard_map/ppermute | solution.py:331
  73.3 1.1 %collective-permute-start.30 = (bf16[32,1024]{1,0:T(8,128)(2,1)S(1)}, bf16[32,1024]{1,0:T(8,128)(2,1)S(1)}, u32[]{:S(2)}, u32[]{:S(2)}) collective-permute-start(bf16[32,1024]{1,0:T(8,128)(2,1)S(1)} %get-tuple-element.78), channel_id=1, source_target_pairs={{0,28},{4,24},{8,20},{12,16},{16,12},{20,8},{24,4},{28,0},{1,29},{... | collective-permute-start | bytes 196616 | tf_op jit(solution)/shard_map/ppermute | solution.py:331
  74.4 0.1 shard_map.138
  74.5 2.1 %collective-permute-start.25 = (bf16[256,256]{1,0:T(8,128)(2,1)S(1)}, bf16[256,256]{1,0:T(8,128)(2,1)S(1)}, u32[]{:S(2)}, u32[]{:S(2)}) collective-permute-start(bf16[256,256]{1,0:T(8,128)(2,1)S(1)} %get-tuple-element.73), channel_id=1, source_target_pairs={{0,8},{4,12},{8,0},{12,4},{16,24},{20,28},{24,16},{28,20},{1,9},{5... | collective-permute-start | bytes 393224 | tf_op jit(solution)/shard_map/ppermute | solution.py:331
  76.6 1.4 %collective-permute-start.27 = (bf16[256,256]{1,0:T(8,128)(2,1)S(1)}, bf16[256,256]{1,0:T(8,128)(2,1)S(1)}, u32[]{:S(2)}, u32[]{:S(2)}) collective-permute-start(bf16[256,256]{1,0:T(8,128)(2,1)S(1)} %get-tuple-element.75), channel_id=1, source_target_pairs={{0,16},{4,20},{8,24},{12,28},{16,0},{20,4},{24,8},{28,12},{1,17},{... | collective-permute-start | bytes 393224 | tf_op jit(solution)/shard_map/ppermute | solution.py:331
  77.9 1.4 %collective-permute-start.29 = (bf16[256,256]{1,0:T(8,128)(2,1)S(1)}, bf16[256,256]{1,0:T(8,128)(2,1)S(1)}, u32[]{:S(2)}, u32[]{:S(2)}) collective-permute-start(bf16[256,256]{1,0:T(8,128)(2,1)S(1)} %get-tuple-element.77), channel_id=1, source_target_pairs={{0,24},{4,28},{8,16},{12,20},{16,8},{20,12},{24,0},{28,4},{1,25},{... | collective-permute-start | bytes 393224 | tf_op jit(solution)/shard_map/ppermute | solution.py:331
  79.4 0.2 shard_map.131
  79.6 1.5 %collective-permute-done.30.refs_7_ = bf16[32,1024]{1,0:T(8,128)(2,1)S(1)} collective-permute-done((bf16[32,1024]{1,0:T(8,128)(2,1)S(1)}, bf16[32,1024]{1,0:T(8,128)(2,1)S(1)}, u32[]{:S(2)}, u32[]{:S(2)}) %collective-permute-start.30) | collective-permute-done | bytes 65568 | tf_op jit(solution)/shard_map/ppermute | solution.py:331
  81.0 0.4 collective-permute-done.25.refs_2_
  81.4 8.1 %collective-permute-done.27.refs_4_ = bf16[256,256]{1,0:T(8,128)(2,1)S(1)} collective-permute-done((bf16[256,256]{1,0:T(8,128)(2,1)S(1)}, bf16[256,256]{1,0:T(8,128)(2,1)S(1)}, u32[]{:S(2)}, u32[]{:S(2)}) %collective-permute-start.27) | collective-permute-done | bytes 131104 | tf_op jit(solution)/shard_map/ppermute | solution.py:331
  89.6 1.0 %shard_map.142 = (bf16[64,1024]{1,0:T(8,128)(2,1)}, bf16[128,1024]{1,0:T(8,128)(2,1)}) custom-call(bf16[256,64]{1,0:T(8,128)(2,1)S(1)} %get-tuple-element.42.high_ref, bf16[256,64]{1,0:T(8,128)(2,1)S(1)} %get-tuple-element.43.low_ref, bf16[32,1024]{1,0:T(8,128)(2,1)S(1)} %get-tuple-element.65.refs_0_, bf16[32,1024]{1,0:T(8,128)(2,1)S(1)} %collective-permute-done.24.refs_1_, ...), custom_call_target="tpu_custom_call" | custom-call | tf_op jit(solution)/shard_map/pallas_call | solution.py:339
  (43 shorter events, 0.2 us)
Async XLA Ops:
  2.3 9.0 %collective-permute-start.5 = (bf16[32,1024]{1,0:T(8,128)(2,1)S(1)}, bf16[32,1024]{1,0:T(8,128)(2,1)S(1)}, u32[]{:S(2)}, u32[]{:S(2)}) collective-permute-start(bf16[32,1024]{1,0:T(8,128)(2,1)S(1)} %get-tuple-element.48), channel_id=1, source_target_pairs={{0,4},{4,0},{8,12},{12,8},{16,20},{20,16},{24,28},{28,24},{1,5},{5... | collective-permute-start | bytes 196616 | tf_op jit(solution)/shard_map/ppermute | solution.py:331
  5.4 9.5 %collective-permute-start.6 = (bf16[32,1024]{1,0:T(8,128)(2,1)S(1)}, bf16[32,1024]{1,0:T(8,128)(2,1)S(1)}, u32[]{:S(2)}, u32[]{:S(2)}) collective-permute-start(bf16[32,1024]{1,0:T(8,128)(2,1)S(1)} %get-tuple-element.49), channel_id=1, source_target_pairs={{0,12},{4,8},{8,4},{12,0},{16,28},{20,24},{24,20},{28,16},{1,13},{... | collective-permute-start | bytes 196616 | tf_op jit(solution)/shard_map/ppermute | solution.py:331
  6.9 8.1 %collective-permute-start.7 = (bf16[32,1024]{1,0:T(8,128)(2,1)S(1)}, bf16[32,1024]{1,0:T(8,128)(2,1)S(1)}, u32[]{:S(2)}, u32[]{:S(2)}) collective-permute-start(bf16[32,1024]{1,0:T(8,128)(2,1)S(1)} %get-tuple-element.50), channel_id=1, source_target_pairs={{0,20},{4,16},{8,28},{12,24},{16,4},{20,0},{24,12},{28,8},{1,21},{... | collective-permute-start | bytes 196616 | tf_op jit(solution)/shard_map/ppermute | solution.py:331
  10.4 7.2 %collective-permute-start.8 = (bf16[32,1024]{1,0:T(8,128)(2,1)S(1)}, bf16[32,1024]{1,0:T(8,128)(2,1)S(1)}, u32[]{:S(2)}, u32[]{:S(2)}) collective-permute-start(bf16[32,1024]{1,0:T(8,128)(2,1)S(1)} %get-tuple-element.51), channel_id=1, source_target_pairs={{0,28},{4,24},{8,20},{12,16},{16,12},{20,8},{24,4},{28,0},{1,29},{... | collective-permute-start | bytes 196616 | tf_op jit(solution)/shard_map/ppermute | solution.py:331
  10.4 8.7 %collective-permute-start = (bf16[32,1024]{1,0:T(8,128)(2,1)S(1)}, bf16[32,1024]{1,0:T(8,128)(2,1)S(1)}, u32[]{:S(2)}, u32[]{:S(2)}) collective-permute-start(bf16[32,1024]{1,0:T(8,128)(2,1)S(1)} %get-tuple-element.45), channel_id=1, source_target_pairs={{0,8},{4,12},{8,0},{12,4},{16,24},{20,28},{24,16},{28,20},{1,9},{5... | collective-permute-start | bytes 196616 | tf_op jit(solution)/shard_map/ppermute | solution.py:331
  11.3 9.0 %collective-permute-start.1 = (bf16[32,1024]{1,0:T(8,128)(2,1)S(1)}, bf16[32,1024]{1,0:T(8,128)(2,1)S(1)}, u32[]{:S(2)}, u32[]{:S(2)}) collective-permute-start(bf16[32,1024]{1,0:T(8,128)(2,1)S(1)} %get-tuple-element.46), channel_id=1, source_target_pairs={{0,16},{4,20},{8,24},{12,28},{16,0},{20,4},{24,8},{28,12},{1,17},{... | collective-permute-start | bytes 196616 | tf_op jit(solution)/shard_map/ppermute | solution.py:331
  14.9 6.2 %collective-permute-start.2 = (bf16[32,1024]{1,0:T(8,128)(2,1)S(1)}, bf16[32,1024]{1,0:T(8,128)(2,1)S(1)}, u32[]{:S(2)}, u32[]{:S(2)}) collective-permute-start(bf16[32,1024]{1,0:T(8,128)(2,1)S(1)} %get-tuple-element.47), channel_id=1, source_target_pairs={{0,24},{4,28},{8,16},{12,20},{16,8},{20,12},{24,0},{28,4},{1,25},{... | collective-permute-start | bytes 196616 | tf_op jit(solution)/shard_map/ppermute | solution.py:331
  17.6 9.1 %collective-permute-start.19 = (bf16[128,1024]{1,0:T(8,128)(2,1)S(1)}, bf16[128,1024]{1,0:T(8,128)(2,1)S(1)}, u32[]{:S(2)}, u32[]{:S(2)}) collective-permute-start(bf16[128,1024]{1,0:T(8,128)(2,1)S(1)} %constant_dynamic-update-slice_fusion.4.refs_0_), channel_id=1, source_target_pairs={{0,2},{1,3},{2,0},{3,1},{4,6},{5,7},{6,4},{7,5},{8,10},{9,11},{10,... | collective-permute-start | bytes 786440 | tf_op jit(solution)/shard_map/ppermute | solution.py:331
  21.1 8.5 %collective-permute-start.3 = (bf16[128,1024]{1,0:T(8,128)(2,1)S(1)}, bf16[128,1024]{1,0:T(8,128)(2,1)S(1)}, u32[]{:S(2)}, u32[]{:S(2)}) collective-permute-start(bf16[128,1024]{1,0:T(8,128)(2,1)S(1)} %constant_dynamic-update-slice_fusion.refs_1_), channel_id=1, source_target_pairs={{0,2},{1,3},{2,0},{3,1},{4,6},{5,7},{6,4},{7,5},{8,10},{9,11},{10,... | collective-permute-start | bytes 786440 | tf_op jit(solution)/shard_map/ppermute | solution.py:331
  22.6 9.0 %collective-permute-start.9 = (bf16[128,1024]{1,0:T(8,128)(2,1)S(1)}, bf16[128,1024]{1,0:T(8,128)(2,1)S(1)}, u32[]{:S(2)}, u32[]{:S(2)}) collective-permute-start(bf16[128,1024]{1,0:T(8,128)(2,1)S(1)} %constant_dynamic-update-slice_fusion.4.refs_0_), channel_id=1, source_target_pairs={{0,1},{1,0},{2,3},{3,2},{4,5},{5,4},{6,7},{7,6},{8,9},{9,8},{10,11... | collective-permute-start | bytes 786440 | tf_op jit(solution)/shard_map/ppermute | solution.py:331
  22.6 9.7 %collective-permute-start.10 = (bf16[128,1024]{1,0:T(8,128)(2,1)S(1)}, bf16[128,1024]{1,0:T(8,128)(2,1)S(1)}, u32[]{:S(2)}, u32[]{:S(2)}) collective-permute-start(bf16[128,1024]{1,0:T(8,128)(2,1)S(1)} %constant_dynamic-update-slice_fusion.refs_1_), channel_id=1, source_target_pairs={{0,1},{1,0},{2,3},{3,2},{4,5},{5,4},{6,7},{7,6},{8,9},{9,8},{10,11... | collective-permute-start | bytes 786440 | tf_op jit(solution)/shard_map/ppermute | solution.py:331
  26.7 12.9 %collective-permute-start.20 = (bf16[128,1024]{1,0:T(8,128)(2,1)S(1)}, bf16[128,1024]{1,0:T(8,128)(2,1)S(1)}, u32[]{:S(2)}, u32[]{:S(2)}) collective-permute-start(bf16[128,1024]{1,0:T(8,128)(2,1)S(1)} %collective-permute-done.19.refs_0_), channel_id=1, source_target_pairs={{0,1},{1,0},{2,3},{3,2},{4,5},{5,4},{6,7},{7,6},{8,9},{9,8},{10,11... | collective-permute-start | bytes 786440 | tf_op jit(solution)/shard_map/ppermute | solution.py:331
  29.6 15.9 %collective-permute-start.4 = (bf16[128,1024]{1,0:T(8,128)(2,1)S(1)}, bf16[128,1024]{1,0:T(8,128)(2,1)S(1)}, u32[]{:S(2)}, u32[]{:S(2)}) collective-permute-start(bf16[128,1024]{1,0:T(8,128)(2,1)S(1)} %collective-permute-done.3.refs_0_), channel_id=1, source_target_pairs={{0,1},{1,0},{2,3},{3,2},{4,5},{5,4},{6,7},{7,6},{8,9},{9,8},{10,11... | collective-permute-start | bytes 786440 | tf_op jit(solution)/shard_map/ppermute | solution.py:331
  29.6 18.2 %collective-permute-start.14 = (bf16[384,256]{1,0:T(8,128)(2,1)S(1)}, bf16[384,256]{1,0:T(8,128)(2,1)S(1)}, u32[]{:S(2)}, u32[]{:S(2)}) collective-permute-start(bf16[384,256]{1,0:T(8,128)(2,1)S(1)} %get-tuple-element.59), channel_id=1, source_target_pairs={{0,8},{4,12},{8,0},{12,4},{16,24},{20,28},{24,16},{28,20},{1,9},{5... | collective-permute-start | bytes 589832 | tf_op jit(solution)/shard_map/ppermute | solution.py:331
  31.6 17.1 %collective-permute-start.15 = (bf16[384,256]{1,0:T(8,128)(2,1)S(1)}, bf16[384,256]{1,0:T(8,128)(2,1)S(1)}, u32[]{:S(2)}, u32[]{:S(2)}) collective-permute-start(bf16[384,256]{1,0:T(8,128)(2,1)S(1)} %get-tuple-element.60), channel_id=1, source_target_pairs={{0,16},{4,20},{8,24},{12,28},{16,0},{20,4},{24,8},{28,12},{1,17},{... | collective-permute-start | bytes 589832 | tf_op jit(solution)/shard_map/ppermute | solution.py:331
  32.3 16.5 %collective-permute-start.16 = (bf16[384,256]{1,0:T(8,128)(2,1)S(1)}, bf16[384,256]{1,0:T(8,128)(2,1)S(1)}, u32[]{:S(2)}, u32[]{:S(2)}) collective-permute-start(bf16[384,256]{1,0:T(8,128)(2,1)S(1)} %get-tuple-element.61), channel_id=1, source_target_pairs={{0,24},{4,28},{8,16},{12,20},{16,8},{20,12},{24,0},{28,4},{1,25},{... | collective-permute-start | bytes 589832 | tf_op jit(solution)/shard_map/ppermute | solution.py:331
  34.0 2.2 %copy-start = (bf16[1,4096,512]{2,1,0:T(8,128)(2,1)S(1)}, bf16[1,4096,512]{2,1,0:T(8,128)(2,1)}, u32[]{:S(2)}) copy-start(bf16[1,4096,512]{2,1,0:T(8,128)(2,1)} %param.21) | copy-start | bytes 12582916
  36.2 2.2 %copy-start.2 = (bf16[1,4096,512]{2,1,0:T(8,128)(2,1)S(1)}, bf16[1,4096,512]{2,1,0:T(8,128)(2,1)}, u32[]{:S(2)}) copy-start(bf16[1,4096,512]{2,1,0:T(8,128)(2,1)} %param.22) | copy-start | bytes 12582916
  38.4 2.2 %copy-start.1 = (bf16[1,4096,512]{2,1,0:T(8,128)(2,1)S(1)}, bf16[1,4096,512]{2,1,0:T(8,128)(2,1)}, u32[]{:S(2)}) copy-start(bf16[1,4096,512]{2,1,0:T(8,128)(2,1)} %param.21) | copy-start | bytes 12582916
  38.4 3.5 %copy-start.3 = (bf16[1,4096,512]{2,1,0:T(8,128)(2,1)S(1)}, bf16[1,4096,512]{2,1,0:T(8,128)(2,1)}, u32[]{:S(2)}) copy-start(bf16[1,4096,512]{2,1,0:T(8,128)(2,1)} %param.22) | copy-start | bytes 12582916
  41.9 2.2 %copy-start.4 = (bf16[1,512,4096]{2,1,0:T(8,128)(2,1)S(1)}, bf16[1,512,4096]{2,1,0:T(8,128)(2,1)}, u32[]{:S(2)}) copy-start(bf16[1,512,4096]{2,1,0:T(8,128)(2,1)} %param.23) | copy-start | bytes 12582916
  44.1 2.2 %copy-start.5 = (bf16[1,512,4096]{2,1,0:T(8,128)(2,1)S(1)}, bf16[1,512,4096]{2,1,0:T(8,128)(2,1)}, u32[]{:S(2)}) copy-start(bf16[1,512,4096]{2,1,0:T(8,128)(2,1)} %param.23) | copy-start | bytes 12582916
  45.5 5.0 %collective-permute-start.21 = (bf16[128,1024]{1,0:T(8,128)(2,1)S(1)}, bf16[128,1024]{1,0:T(8,128)(2,1)S(1)}, u32[]{:S(2)}, u32[]{:S(2)}) collective-permute-start(bf16[128,1024]{1,0:T(8,128)(2,1)S(1)} %get-tuple-element.69), channel_id=1, source_target_pairs={{0,1},{1,0},{2,3},{3,2},{4,5},{5,4},{6,7},{7,6},{8,9},{9,8},{10,11... | collective-permute-start | bytes 786440 | tf_op jit(solution)/shard_map/ppermute | solution.py:331
  47.7 21.0 %copy-start.7 = (f32[256]{0:T(256)S(1)}, f32[256]{0:T(256)}, u32[]{:S(2)}) copy-start(f32[256]{0:T(256)} %param.16) | copy-start | bytes 3076
  47.7 21.0 %copy-start.8 = (f32[4]{0:T(128)S(1)}, f32[4]{0:T(128)}, u32[]{:S(2)}) copy-start(f32[4]{0:T(128)} %lambda_ref.1) | copy-start | bytes 52
  47.7 31.7 %copy-start.6 = (s32[64,2]{0,1:T(2,128)S(1)}, s32[64,2]{0,1:T(2,128)}, u32[]{:S(2)}) copy-start(s32[64,2]{0,1:T(2,128)} %param.19) | copy-start | bytes 1540
  47.7 31.7 %copy-start.9 = (f32[64,2]{0,1:T(2,128)S(1)}, f32[64,2]{0,1:T(2,128)}, u32[]{:S(2)}) copy-start(f32[64,2]{0,1:T(2,128)} %param.20) | copy-start | bytes 1540
  47.7 4.4 %collective-permute-start.11 = (bf16[128,1024]{1,0:T(8,128)(2,1)S(1)}, bf16[128,1024]{1,0:T(8,128)(2,1)S(1)}, u32[]{:S(2)}, u32[]{:S(2)}) collective-permute-start(bf16[128,1024]{1,0:T(8,128)(2,1)S(1)} %get-tuple-element.55), channel_id=1, source_target_pairs={{0,1},{1,0},{2,3},{3,2},{4,5},{5,4},{6,7},{7,6},{8,9},{9,8},{10,11... | collective-permute-start | bytes 786440 | tf_op jit(solution)/shard_map/ppermute | solution.py:331
  48.8 4.0 %collective-permute-start.23 = (bf16[128,1024]{1,0:T(8,128)(2,1)S(1)}, bf16[128,1024]{1,0:T(8,128)(2,1)S(1)}, u32[]{:S(2)}, u32[]{:S(2)}) collective-permute-start(bf16[128,1024]{1,0:T(8,128)(2,1)S(1)} %get-tuple-element.71), channel_id=1, source_target_pairs={{0,1},{1,0},{2,3},{3,2},{4,5},{5,4},{6,7},{7,6},{8,9},{9,8},{10,11... | collective-permute-start | bytes 786440 | tf_op jit(solution)/shard_map/ppermute | solution.py:331
  48.9 19.8 %collective-permute-start.18 = (bf16[768,256]{1,0:T(8,128)(2,1)S(1)}, bf16[768,256]{1,0:T(8,128)(2,1)S(1)}, u32[]{:S(2)}, u32[]{:S(2)}) collective-permute-start(bf16[768,256]{1,0:T(8,128)(2,1)S(1)} %pad_maximum_fusion), channel_id=1, source_target_pairs={{0,4},{4,0},{8,12},{12,8},{16,20},{20,16},{24,28},{28,24},{1,5},{5... | collective-permute-start | bytes 1179656 | tf_op jit(solution)/shard_map/ppermute | solution.py:331
  50.5 9.2 %collective-permute-start.22 = (bf16[128,1024]{1,0:T(8,128)(2,1)S(1)}, bf16[128,1024]{1,0:T(8,128)(2,1)S(1)}, u32[]{:S(2)}, u32[]{:S(2)}) collective-permute-start(bf16[128,1024]{1,0:T(8,128)(2,1)S(1)} %shard_map.140), channel_id=1, source_target_pairs={{0,2},{1,3},{2,0},{3,1},{4,6},{5,7},{6,4},{7,5},{8,10},{9,11},{10,... | collective-permute-start | bytes 786440 | tf_op jit(solution)/shard_map/ppermute | solution.py:331
  52.1 21.2 %collective-permute-start.13 = (bf16[128,1024]{1,0:T(8,128)(2,1)S(1)}, bf16[128,1024]{1,0:T(8,128)(2,1)S(1)}, u32[]{:S(2)}, u32[]{:S(2)}) collective-permute-start(bf16[128,1024]{1,0:T(8,128)(2,1)S(1)} %get-tuple-element.57), channel_id=1, source_target_pairs={{0,1},{1,0},{2,3},{3,2},{4,5},{5,4},{6,7},{7,6},{8,9},{9,8},{10,11... | collective-permute-start | bytes 786440 | tf_op jit(solution)/shard_map/ppermute | solution.py:331
  52.2 22.2 %collective-permute-start.12 = (bf16[128,1024]{1,0:T(8,128)(2,1)S(1)}, bf16[128,1024]{1,0:T(8,128)(2,1)S(1)}, u32[]{:S(2)}, u32[]{:S(2)}) collective-permute-start(bf16[128,1024]{1,0:T(8,128)(2,1)S(1)} %shard_map.135), channel_id=1, source_target_pairs={{0,2},{1,3},{2,0},{3,1},{4,6},{5,7},{6,4},{7,5},{8,10},{9,11},{10,... | collective-permute-start | bytes 786440 | tf_op jit(solution)/shard_map/ppermute | solution.py:331
  52.8 11.0 %collective-permute-start.17 = (bf16[256,256]{1,0:T(8,128)(2,1)S(1)}, bf16[256,256]{1,0:T(8,128)(2,1)S(1)}, u32[]{:S(2)}, u32[]{:S(2)}) collective-permute-start(bf16[256,256]{1,0:T(8,128)(2,1)S(1)} %slice.12), channel_id=1, source_target_pairs={{0,4},{4,0},{8,12},{12,8},{16,20},{20,16},{24,28},{28,24},{1,5},{5... | collective-permute-start | bytes 393224 | tf_op jit(solution)/shard_map/ppermute | solution.py:331
  59.9 16.7 %collective-permute-start.24 = (bf16[32,1024]{1,0:T(8,128)(2,1)S(1)}, bf16[32,1024]{1,0:T(8,128)(2,1)S(1)}, u32[]{:S(2)}, u32[]{:S(2)}) collective-permute-start(bf16[32,1024]{1,0:T(8,128)(2,1)S(1)} %get-tuple-element.72), channel_id=1, source_target_pairs={{0,4},{4,0},{8,12},{12,8},{16,20},{20,16},{24,28},{28,24},{1,5},{5... | collective-permute-start | bytes 196616 | tf_op jit(solution)/shard_map/ppermute | solution.py:331
  63.8 14.1 %collective-permute-start.26 = (bf16[32,1024]{1,0:T(8,128)(2,1)S(1)}, bf16[32,1024]{1,0:T(8,128)(2,1)S(1)}, u32[]{:S(2)}, u32[]{:S(2)}) collective-permute-start(bf16[32,1024]{1,0:T(8,128)(2,1)S(1)} %get-tuple-element.74), channel_id=1, source_target_pairs={{0,12},{4,8},{8,4},{12,0},{16,28},{20,24},{24,20},{28,16},{1,13},{... | collective-permute-start | bytes 196616 | tf_op jit(solution)/shard_map/ppermute | solution.py:331
  71.9 7.6 %collective-permute-start.28 = (bf16[32,1024]{1,0:T(8,128)(2,1)S(1)}, bf16[32,1024]{1,0:T(8,128)(2,1)S(1)}, u32[]{:S(2)}, u32[]{:S(2)}) collective-permute-start(bf16[32,1024]{1,0:T(8,128)(2,1)S(1)} %get-tuple-element.76), channel_id=1, source_target_pairs={{0,20},{4,16},{8,28},{12,24},{16,4},{20,0},{24,12},{28,8},{1,21},{... | collective-permute-start | bytes 196616 | tf_op jit(solution)/shard_map/ppermute | solution.py:331
  73.3 7.8 %collective-permute-start.30 = (bf16[32,1024]{1,0:T(8,128)(2,1)S(1)}, bf16[32,1024]{1,0:T(8,128)(2,1)S(1)}, u32[]{:S(2)}, u32[]{:S(2)}) collective-permute-start(bf16[32,1024]{1,0:T(8,128)(2,1)S(1)} %get-tuple-element.78), channel_id=1, source_target_pairs={{0,28},{4,24},{8,20},{12,16},{16,12},{20,8},{24,4},{28,0},{1,29},{... | collective-permute-start | bytes 196616 | tf_op jit(solution)/shard_map/ppermute | solution.py:331
  74.5 7.0 %collective-permute-start.25 = (bf16[256,256]{1,0:T(8,128)(2,1)S(1)}, bf16[256,256]{1,0:T(8,128)(2,1)S(1)}, u32[]{:S(2)}, u32[]{:S(2)}) collective-permute-start(bf16[256,256]{1,0:T(8,128)(2,1)S(1)} %get-tuple-element.73), channel_id=1, source_target_pairs={{0,8},{4,12},{8,0},{12,4},{16,24},{20,28},{24,16},{28,20},{1,9},{5... | collective-permute-start | bytes 393224 | tf_op jit(solution)/shard_map/ppermute | solution.py:331
  76.6 13.0 %collective-permute-start.27 = (bf16[256,256]{1,0:T(8,128)(2,1)S(1)}, bf16[256,256]{1,0:T(8,128)(2,1)S(1)}, u32[]{:S(2)}, u32[]{:S(2)}) collective-permute-start(bf16[256,256]{1,0:T(8,128)(2,1)S(1)} %get-tuple-element.75), channel_id=1, source_target_pairs={{0,16},{4,20},{8,24},{12,28},{16,0},{20,4},{24,8},{28,12},{1,17},{... | collective-permute-start | bytes 393224 | tf_op jit(solution)/shard_map/ppermute | solution.py:331
  77.9 11.7 %collective-permute-start.29 = (bf16[256,256]{1,0:T(8,128)(2,1)S(1)}, bf16[256,256]{1,0:T(8,128)(2,1)S(1)}, u32[]{:S(2)}, u32[]{:S(2)}) collective-permute-start(bf16[256,256]{1,0:T(8,128)(2,1)S(1)} %get-tuple-element.77), channel_id=1, source_target_pairs={{0,24},{4,28},{8,16},{12,20},{16,8},{20,12},{24,0},{28,4},{1,25},{... | collective-permute-start | bytes 393224 | tf_op jit(solution)/shard_map/ppermute | solution.py:331

commit v3 on v2

--- a/solution.py
+++ b/solution.py
@@ -1,4 +1,5 @@
 import functools
+import math
 
 import jax
 import jax.numpy as jnp
@@ -17,6 +18,7 @@
 head_eps = 1e-05
 moe_eps = 1e-06
 head_scale = 0.8
+per_score = QKD ** (-0.5) * math.log2(math.e)
 
 VMEM = pl.BlockSpec(memory_space=pltpu.VMEM)
 SMEM = pl.BlockSpec(memory_space=pltpu.SMEM)
@@ -38,6 +40,10 @@
 def where_am_i(nx):
     ep = lax.axis_index("ep")
     return lax.div(ep, nx), lax.rem(ep, nx), lax.axis_index("tp")
+
+
+def columns_of(q, width):
+    return pl.ds(pl.multiple_of((lax.axis_index("tp") ^ q) * width, width), width)
 
 
 def slot_hits(nz, nx, cap, routes):
@@ -55,13 +61,14 @@
     return place[:, None, :] == slot, first
 
 
-def prep_kernel(nz, nx, cap, width, wide, tokens_ref, gain_ref, routes_ref, *refs):
+def prep_kernel(nz, nx, cap, width, near, wide, tokens_ref, gain_ref, routes_ref, scores_ref, *refs):
     blocks = nz * nx
-    tokens_s, gain_s, routes_s, sems = refs[-4:]
+    routes_s, scores_s, tokens_s, gain_s, sems = refs[-5:]
     copies = [
         pltpu.make_async_copy(routes_ref, routes_s, sems.at[0]),
         pltpu.make_async_copy(tokens_ref, tokens_s, sems.at[1]),
         pltpu.make_async_copy(gain_ref, gain_s, sems.at[2]),
+        pltpu.make_async_copy(scores_ref, scores_s, sems.at[3]),
     ]
     slices = []
     if wide:
@@ -72,7 +79,7 @@
             columns = pl.ds(pl.multiple_of((z ^ k) * wide, wide), wide)
             for i, source in enumerate(sources):
                 target = refs[blocks + k].at[pl.ds(i * count, count), :]
-                sem = sems.at[3 + 3 * k + i]
+                sem = sems.at[4 + 3 * k + i]
                 slices.append(pltpu.make_async_copy(source.at[:, columns], target, sem))
     out_refs = refs[:blocks]
     for copy in copies + slices:
@@ -85,11 +92,13 @@
         copy.wait()
     tokens = tokens_s[...].astype(jnp.float32)
     scale = lax.rsqrt(jnp.mean(tokens * tokens, axis=-1, keepdims=True) + moe_eps)
-    columns = pl.ds(pl.multiple_of(lax.axis_index("tp") * width, width), width)
-    normed = tokens_s[:, columns].astype(jnp.float32) * scale * gain_s[:, columns]
-    picked = dot(picker, normed.astype(jnp.bfloat16)).astype(jnp.bfloat16)
-    for j in range(blocks):
-        out_refs[j][...] = picked[j * cap : (j + 1) * cap]
+    for q in range(0, tokens.shape[1] // width, 2):
+        columns = columns_of(q, width)
+        normed = tokens_s[:, columns].astype(jnp.float32) * scale * gain_s[:, columns]
+        count = near * nx if q else blocks
+        picked = dot(picker[: count * cap], normed.astype(jnp.bfloat16)).astype(jnp.bfloat16)
+        for j in range(count):
+            out_refs[j][q // 2 * cap : (q // 2 + 1) * cap, :] = picked[j * cap : (j + 1) * cap]
     for copy in slices:
         copy.wait()
 
@@ -107,33 +116,22 @@
     low_ref[...] = (weight - high.astype(jnp.float32)).astype(jnp.bfloat16)
 
 
-def total_of(refs):
-    total = refs[0][...].astype(jnp.float32)
-    for ref in refs[1:]:
-        total = total + ref[...].astype(jnp.float32)
+def total_of(refs, first=0, count=None):
+    count = count or refs[0].shape[0]
+    total = 0.0
+    for ref in refs:
+        base = 0 if ref.shape[0] == count else first
+        total = total + ref[base : base + count, :].astype(jnp.float32)
     return total.astype(jnp.bfloat16)
 
 
-def add_kernel(n_sums, *refs):
-    total = total_of(refs[:n_sums])
-    count = refs[n_sums].shape[0]
-    for k, out_ref in enumerate(refs[n_sums:]):
-        out_ref[...] = total[k * count : (k + 1) * count]
-
-
-def blend_kernel(nz, cap, n_sums, *refs):
-    sum_refs, refs = refs[:n_sums], refs[n_sums:]
-    attend_refs, near_ref, out_refs = refs[: nz - 1], refs[nz - 1], refs[nz:]
-    total = total_of(sum_refs)
-    near_ref[...] = total[:cap]
-    for k in range(1, nz):
-        out_ref = out_refs[k - 1]
-        count, wide = attend_refs[k - 1].shape
-        out_ref[:count, :] = attend_refs[k - 1][...]
-        for c in range(total.shape[1] // wide):
-            out_ref[count + c * cap : count + (c + 1) * cap, :] = total[
-                k * cap : (k + 1) * cap, c * wide : (c + 1) * wide
-            ]
+def add_kernel(n_sums, first, *refs):
+    outs = refs[n_sums:]
+    total = total_of(refs[:n_sums], first, sum(ref.shape[0] for ref in outs))
+    row = 0
+    for out_ref in outs:
+        out_ref[...] = total[row : row + out_ref.shape[0]]
+        row += out_ref.shape[0]
 
 
 def finish_kernel(nz, nx, cap, wide, high_ref, low_ref, *refs):
@@ -141,25 +139,17 @@
     *refs, held, out_s, sems = refs
     copies = []
     if wide:
-        own_ref, out_ref, attended_ref = refs
+        *heads, out_ref, attended_ref = refs
         z = where_am_i(nx)[0]
-        count = own_ref.shape[0]
         for k in range(nz):
-            source = blocks[k * nx].at[pl.ds(0, count), :] if k else own_ref
             columns = pl.ds(pl.multiple_of((z ^ k) * wide, wide), wide)
-            copies.append(pltpu.make_async_copy(source, attended_ref.at[:, columns], sems.at[k]))
+            copies.append(pltpu.make_async_copy(heads[k], attended_ref.at[:, columns], sems.at[k]))
     else:
         (out_ref,) = refs
     for copy in copies:
         copy.start()
     for j, ref in enumerate(blocks):
-        slots = slice(j * cap, (j + 1) * cap)
-        if wide and j >= nx and j % nx == 0:
-            for c in range(held.shape[1] // wide):
-                first = count + c * cap
-                held[slots, c * wide : (c + 1) * wide] = ref[first : first + cap, :]
-        else:
-            held[slots, :] = ref[...]
+        held[j * cap : (j + 1) * cap, :] = ref[...]
     returned = held[...]
     rows = ((0,), (0,))
     out_s[...] = (
@@ -175,25 +165,13 @@
     out_ref[...] = in_ref[...]
 
 
-def columns_of(q, width):
-    return pl.ds(pl.multiple_of((lax.axis_index("tp") ^ q) * width, width), width)
-
-
-def early_kernel(groups, *refs):
-    row_refs, (gate_ref, up_ref), out_refs = (
-        refs[: 2 * groups],
-        refs[2 * groups : 2 * groups + 2],
-        refs[2 * groups + 2 :],
-    )
-    rows = [
-        jnp.concatenate([ref[...] for ref in row_refs[q * groups : (q + 1) * groups]], axis=0)
-        for q in range(2)
-    ]
-    size = row_refs[0].shape[0]
-    width = rows[0].shape[1]
+def early_kernel(first_ref, second_ref, gate_ref, up_ref, *out_refs):
+    width = first_ref.shape[1]
+    groups = len(out_refs) // 2
+    size = first_ref.shape[0] // groups
     for i, ref in enumerate((gate_ref, up_ref)):
-        product = dot(rows[0], ref[columns_of(0, width), :])
-        product = product + dot(rows[1], ref[columns_of(1, width), :])
+        product = dot(first_ref[...], ref[columns_of(0, width), :])
+        product = product + dot(second_ref[...], ref[columns_of(1, width), :])
         for g in range(groups):
             out_refs[i * groups + g][...] = product[g * size : (g + 1) * size]
 
@@ -213,9 +191,10 @@
         out_refs[q][...] = dot(hidden, block).astype(jnp.bfloat16)
 
 
-def attend_kernel(nz, nx, heads, lambda_ref, gain_ref, *refs):
+def attend_kernel(nz, nx, heads, swaps, lambda_ref, gain_ref, *refs):
     pack_refs, refs = refs[:nz], refs[nz:]
-    near_refs, rest_refs, refs = refs[: nx - 1], refs[nx - 1 : 2 * nx - 2], refs[2 * nx - 2 :]
+    count = (nx - 1) * len(swaps)
+    swap_refs, refs = refs[:count], refs[count:]
     out_refs = refs[:nz]
     query_s, key_s, value_s, out_s = refs[nz:]
     z, x, _ = where_am_i(nx)
@@ -229,19 +208,18 @@
         for m in range(nx):
             if m == 0:
                 source, first = pack_refs[k], 0
-            elif k == 0:
-                source, first = near_refs[m - 1], 0
             else:
-                source, first = rest_refs[m - 1], (k - 1) * 2 * rows
+                i = next(i for i, group in enumerate(swaps) if k in group)
+                source, first = swap_refs[i * (nx - 1) + m - 1], swaps[i].index(k) * 2 * rows
             block = at((z ^ k) * nx + (x ^ m))
             key_s[block, :] = source[first : first + rows, :]
             value_s[block, :] = source[first + rows : first + 2 * rows, :]
     for head in range(heads):
         weight = lambda_ref[z * heads + head]
         for group in range(nz):
-            count = (group + 1) * nx * rows
-            query_pos = (group * nx + x) * rows + lax.broadcasted_iota(jnp.int32, (rows, count), 0)
-            visible = lax.broadcasted_iota(jnp.int32, (rows, count), 1) <= query_pos
+            count, last = (group + 1) * nx * rows, nx * rows
+            query_pos = x * rows + lax.broadcasted_iota(jnp.int32, (rows, last), 0)
+            visible = lax.broadcasted_iota(jnp.int32, (rows, last), 1) <= query_pos
             maps = []
             for index in range(2):
                 lanes = slice(head * VD + index * QKD, head * VD + (index + 1) * QKD)
@@ -250,15 +228,15 @@
                     key_s[:count, lanes],
                     ((1,), (1,)),
                 )
-                scores = jnp.where(visible, scores * QKD ** (-0.5), neg_big)
-                weights = jnp.exp(scores - jnp.max(scores, axis=-1, keepdims=True))
+                diagonal = jnp.where(visible, scores[:, count - last :], neg_big)
+                if group:
+                    diagonal = jnp.concatenate([scores[:, : count - last], diagonal], axis=1)
+                scores = diagonal
+                weights = jnp.exp2((scores - jnp.max(scores, axis=-1, keepdims=True)) * per_score)
                 maps.append((weights, jnp.sum(weights, axis=-1, keepdims=True)))
             mixing = maps[0][0] * (1.0 / maps[0][1]) - maps[1][0] * (weight / maps[1][1])
             lanes = slice(head * VD, (head + 1) * VD)
-            high = mixing.astype(jnp.bfloat16)
-            low = (mixing - high.astype(jnp.float32)).astype(jnp.bfloat16)
-            held = value_s[:count, lanes]
-            mixed = dot(high, held) + dot(low, held)
+            mixed = dot(mixing.astype(jnp.bfloat16), value_s[:count, lanes])
             scaled = mixed * lax.rsqrt(jnp.mean(mixed * mixed, axis=-1, keepdims=True) + head_eps)
             scaled = scaled * gain_ref[...] * head_scale
             out_s[group * rows : (group + 1) * rows, lanes] = scaled.astype(jnp.bfloat16)
@@ -350,45 +328,51 @@
     wide = 0 if odd or width % (heads * VD) else heads * VD
     rows_a = queries.shape[0]
     slices = (key_rows, values, queries) if wide else ()
+    near = min(2, nz)
     sends = kernel(
-        functools.partial(prep_kernel, nz, nx, cap, width, wide),
-        (tokens, moe_gain.reshape(1, model), routes.T, *slices),
-        [struct((cap, width))] * ep_n
-        + [struct((3 * rows_a, wide))] * (nz if wide else 0),
-        in_specs=[HBM] * (3 + len(slices)),
+        functools.partial(prep_kernel, nz, nx, cap, width, near, wide),
+        (tokens, moe_gain.reshape(1, model), routes.T, route_scores.T, *slices),
+        [struct(((tp_n // 2 if j < near * nx else 1) * cap, width)) for j in range(ep_n)]
+        + [struct((3 * rows_a, wide))] * (nz if wide else 0)
+        + [struct((TOP, rows_b), jnp.int32), struct((TOP, rows_b), jnp.float32)],
+        in_specs=[HBM] * (4 + len(slices)),
         scratch=[
             pltpu.VMEM((rows_b, model), jnp.bfloat16),
             pltpu.VMEM((1, model), jnp.float32),
-            pltpu.VMEM((TOP, rows_b), jnp.int32),
-            pltpu.SemaphoreType.DMA((3 + 3 * nz,)),
+            pltpu.SemaphoreType.DMA((4 + 3 * nz,)),
         ],
     )
+    *sends, routes_v, scores_v = sends
     sends, packs = sends[:ep_n], sends[ep_n:]
     order = list(range(1, nx)) + [0]
     parts = {}
     for m in order:
         arrived = [shift(sends[k * nx + m], "ep", k * nx + m) for k in range(nz)]
-        parts[0, m] = jnp.concatenate(arrived, axis=0)
+        far = jnp.concatenate(arrived[near:], axis=0)
+        for q in range(0, tp_n, 2):
+            pieces = [block[q // 2 * cap : (q // 2 + 1) * cap] for block in arrived[:near]]
+            pieces.append(shift(far, "tp", q))
+            parts[q, m] = jnp.concatenate(pieces, axis=0)
+            if q:
+                parts[q + 1, m] = shift(parts[q, m], "tp", 1)
+    first = jnp.concatenate([parts[0, m] for m in order], axis=0)
+    second = shift(first, "tp", 1)
 
     packs = [shift(pack, "ep", k * nx) for k, pack in enumerate(packs)]
-
-    for q in range(0, tp_n, 2):
-        for m in order:
-            parts[q, m] = shift(parts[0, m], "tp", q)
-            parts[q + 1, m] = shift(parts[q, m], "tp", 1)
 
     attended = None
     if wide:
-        near = packs[0][: 2 * rows_a]
-        rest = jnp.concatenate([pack[: 2 * rows_a] for pack in packs[1:]], axis=0)
-        near = [shift(near, "ep", m) for m in range(1, nx)]
-        rest = [shift(rest, "ep", m) for m in range(1, nx)]
+        swaps = [[0], [nz // 2], [k for k in range(1, nz) if k != nz // 2]]
+        swapped = []
+        for group in swaps:
+            pairs = jnp.concatenate([packs[k][: 2 * rows_a] for k in group], axis=0)
+            swapped += [shift(pairs, "ep", m) for m in range(1, nx)]
         gain = kernel(fence_kernel, (head_gain.reshape(1, VD),), struct((1, VD), jnp.float32))
         outs = kernel(
-            functools.partial(attend_kernel, nz, nx, heads),
-            (lambdas, gain, *packs, *near, *rest),
+            functools.partial(attend_kernel, nz, nx, heads, swaps),
+            (lambdas, gain, *packs, *swapped),
             [struct((rows_a, wide))] * nz,
-            in_specs=[SMEM] + [VMEM] * (1 + nz + 2 * (nx - 1)),
+            in_specs=[SMEM] + [VMEM] * (1 + nz + len(swapped)),
             scratch=[
                 pltpu.VMEM((nz * rows_a, wide), jnp.bfloat16),
                 pltpu.VMEM((ep_n * rows_a, wide), jnp.bfloat16),
@@ -397,14 +381,15 @@
             ],
             mib=16,
         )
+        outs = [shift(outs[k], "ep", k * nx) for k in range(nz)]
     else:
         attended = gathered_attention(queries, key_rows, values, lambdas, head_gain)
 
     slots, span = ep_n * cap, nz * cap
     gate, up, down = w_gate[0], w_up[0], w_down[0]
     sums = kernel(
-        functools.partial(early_kernel, nx),
-        (*[parts[q, m] for q in range(2) for m in order], gate, up),
+        early_kernel,
+        (first, second, gate, up),
         [struct((span, units), jnp.float32)] * (2 * nx),
         mib=20,
     )
@@ -419,31 +404,31 @@
 
     returned = {}
     for m in order:
-        pieces = []
-        for q in list(range(2, tp_n, 2)) + [0]:
-            both = [results[m][q], shift(results[m][q + 1], "tp", 1)]
-            if q:
-                (piece,) = kernel(functools.partial(add_kernel, 2), both, [struct((span, width))])
-                pieces.append(shift(piece, "tp", q))
-            else:
-                pieces += both
-        if wide and m == 0:
+        other = [shift(results[m][q + 1], "tp", 1) for q in range(0, tp_n, 2)]
+        bounds = [0, nz] if m == 0 or near == nz else [0, near, nz]
+        sizes = [(b - a) * cap for a, b in zip(bounds, bounds[1:])]
+        crossed = {i: [] for i in range(len(sizes))}
+        for q in range(2, tp_n, 2):
+            pieces = kernel(
+                functools.partial(add_kernel, 2, 0),
+                (results[m][q], other[q // 2]),
+                [struct((size, width)) for size in sizes],
+            )
+            for i, piece in enumerate(pieces):
+                crossed[i].append(shift(piece, "tp", q))
+        for i, size in enumerate(sizes):
+            pieces = (*crossed[i], results[m][0], other[0])
             blocks = kernel(
-                functools.partial(blend_kernel, nz, cap, len(pieces)),
-                (*pieces, *outs[1:]),
-                [struct((cap, width))]
-                + [struct((rows_a + cap * width // wide, wide))] * (nz - 1),
+                functools.partial(add_kernel, len(pieces), bounds[i] * cap),
+                pieces,
+                [struct((cap, width))] * (size // cap),
             )
-        else:
-            blocks = kernel(
-                functools.partial(add_kernel, len(pieces)), pieces, [struct((cap, width))] * nz
-            )
-        for k in range(nz):
-            returned[k, m] = shift(blocks[k], "ep", k * nx + m)
+            for k, block in enumerate(blocks, bounds[i]):
+                returned[k, m] = shift(block, "ep", k * nx + m)
 
     high, low = kernel(
         functools.partial(gates_kernel, nz, nx, cap),
-        (routes.T, route_scores.T),
+        (routes_v, scores_v),
         [struct((slots, rows_b))] * 2,
         cost=pl.CostEstimate(flops=20_000_000_000, bytes_accessed=100_000, transcendentals=0),
     )
@@ -454,7 +439,7 @@
             high,
             low,
             *[returned[k, m] for k in range(nz) for m in range(nx)],
-            *(outs[:1] if wide else ()),
+            *(outs if wide else ()),
         ),
         shapes,
         out_specs=[HBM] * len(shapes),

time: 90.9 us -> 88.4 us (0.972)
  local copies, waits for them, and re-layouts: 9.58 us -> 4.51 us
  starting transfers between devices: 38 us -> 43 us
  waiting for transfers between devices: 31.7 us -> 29.4 us
    unnamed x26 -> x17, local copies, waits for them, and re-layouts: 9.53 us -> 4.45 us
    ppermute x31 -> x35, starting transfers between devices: 38 us -> 43 us  [shift(): return lax.ppermute(v, axis, [(i, i ^ mask) for i in range(n)])]
    ppermute x31 -> x35, waiting for transfers between devices: 31.7 us -> 29.4 us  [shift(): return lax.ppermute(v, axis, [(i, i ^ mask) for i in range(n)])]
    pallas_call x12 -> x13, Pallas kernels: 10.4 us -> 10.2 us  [kernel(): pl.pallas_call(body, out_shape=outs, in_specs=in_specs or [VMEM] * len(in...]
  transfers between devices with their start and end apart: 31 -> 35, of which waited for: 11 -> 10; matrix products, arithmetic and copies ran while one was open for 0% -> 0% of each run, Pallas kernels for 9% -> 8%
where the time goes in v3:
time: 88.4 us; the launch traced here: 88.2 us
  starting transfers between devices  43 us (49%)
  waiting for transfers between devices  29.4 us (33%)
  Pallas kernels  10.2 us (12%)
  local copies, waits for them, and re-layouts  4.51 us (5%)
  between operations  0.99 us (1%)
    ppermute x35, starting transfers between devices, shift(): return lax.ppermute(v, axis, [(i, i ^ mask) for i in range(n)])  43 us
    ppermute x35, waiting for transfers between devices, shift(): return lax.ppermute(v, axis, [(i, i ^ mask) for i in range(n)])  29.4 us
    pallas_call x13, Pallas kernels, kernel(): pl.pallas_call(body, out_shape=outs, in_specs=in_specs or [VMEM] * len(in...  10.2 us
    unnamed x17, local copies, waits for them, and re-layouts  4.45 us
  transfers between devices with their start and end apart: 35, of which 10 were waited for; matrix products, arithmetic and copies ran while one was open for 0% of the time, Pallas kernels for 8%

profile of v3, /device:TPU:0, one launch (start us, length us, event | category | flops | bytes accessed | tf_op | source)
XLA Modules:
  0.0 88.2 jit_solution(11855590533249325307)
XLA Ops:
  0.6 1.9 %shard_map.131 = (bf16[64,1024]{1,0:T(8,128)(2,1)S(1)}, bf16[64,1024]{1,0:T(8,128)(2,1)S(1)}, bf16[64,1024]{1,0:T(8,128)(2,1)S(1)}, bf16[64,1024]{1,0:T(8,128)(2...) custom-call(bf16[64,4096]{1,0:T(8,128)(2,1)} %tokens_ref.1, ...), custom_call_target="tpu_custom_call" | custom-call | tf_op jit(solution)/shard_map/pallas_call | solution.py:317
  2.6 4.1 %collective-permute-start.1 = (bf16[32,1024]{1,0:T(8,128)(2,1)S(1)}, bf16[32,1024]{1,0:T(8,128)(2,1)S(1)}, u32[]{:S(2)}, u32[]{:S(2)}) collective-permute-start(bf16[32,1024]{1,0:T(8,128)(2,1)S(1)} %get-tuple-element.52), channel_id=1, source_target_pairs={{0,16},{4,20},{8,24},{12,28},{16,0},{20,4},{24,8},{28,12},{1,17},{... | collective-permute-start | bytes 196616 | tf_op jit(solution)/shard_map/ppermute | solution.py:309
  6.7 1.3 %collective-permute-start.2 = (bf16[32,1024]{1,0:T(8,128)(2,1)S(1)}, bf16[32,1024]{1,0:T(8,128)(2,1)S(1)}, u32[]{:S(2)}, u32[]{:S(2)}) collective-permute-start(bf16[32,1024]{1,0:T(8,128)(2,1)S(1)} %get-tuple-element.53), channel_id=1, source_target_pairs={{0,24},{4,28},{8,16},{12,20},{16,8},{20,12},{24,0},{28,4},{1,25},{... | collective-permute-start | bytes 196616 | tf_op jit(solution)/shard_map/ppermute | solution.py:309
  8.0 1.5 %collective-permute-start.5 = (bf16[64,1024]{1,0:T(8,128)(2,1)S(1)}, bf16[64,1024]{1,0:T(8,128)(2,1)S(1)}, u32[]{:S(2)}, u32[]{:S(2)}) collective-permute-start(bf16[64,1024]{1,0:T(8,128)(2,1)S(1)} %get-tuple-element.54), channel_id=1, source_target_pairs={{0,4},{4,0},{8,12},{12,8},{16,20},{20,16},{24,28},{28,24},{1,5},{5... | collective-permute-start | bytes 393224 | tf_op jit(solution)/shard_map/ppermute | solution.py:309
  9.5 1.7 %collective-permute-start.7 = (bf16[32,1024]{1,0:T(8,128)(2,1)S(1)}, bf16[32,1024]{1,0:T(8,128)(2,1)S(1)}, u32[]{:S(2)}, u32[]{:S(2)}) collective-permute-start(bf16[32,1024]{1,0:T(8,128)(2,1)S(1)} %get-tuple-element.56), channel_id=1, source_target_pairs={{0,20},{4,16},{8,28},{12,24},{16,4},{20,0},{24,12},{28,8},{1,21},{... | collective-permute-start | bytes 196616 | tf_op jit(solution)/shard_map/ppermute | solution.py:309
  11.2 1.8 %collective-permute-start.8 = (bf16[32,1024]{1,0:T(8,128)(2,1)S(1)}, bf16[32,1024]{1,0:T(8,128)(2,1)S(1)}, u32[]{:S(2)}, u32[]{:S(2)}) collective-permute-start(bf16[32,1024]{1,0:T(8,128)(2,1)S(1)} %get-tuple-element.57), channel_id=1, source_target_pairs={{0,28},{4,24},{8,20},{12,16},{16,12},{20,8},{24,4},{28,0},{1,29},{... | collective-permute-start | bytes 196616 | tf_op jit(solution)/shard_map/ppermute | solution.py:309
  13.0 0.9 %collective-permute-start = (bf16[64,1024]{1,0:T(8,128)(2,1)S(1)}, bf16[64,1024]{1,0:T(8,128)(2,1)S(1)}, u32[]{:S(2)}, u32[]{:S(2)}) collective-permute-start(bf16[64,1024]{1,0:T(8,128)(2,1)S(1)} %get-tuple-element.51), channel_id=1, source_target_pairs={{0,8},{4,12},{8,0},{12,4},{16,24},{20,28},{24,16},{28,20},{1,9},{5... | collective-permute-start | bytes 393224 | tf_op jit(solution)/shard_map/ppermute | solution.py:309
  13.9 0.0 collective-permute-done.2
  13.9 3.8 %collective-permute-start.6 = (bf16[64,1024]{1,0:T(8,128)(2,1)S(1)}, bf16[64,1024]{1,0:T(8,128)(2,1)S(1)}, u32[]{:S(2)}, u32[]{:S(2)}) collective-permute-start(bf16[64,1024]{1,0:T(8,128)(2,1)S(1)} %get-tuple-element.55), channel_id=1, source_target_pairs={{0,12},{4,8},{8,4},{12,0},{16,28},{20,24},{24,20},{28,16},{1,13},{... | collective-permute-start | bytes 393224 | tf_op jit(solution)/shard_map/ppermute | solution.py:309
  17.7 1.6 %collective-permute-start.3 = (bf16[64,1024]{1,0:T(8,128)(2,1)S(1)}, bf16[64,1024]{1,0:T(8,128)(2,1)S(1)}, u32[]{:S(2)}, u32[]{:S(2)}) collective-permute-start(bf16[64,1024]{1,0:T(8,128)(2,1)S(1)} %pad_maximum_fusion.3), channel_id=1, source_target_pairs={{0,2},{1,3},{2,0},{3,1},{4,6},{5,7},{6,4},{7,5},{8,10},{9,11},{10,... | collective-permute-start | bytes 393224 | tf_op jit(solution)/shard_map/ppermute | solution.py:309
  19.3 3.5 %collective-permute-done.6 = bf16[64,1024]{1,0:T(8,128)(2,1)S(1)} collective-permute-done((bf16[64,1024]{1,0:T(8,128)(2,1)S(1)}, bf16[64,1024]{1,0:T(8,128)(2,1)S(1)}, u32[]{:S(2)}, u32[]{:S(2)}) %collective-permute-start.6) | collective-permute-done | bytes 131104 | tf_op jit(solution)/shard_map/ppermute | solution.py:309
  22.8 0.0 collective-permute-done.7
  22.8 0.0 collective-permute-done.8
  22.9 0.0 collective-permute-done
  22.9 0.1 collective-permute-start.9
  23.0 1.6 %collective-permute-start.13 = (bf16[64,1024]{1,0:T(8,128)(2,1)S(1)}, bf16[64,1024]{1,0:T(8,128)(2,1)S(1)}, u32[]{:S(2)}, u32[]{:S(2)}) collective-permute-start(bf16[64,1024]{1,0:T(8,128)(2,1)S(1)} %pad_maximum_fusion.4), channel_id=1, source_target_pairs={{0,2},{1,3},{2,0},{3,1},{4,6},{5,7},{6,4},{7,5},{8,10},{9,11},{10,... | collective-permute-start | bytes 393224 | tf_op jit(solution)/shard_map/ppermute | solution.py:309
  24.6 0.0 collective-permute-done.3
  24.7 0.3 collective-permute-start.4
  24.9 4.1 %collective-permute-done.13 = bf16[64,1024]{1,0:T(8,128)(2,1)S(1)} collective-permute-done((bf16[64,1024]{1,0:T(8,128)(2,1)S(1)}, bf16[64,1024]{1,0:T(8,128)(2,1)S(1)}, u32[]{:S(2)}, u32[]{:S(2)}) %collective-permute-start.13) | collective-permute-done | bytes 131104 | tf_op jit(solution)/shard_map/ppermute | solution.py:309
  29.0 0.1 collective-permute-start.14
  29.1 0.1 collective-permute-start.26
  29.2 4.0 %collective-permute-start.28 = (bf16[384,256]{1,0:T(8,128)(2,1)S(1)}, bf16[384,256]{1,0:T(8,128)(2,1)S(1)}, u32[]{:S(2)}, u32[]{:S(2)}) collective-permute-start(bf16[384,256]{1,0:T(8,128)(2,1)S(1)} %get-tuple-element.83), channel_id=1, source_target_pairs={{0,24},{4,28},{8,16},{12,20},{16,8},{20,12},{24,0},{28,4},{1,25},{... | collective-permute-start | bytes 589832 | tf_op jit(solution)/shard_map/ppermute | solution.py:309
  33.2 2.2 %copy-done.1 = bf16[1,4096,512]{2,1,0:T(8,128)(2,1)S(1)} copy-done((bf16[1,4096,512]{2,1,0:T(8,128)(2,1)S(1)}, bf16[1,4096,512]{2,1,0:T(8,128)(2,1)}, u32[]{:S(2)}) %copy-start.1) | copy-done | bytes 4194328
  35.4 1.2 %shard_map.133 = (f32[128,512]{1,0:T(8,128)S(1)}, f32[128,512]{1,0:T(8,128)S(1)}, f32[128,512]{1,0:T(8,128)S(1)}, f32[128,512]{1,0:T(8,128)S(1)}) custom-call(bf16[256,1024]{1,0:T(8,128)(2,1)S(1)} %constant_dynamic-update-slice_fusion.first_ref, bf16[256,1024]{1,0:T(8,128)(2,1)S(1)} %collective-permute-done.9.second_ref, bf16[4096,512]{1,0:T(8,128)(2,1)S(1)} %bitcast.7, ...), custom_call_target="tpu_custom_call" | custom-call | tf_op jit(solution)/shard_map/pallas_call | solution.py:317
  36.6 0.0 collective-permute-done.4.refs_1_
  36.6 0.9 %copy-done.2 = bf16[1,4096,512]{2,1,0:T(8,128)(2,1)S(1)} copy-done((bf16[1,4096,512]{2,1,0:T(8,128)(2,1)S(1)}, bf16[1,4096,512]{2,1,0:T(8,128)(2,1)}, u32[]{:S(2)}) %copy-start.2) | copy-done | bytes 4194328
  37.5 1.3 %copy-done.3 = bf16[1,512,4096]{2,1,0:T(8,128)(2,1)S(1)} copy-done((bf16[1,512,4096]{2,1,0:T(8,128)(2,1)S(1)}, bf16[1,512,4096]{2,1,0:T(8,128)(2,1)}, u32[]{:S(2)}) %copy-start.3) | copy-done | bytes 4194328
  38.8 1.4 %shard_map.134 = (bf16[128,1024]{1,0:T(8,128)(2,1)S(1)}, bf16[128,1024]{1,0:T(8,128)(2,1)S(1)}, bf16[128,1024]{1,0:T(8,128)(2,1)S(1)}, bf16[128,1024]{1,0:T(8,128)(2,1)S(1)}) custom-call(bf16[128,1024]{1,0:T(8,128)(2,1)S(1)} %pad_maximum_fusion.refs_0_, bf16[128,1024]{1,0:T(8,128)(2,1)S(1)} %collective-permute-done.4.refs_1_, ...), custom_call_target="tpu_custom_call" | custom-call | tf_op jit(solution)/shard_map/pallas_call | solution.py:317
  40.2 0.1 collective-permute-start.10
  40.4 0.0 collective-permute-done.14.refs_1_
  40.4 1.4 %shard_map.137 = (bf16[128,1024]{1,0:T(8,128)(2,1)S(1)}, bf16[128,1024]{1,0:T(8,128)(2,1)S(1)}, bf16[128,1024]{1,0:T(8,128)(2,1)S(1)}, bf16[128,1024]{1,0:T(8,128)(2,1)S(1)}) custom-call(bf16[128,1024]{1,0:T(8,128)(2,1)S(1)} %pad_maximum_fusion.1.refs_0_, bf16[128,1024]{1,0:T(8,128)(2,1)S(1)} %collective-permute-done.14.refs_1_, ...), custom_call_target="tpu_custom_call" | custom-call | tf_op jit(solution)/shard_map/pallas_call | solution.py:317
  41.8 0.5 collective-permute-start.15
  42.3 0.9 %collective-permute-start.29 = (bf16[256,256]{1,0:T(8,128)(2,1)S(1)}, bf16[256,256]{1,0:T(8,128)(2,1)S(1)}, u32[]{:S(2)}, u32[]{:S(2)}) collective-permute-start(bf16[256,256]{1,0:T(8,128)(2,1)S(1)} %slice.44), channel_id=1, source_target_pairs={{0,4},{4,0},{8,12},{12,8},{16,20},{20,16},{24,28},{28,24},{1,5},{5... | collective-permute-start | bytes 393224 | tf_op jit(solution)/shard_map/ppermute | solution.py:309
  43.2 0.3 collective-permute-start.27
  43.5 1.4 %collective-permute-start.31 = (bf16[512,256]{1,0:T(8,128)(2,1)S(1)}, bf16[512,256]{1,0:T(8,128)(2,1)S(1)}, u32[]{:S(2)}, u32[]{:S(2)}) collective-permute-start(bf16[512,256]{1,0:T(8,128)(2,1)S(1)} %pad_maximum_fusion.2), channel_id=1, source_target_pairs={{0,4},{4,0},{8,12},{12,8},{16,20},{20,16},{24,28},{28,24},{1,5},{5... | collective-permute-start | bytes 786440 | tf_op jit(solution)/shard_map/ppermute | solution.py:309
  45.0 9.9 %collective-permute-done.27.refs_2_ = bf16[384,256]{1,0:T(8,128)(2,1)S(1)} collective-permute-done((bf16[384,256]{1,0:T(8,128)(2,1)S(1)}, bf16[384,256]{1,0:T(8,128)(2,1)S(1)}, u32[]{:S(2)}, u32[]{:S(2)}) %collective-permute-start.27) | collective-permute-done | bytes 196640 | tf_op jit(solution)/shard_map/ppermute | solution.py:309
  54.9 0.1 collective-permute-start.17
  55.0 1.2 %collective-permute-start.30 = (bf16[256,256]{1,0:T(8,128)(2,1)S(1)}, bf16[256,256]{1,0:T(8,128)(2,1)S(1)}, u32[]{:S(2)}, u32[]{:S(2)}) collective-permute-start(bf16[256,256]{1,0:T(8,128)(2,1)S(1)} %slice.54), channel_id=1, source_target_pairs={{0,4},{4,0},{8,12},{12,8},{16,20},{20,16},{24,28},{28,24},{1,5},{5... | collective-permute-start | bytes 393224 | tf_op jit(solution)/shard_map/ppermute | solution.py:309
  56.2 0.1 collective-permute-start.12
  56.4 0.1 shard_map.135
  56.5 1.6 %collective-permute-start.11 = (bf16[128,1024]{1,0:T(8,128)(2,1)S(1)}, bf16[128,1024]{1,0:T(8,128)(2,1)S(1)}, u32[]{:S(2)}, u32[]{:S(2)}) collective-permute-start(bf16[128,1024]{1,0:T(8,128)(2,1)S(1)} %shard_map.135), channel_id=1, source_target_pairs={{0,2},{1,3},{2,0},{3,1},{4,6},{5,7},{6,4},{7,5},{8,10},{9,11},{10,... | collective-permute-start | bytes 786440 | tf_op jit(solution)/shard_map/ppermute | solution.py:309
  58.1 0.1 shard_map.138
  58.1 2.8 %collective-permute-done.30.refs_5_ = bf16[256,256]{1,0:T(8,128)(2,1)S(1)} collective-permute-done((bf16[256,256]{1,0:T(8,128)(2,1)S(1)}, bf16[256,256]{1,0:T(8,128)(2,1)S(1)}, u32[]{:S(2)}, u32[]{:S(2)}) %collective-permute-start.30) | collective-permute-done | bytes 131104 | tf_op jit(solution)/shard_map/ppermute | solution.py:309
  60.9 1.5 %collective-permute-start.22 = (bf16[64,1024]{1,0:T(8,128)(2,1)S(1)}, bf16[64,1024]{1,0:T(8,128)(2,1)S(1)}, u32[]{:S(2)}, u32[]{:S(2)}) collective-permute-start(bf16[64,1024]{1,0:T(8,128)(2,1)S(1)} %get-tuple-element.76), channel_id=1, source_target_pairs={{0,2},{1,3},{2,0},{3,1},{4,6},{5,7},{6,4},{7,5},{8,10},{9,11},{10,... | collective-permute-start | bytes 393224 | tf_op jit(solution)/shard_map/ppermute | solution.py:309
  62.4 0.5 collective-permute-start.16
  62.9 2.7 %shard_map.142 = (bf16[128,256]{1,0:T(8,128)(2,1)S(1)}, bf16[128,256]{1,0:T(8,128)(2,1)S(1)}, bf16[128,256]{1,0:T(8,128)(2,1)S(1)}, bf16[128,256]{1,0:T(8,128)(2,1)S(1)}) custom-call(f32[4]{0:T(128)S(1)} %copy-done.5, f32[1,256]{1,0:T(1,128)S(1)} %shard_map.141.gain_ref, bf16[384,256]{1,0:T(8,128)(2,1)S(1)} %get-tuple-element.80.refs_0_, ...), custom_call_target="tpu_custom_call" | custom-call | tf_op jit(solution)/shard_map/pallas_call | solution.py:317
  65.7 0.1 collective-permute-start.32
  65.8 2.7 %collective-permute-done.22.refs_0_ = bf16[64,1024]{1,0:T(8,128)(2,1)S(1)} collective-permute-done((bf16[64,1024]{1,0:T(8,128)(2,1)S(1)}, bf16[64,1024]{1,0:T(8,128)(2,1)S(1)}, u32[]{:S(2)}, u32[]{:S(2)}) %collective-permute-start.22) | collective-permute-done | bytes 131104 | tf_op jit(solution)/shard_map/ppermute | solution.py:309
  68.5 0.1 shard_map.140
  68.6 1.7 %collective-permute-start.34 = (bf16[128,256]{1,0:T(8,128)(2,1)S(1)}, bf16[128,256]{1,0:T(8,128)(2,1)S(1)}, u32[]{:S(2)}, u32[]{:S(2)}) collective-permute-start(bf16[128,256]{1,0:T(8,128)(2,1)S(1)} %get-tuple-element.87), channel_id=1, source_target_pairs={{0,24},{4,28},{8,16},{12,20},{16,8},{20,12},{24,0},{28,4},{1,25},{... | collective-permute-start | bytes 196616 | tf_op jit(solution)/shard_map/ppermute | solution.py:309
  70.3 0.4 collective-permute-done.16.refs_0_
  70.7 1.4 %collective-permute-start.23 = (bf16[32,1024]{1,0:T(8,128)(2,1)S(1)}, bf16[32,1024]{1,0:T(8,128)(2,1)S(1)}, u32[]{:S(2)}, u32[]{:S(2)}) collective-permute-start(bf16[32,1024]{1,0:T(8,128)(2,1)S(1)} %get-tuple-element.77), channel_id=1, source_target_pairs={{0,20},{4,16},{8,28},{12,24},{16,4},{20,0},{24,12},{28,8},{1,21},{... | collective-permute-start | bytes 196616 | tf_op jit(solution)/shard_map/ppermute | solution.py:309
  72.1 3.3 %collective-permute-start.25 = (bf16[32,1024]{1,0:T(8,128)(2,1)S(1)}, bf16[32,1024]{1,0:T(8,128)(2,1)S(1)}, u32[]{:S(2)}, u32[]{:S(2)}) collective-permute-start(bf16[32,1024]{1,0:T(8,128)(2,1)S(1)} %get-tuple-element.79), channel_id=1, source_target_pairs={{0,28},{4,24},{8,20},{12,16},{16,12},{20,8},{24,4},{28,0},{1,29},{... | collective-permute-start | bytes 196616 | tf_op jit(solution)/shard_map/ppermute | solution.py:309
  75.4 0.1 shard_map.139
  75.5 0.1 shard_map.136
  75.6 0.9 %collective-permute-start.18 = (bf16[32,1024]{1,0:T(8,128)(2,1)S(1)}, bf16[32,1024]{1,0:T(8,128)(2,1)S(1)}, u32[]{:S(2)}, u32[]{:S(2)}) collective-permute-start(bf16[32,1024]{1,0:T(8,128)(2,1)S(1)} %get-tuple-element.72), channel_id=1, source_target_pairs={{0,4},{4,0},{8,12},{12,8},{16,20},{20,16},{24,28},{28,24},{1,5},{5... | collective-permute-start | bytes 196616 | tf_op jit(solution)/shard_map/ppermute | solution.py:309
  76.5 0.9 %collective-permute-done.33.refs_10_ = bf16[128,256]{1,0:T(8,128)(2,1)S(1)} collective-permute-done((bf16[128,256]{1,0:T(8,128)(2,1)S(1)}, bf16[128,256]{1,0:T(8,128)(2,1)S(1)}, u32[]{:S(2)}, u32[]{:S(2)}) %collective-permute-start.33) | collective-permute-done | bytes 65568 | tf_op jit(solution)/shard_map/ppermute | solution.py:309
  77.4 2.6 %collective-permute-start.19 = (bf16[32,1024]{1,0:T(8,128)(2,1)S(1)}, bf16[32,1024]{1,0:T(8,128)(2,1)S(1)}, u32[]{:S(2)}, u32[]{:S(2)}) collective-permute-start(bf16[32,1024]{1,0:T(8,128)(2,1)S(1)} %get-tuple-element.73), channel_id=1, source_target_pairs={{0,8},{4,12},{8,0},{12,4},{16,24},{20,28},{24,16},{28,20},{1,9},{5... | collective-permute-start | bytes 196616 | tf_op jit(solution)/shard_map/ppermute | solution.py:309
  80.1 1.0 %collective-permute-done.23.refs_5_ = bf16[32,1024]{1,0:T(8,128)(2,1)S(1)} collective-permute-done((bf16[32,1024]{1,0:T(8,128)(2,1)S(1)}, bf16[32,1024]{1,0:T(8,128)(2,1)S(1)}, u32[]{:S(2)}, u32[]{:S(2)}) %collective-permute-start.23) | collective-permute-done | bytes 65568 | tf_op jit(solution)/shard_map/ppermute | solution.py:309
  81.0 1.8 %collective-permute-start.24 = (bf16[32,1024]{1,0:T(8,128)(2,1)S(1)}, bf16[32,1024]{1,0:T(8,128)(2,1)S(1)}, u32[]{:S(2)}, u32[]{:S(2)}) collective-permute-start(bf16[32,1024]{1,0:T(8,128)(2,1)S(1)} %get-tuple-element.78), channel_id=1, source_target_pairs={{0,24},{4,28},{8,16},{12,20},{16,8},{20,12},{24,0},{28,4},{1,25},{... | collective-permute-start | bytes 196616 | tf_op jit(solution)/shard_map/ppermute | solution.py:309
  82.9 0.2 shard_map.132
  83.1 3.3 %collective-permute-done.21.refs_4_ = bf16[32,1024]{1,0:T(8,128)(2,1)S(1)} collective-permute-done((bf16[32,1024]{1,0:T(8,128)(2,1)S(1)}, bf16[32,1024]{1,0:T(8,128)(2,1)S(1)}, u32[]{:S(2)}, u32[]{:S(2)}) %collective-permute-start.21) | collective-permute-done | bytes 65568 | tf_op jit(solution)/shard_map/ppermute | solution.py:309
  86.4 0.8 collective-permute-done.24.refs_6_
  87.2 1.0 %shard_map.143 = (bf16[64,1024]{1,0:T(8,128)(2,1)}, bf16[128,1024]{1,0:T(8,128)(2,1)}) custom-call(bf16[256,64]{1,0:T(8,128)(2,1)S(1)} %get-tuple-element.48.high_ref, bf16[256,64]{1,0:T(8,128)(2,1)S(1)} %get-tuple-element.49.low_ref, bf16[32,1024]{1,0:T(8,128)(2,1)S(1)} %get-tuple-element.64.refs_0_, bf16[32,1024]{1,0:T(8,128)(2,1)S(1)} %collective-permute-done.18.refs_1_, ...), custom_call_target="tpu_custom_call" | custom-call | tf_op jit(solution)/shard_map/pallas_call | solution.py:317
  (48 shorter events, 0.3 us)
Async XLA Ops:
  0.6 32.5 %copy-start = (bf16[1,4096,512]{2,1,0:T(8,128)(2,1)S(1)}, bf16[1,4096,512]{2,1,0:T(8,128)(2,1)}, u32[]{:S(2)}) copy-start(bf16[1,4096,512]{2,1,0:T(8,128)(2,1)} %param.21) | copy-start | bytes 12582916
  2.6 10.5 %collective-permute-start.1 = (bf16[32,1024]{1,0:T(8,128)(2,1)S(1)}, bf16[32,1024]{1,0:T(8,128)(2,1)S(1)}, u32[]{:S(2)}, u32[]{:S(2)}) collective-permute-start(bf16[32,1024]{1,0:T(8,128)(2,1)S(1)} %get-tuple-element.52), channel_id=1, source_target_pairs={{0,16},{4,20},{8,24},{12,28},{16,0},{20,4},{24,8},{28,12},{1,17},{... | collective-permute-start | bytes 196616 | tf_op jit(solution)/shard_map/ppermute | solution.py:309
  6.7 7.2 %collective-permute-start.2 = (bf16[32,1024]{1,0:T(8,128)(2,1)S(1)}, bf16[32,1024]{1,0:T(8,128)(2,1)S(1)}, u32[]{:S(2)}, u32[]{:S(2)}) collective-permute-start(bf16[32,1024]{1,0:T(8,128)(2,1)S(1)} %get-tuple-element.53), channel_id=1, source_target_pairs={{0,24},{4,28},{8,16},{12,20},{16,8},{20,12},{24,0},{28,4},{1,25},{... | collective-permute-start | bytes 196616 | tf_op jit(solution)/shard_map/ppermute | solution.py:309
  8.0 9.7 %collective-permute-start.5 = (bf16[64,1024]{1,0:T(8,128)(2,1)S(1)}, bf16[64,1024]{1,0:T(8,128)(2,1)S(1)}, u32[]{:S(2)}, u32[]{:S(2)}) collective-permute-start(bf16[64,1024]{1,0:T(8,128)(2,1)S(1)} %get-tuple-element.54), channel_id=1, source_target_pairs={{0,4},{4,0},{8,12},{12,8},{16,20},{20,16},{24,28},{28,24},{1,5},{5... | collective-permute-start | bytes 393224 | tf_op jit(solution)/shard_map/ppermute | solution.py:309
  9.5 13.3 %collective-permute-start.7 = (bf16[32,1024]{1,0:T(8,128)(2,1)S(1)}, bf16[32,1024]{1,0:T(8,128)(2,1)S(1)}, u32[]{:S(2)}, u32[]{:S(2)}) collective-permute-start(bf16[32,1024]{1,0:T(8,128)(2,1)S(1)} %get-tuple-element.56), channel_id=1, source_target_pairs={{0,20},{4,16},{8,28},{12,24},{16,4},{20,0},{24,12},{28,8},{1,21},{... | collective-permute-start | bytes 196616 | tf_op jit(solution)/shard_map/ppermute | solution.py:309
  11.2 11.6 %collective-permute-start.8 = (bf16[32,1024]{1,0:T(8,128)(2,1)S(1)}, bf16[32,1024]{1,0:T(8,128)(2,1)S(1)}, u32[]{:S(2)}, u32[]{:S(2)}) collective-permute-start(bf16[32,1024]{1,0:T(8,128)(2,1)S(1)} %get-tuple-element.57), channel_id=1, source_target_pairs={{0,28},{4,24},{8,20},{12,16},{16,12},{20,8},{24,4},{28,0},{1,29},{... | collective-permute-start | bytes 196616 | tf_op jit(solution)/shard_map/ppermute | solution.py:309
  13.0 9.9 %collective-permute-start = (bf16[64,1024]{1,0:T(8,128)(2,1)S(1)}, bf16[64,1024]{1,0:T(8,128)(2,1)S(1)}, u32[]{:S(2)}, u32[]{:S(2)}) collective-permute-start(bf16[64,1024]{1,0:T(8,128)(2,1)S(1)} %get-tuple-element.51), channel_id=1, source_target_pairs={{0,8},{4,12},{8,0},{12,4},{16,24},{20,28},{24,16},{28,20},{1,9},{5... | collective-permute-start | bytes 393224 | tf_op jit(solution)/shard_map/ppermute | solution.py:309
  13.9 8.9 %collective-permute-start.6 = (bf16[64,1024]{1,0:T(8,128)(2,1)S(1)}, bf16[64,1024]{1,0:T(8,128)(2,1)S(1)}, u32[]{:S(2)}, u32[]{:S(2)}) collective-permute-start(bf16[64,1024]{1,0:T(8,128)(2,1)S(1)} %get-tuple-element.55), channel_id=1, source_target_pairs={{0,12},{4,8},{8,4},{12,0},{16,28},{20,24},{24,20},{28,16},{1,13},{... | collective-permute-start | bytes 393224 | tf_op jit(solution)/shard_map/ppermute | solution.py:309
  17.7 6.9 %collective-permute-start.3 = (bf16[64,1024]{1,0:T(8,128)(2,1)S(1)}, bf16[64,1024]{1,0:T(8,128)(2,1)S(1)}, u32[]{:S(2)}, u32[]{:S(2)}) collective-permute-start(bf16[64,1024]{1,0:T(8,128)(2,1)S(1)} %pad_maximum_fusion.3), channel_id=1, source_target_pairs={{0,2},{1,3},{2,0},{3,1},{4,6},{5,7},{6,4},{7,5},{8,10},{9,11},{10,... | collective-permute-start | bytes 393224 | tf_op jit(solution)/shard_map/ppermute | solution.py:309
  22.9 10.2 %collective-permute-start.9 = (bf16[256,1024]{1,0:T(8,128)(2,1)S(1)}, bf16[256,1024]{1,0:T(8,128)(2,1)S(1)}, u32[]{:S(2)}, u32[]{:S(2)}) collective-permute-start(bf16[256,1024]{1,0:T(8,128)(2,1)S(1)} %constant_dynamic-update-slice_fusion.first_ref), channel_id=1, source_target_pairs={{0,1},{1,0},{2,3},{3,2},{4,5},{5,4},{6,7},{7,6},{8,9},{9,8},{10,11... | collective-permute-start | bytes 1572872 | tf_op jit(solution)/shard_map/ppermute | solution.py:309
  23.0 6.0 %collective-permute-start.13 = (bf16[64,1024]{1,0:T(8,128)(2,1)S(1)}, bf16[64,1024]{1,0:T(8,128)(2,1)S(1)}, u32[]{:S(2)}, u32[]{:S(2)}) collective-permute-start(bf16[64,1024]{1,0:T(8,128)(2,1)S(1)} %pad_maximum_fusion.4), channel_id=1, source_target_pairs={{0,2},{1,3},{2,0},{3,1},{4,6},{5,7},{6,4},{7,5},{8,10},{9,11},{10,... | collective-permute-start | bytes 393224 | tf_op jit(solution)/shard_map/ppermute | solution.py:309
  24.7 11.9 %collective-permute-start.4 = (bf16[128,1024]{1,0:T(8,128)(2,1)S(1)}, bf16[128,1024]{1,0:T(8,128)(2,1)S(1)}, u32[]{:S(2)}, u32[]{:S(2)}) collective-permute-start(bf16[128,1024]{1,0:T(8,128)(2,1)S(1)} %pad_maximum_fusion.refs_0_), channel_id=1, source_target_pairs={{0,1},{1,0},{2,3},{3,2},{4,5},{5,4},{6,7},{7,6},{8,9},{9,8},{10,11... | collective-permute-start | bytes 786440 | tf_op jit(solution)/shard_map/ppermute | solution.py:309
  29.0 11.3 %collective-permute-start.14 = (bf16[128,1024]{1,0:T(8,128)(2,1)S(1)}, bf16[128,1024]{1,0:T(8,128)(2,1)S(1)}, u32[]{:S(2)}, u32[]{:S(2)}) collective-permute-start(bf16[128,1024]{1,0:T(8,128)(2,1)S(1)} %pad_maximum_fusion.1.refs_0_), channel_id=1, source_target_pairs={{0,1},{1,0},{2,3},{3,2},{4,5},{5,4},{6,7},{7,6},{8,9},{9,8},{10,11... | collective-permute-start | bytes 786440 | tf_op jit(solution)/shard_map/ppermute | solution.py:309
  29.1 14.1 %collective-permute-start.26 = (bf16[384,256]{1,0:T(8,128)(2,1)S(1)}, bf16[384,256]{1,0:T(8,128)(2,1)S(1)}, u32[]{:S(2)}, u32[]{:S(2)}) collective-permute-start(bf16[384,256]{1,0:T(8,128)(2,1)S(1)} %get-tuple-element.81), channel_id=1, source_target_pairs={{0,8},{4,12},{8,0},{12,4},{16,24},{20,28},{24,16},{28,20},{1,9},{5... | collective-permute-start | bytes 589832 | tf_op jit(solution)/shard_map/ppermute | solution.py:309
  29.2 14.3 %collective-permute-start.28 = (bf16[384,256]{1,0:T(8,128)(2,1)S(1)}, bf16[384,256]{1,0:T(8,128)(2,1)S(1)}, u32[]{:S(2)}, u32[]{:S(2)}) collective-permute-start(bf16[384,256]{1,0:T(8,128)(2,1)S(1)} %get-tuple-element.83), channel_id=1, source_target_pairs={{0,24},{4,28},{8,16},{12,20},{16,8},{20,12},{24,0},{28,4},{1,25},{... | collective-permute-start | bytes 589832 | tf_op jit(solution)/shard_map/ppermute | solution.py:309
  33.2 2.2 %copy-start.1 = (bf16[1,4096,512]{2,1,0:T(8,128)(2,1)S(1)}, bf16[1,4096,512]{2,1,0:T(8,128)(2,1)}, u32[]{:S(2)}) copy-start(bf16[1,4096,512]{2,1,0:T(8,128)(2,1)} %param.22) | copy-start | bytes 12582916
  35.4 2.2 %copy-start.2 = (bf16[1,4096,512]{2,1,0:T(8,128)(2,1)S(1)}, bf16[1,4096,512]{2,1,0:T(8,128)(2,1)}, u32[]{:S(2)}) copy-start(bf16[1,4096,512]{2,1,0:T(8,128)(2,1)} %param.22) | copy-start | bytes 12582916
  35.4 3.5 %copy-start.3 = (bf16[1,512,4096]{2,1,0:T(8,128)(2,1)S(1)}, bf16[1,512,4096]{2,1,0:T(8,128)(2,1)}, u32[]{:S(2)}) copy-start(bf16[1,512,4096]{2,1,0:T(8,128)(2,1)} %param.23) | copy-start | bytes 12582916
  40.2 16.0 %collective-permute-start.10 = (bf16[128,1024]{1,0:T(8,128)(2,1)S(1)}, bf16[128,1024]{1,0:T(8,128)(2,1)S(1)}, u32[]{:S(2)}, u32[]{:S(2)}) collective-permute-start(bf16[128,1024]{1,0:T(8,128)(2,1)S(1)} %get-tuple-element.61), channel_id=1, source_target_pairs={{0,1},{1,0},{2,3},{3,2},{4,5},{5,4},{6,7},{7,6},{8,9},{9,8},{10,11... | collective-permute-start | bytes 786440 | tf_op jit(solution)/shard_map/ppermute | solution.py:309
  40.4 22.6 %copy-start.4 = (f32[256]{0:T(256)S(1)}, f32[256]{0:T(256)}, u32[]{:S(2)}) copy-start(f32[256]{0:T(256)} %param.16) | copy-start | bytes 3076
  40.4 22.6 %copy-start.5 = (f32[4]{0:T(128)S(1)}, f32[4]{0:T(128)}, u32[]{:S(2)}) copy-start(f32[4]{0:T(128)} %lambda_ref.1) | copy-start | bytes 52
  41.8 14.7 %collective-permute-start.15 = (bf16[128,1024]{1,0:T(8,128)(2,1)S(1)}, bf16[128,1024]{1,0:T(8,128)(2,1)S(1)}, u32[]{:S(2)}, u32[]{:S(2)}) collective-permute-start(bf16[128,1024]{1,0:T(8,128)(2,1)S(1)} %get-tuple-element.68), channel_id=1, source_target_pairs={{0,1},{1,0},{2,3},{3,2},{4,5},{5,4},{6,7},{7,6},{8,9},{9,8},{10,11... | collective-permute-start | bytes 786440 | tf_op jit(solution)/shard_map/ppermute | solution.py:309
  42.3 12.7 %collective-permute-start.29 = (bf16[256,256]{1,0:T(8,128)(2,1)S(1)}, bf16[256,256]{1,0:T(8,128)(2,1)S(1)}, u32[]{:S(2)}, u32[]{:S(2)}) collective-permute-start(bf16[256,256]{1,0:T(8,128)(2,1)S(1)} %slice.44), channel_id=1, source_target_pairs={{0,4},{4,0},{8,12},{12,8},{16,20},{20,16},{24,28},{28,24},{1,5},{5... | collective-permute-start | bytes 393224 | tf_op jit(solution)/shard_map/ppermute | solution.py:309
  43.2 11.7 %collective-permute-start.27 = (bf16[384,256]{1,0:T(8,128)(2,1)S(1)}, bf16[384,256]{1,0:T(8,128)(2,1)S(1)}, u32[]{:S(2)}, u32[]{:S(2)}) collective-permute-start(bf16[384,256]{1,0:T(8,128)(2,1)S(1)} %get-tuple-element.82), channel_id=1, source_target_pairs={{0,16},{4,20},{8,24},{12,28},{16,0},{20,4},{24,8},{28,12},{1,17},{... | collective-permute-start | bytes 589832 | tf_op jit(solution)/shard_map/ppermute | solution.py:309
  43.5 18.9 %collective-permute-start.31 = (bf16[512,256]{1,0:T(8,128)(2,1)S(1)}, bf16[512,256]{1,0:T(8,128)(2,1)S(1)}, u32[]{:S(2)}, u32[]{:S(2)}) collective-permute-start(bf16[512,256]{1,0:T(8,128)(2,1)S(1)} %pad_maximum_fusion.2), channel_id=1, source_target_pairs={{0,4},{4,0},{8,12},{12,8},{16,20},{20,16},{24,28},{28,24},{1,5},{5... | collective-permute-start | bytes 786440 | tf_op jit(solution)/shard_map/ppermute | solution.py:309
  54.9 10.8 %collective-permute-start.17 = (bf16[128,1024]{1,0:T(8,128)(2,1)S(1)}, bf16[128,1024]{1,0:T(8,128)(2,1)S(1)}, u32[]{:S(2)}, u32[]{:S(2)}) collective-permute-start(bf16[128,1024]{1,0:T(8,128)(2,1)S(1)} %get-tuple-element.71), channel_id=1, source_target_pairs={{0,1},{1,0},{2,3},{3,2},{4,5},{5,4},{6,7},{7,6},{8,9},{9,8},{10,11... | collective-permute-start | bytes 786440 | tf_op jit(solution)/shard_map/ppermute | solution.py:309
  55.0 5.9 %collective-permute-start.30 = (bf16[256,256]{1,0:T(8,128)(2,1)S(1)}, bf16[256,256]{1,0:T(8,128)(2,1)S(1)}, u32[]{:S(2)}, u32[]{:S(2)}) collective-permute-start(bf16[256,256]{1,0:T(8,128)(2,1)S(1)} %slice.54), channel_id=1, source_target_pairs={{0,4},{4,0},{8,12},{12,8},{16,20},{20,16},{24,28},{28,24},{1,5},{5... | collective-permute-start | bytes 393224 | tf_op jit(solution)/shard_map/ppermute | solution.py:309
  56.2 12.3 %collective-permute-start.12 = (bf16[128,1024]{1,0:T(8,128)(2,1)S(1)}, bf16[128,1024]{1,0:T(8,128)(2,1)S(1)}, u32[]{:S(2)}, u32[]{:S(2)}) collective-permute-start(bf16[128,1024]{1,0:T(8,128)(2,1)S(1)} %get-tuple-element.63), channel_id=1, source_target_pairs={{0,1},{1,0},{2,3},{3,2},{4,5},{5,4},{6,7},{7,6},{8,9},{9,8},{10,11... | collective-permute-start | bytes 786440 | tf_op jit(solution)/shard_map/ppermute | solution.py:309
  56.5 15.6 %collective-permute-start.11 = (bf16[128,1024]{1,0:T(8,128)(2,1)S(1)}, bf16[128,1024]{1,0:T(8,128)(2,1)S(1)}, u32[]{:S(2)}, u32[]{:S(2)}) collective-permute-start(bf16[128,1024]{1,0:T(8,128)(2,1)S(1)} %shard_map.135), channel_id=1, source_target_pairs={{0,2},{1,3},{2,0},{3,1},{4,6},{5,7},{6,4},{7,5},{8,10},{9,11},{10,... | collective-permute-start | bytes 786440 | tf_op jit(solution)/shard_map/ppermute | solution.py:309
  60.9 7.6 %collective-permute-start.22 = (bf16[64,1024]{1,0:T(8,128)(2,1)S(1)}, bf16[64,1024]{1,0:T(8,128)(2,1)S(1)}, u32[]{:S(2)}, u32[]{:S(2)}) collective-permute-start(bf16[64,1024]{1,0:T(8,128)(2,1)S(1)} %get-tuple-element.76), channel_id=1, source_target_pairs={{0,2},{1,3},{2,0},{3,1},{4,6},{5,7},{6,4},{7,5},{8,10},{9,11},{10,... | collective-permute-start | bytes 393224 | tf_op jit(solution)/shard_map/ppermute | solution.py:309
  62.4 8.3 %collective-permute-start.16 = (bf16[64,1024]{1,0:T(8,128)(2,1)S(1)}, bf16[64,1024]{1,0:T(8,128)(2,1)S(1)}, u32[]{:S(2)}, u32[]{:S(2)}) collective-permute-start(bf16[64,1024]{1,0:T(8,128)(2,1)S(1)} %get-tuple-element.69), channel_id=1, source_target_pairs={{0,2},{1,3},{2,0},{3,1},{4,6},{5,7},{6,4},{7,5},{8,10},{9,11},{10,... | collective-permute-start | bytes 393224 | tf_op jit(solution)/shard_map/ppermute | solution.py:309
  65.7 9.9 %collective-permute-start.32 = (bf16[128,256]{1,0:T(8,128)(2,1)S(1)}, bf16[128,256]{1,0:T(8,128)(2,1)S(1)}, u32[]{:S(2)}, u32[]{:S(2)}) collective-permute-start(bf16[128,256]{1,0:T(8,128)(2,1)S(1)} %get-tuple-element.85), channel_id=1, source_target_pairs={{0,8},{4,12},{8,0},{12,4},{16,24},{20,28},{24,16},{28,20},{1,9},{5... | collective-permute-start | bytes 196616 | tf_op jit(solution)/shard_map/ppermute | solution.py:309
  68.5 8.9 %collective-permute-start.33 = (bf16[128,256]{1,0:T(8,128)(2,1)S(1)}, bf16[128,256]{1,0:T(8,128)(2,1)S(1)}, u32[]{:S(2)}, u32[]{:S(2)}) collective-permute-start(bf16[128,256]{1,0:T(8,128)(2,1)S(1)} %get-tuple-element.86), channel_id=1, source_target_pairs={{0,16},{4,20},{8,24},{12,28},{16,0},{20,4},{24,8},{28,12},{1,17},{... | collective-permute-start | bytes 196616 | tf_op jit(solution)/shard_map/ppermute | solution.py:309
  68.6 8.8 %collective-permute-start.34 = (bf16[128,256]{1,0:T(8,128)(2,1)S(1)}, bf16[128,256]{1,0:T(8,128)(2,1)S(1)}, u32[]{:S(2)}, u32[]{:S(2)}) collective-permute-start(bf16[128,256]{1,0:T(8,128)(2,1)S(1)} %get-tuple-element.87), channel_id=1, source_target_pairs={{0,24},{4,28},{8,16},{12,20},{16,8},{20,12},{24,0},{28,4},{1,25},{... | collective-permute-start | bytes 196616 | tf_op jit(solution)/shard_map/ppermute | solution.py:309
  70.7 10.3 %collective-permute-start.23 = (bf16[32,1024]{1,0:T(8,128)(2,1)S(1)}, bf16[32,1024]{1,0:T(8,128)(2,1)S(1)}, u32[]{:S(2)}, u32[]{:S(2)}) collective-permute-start(bf16[32,1024]{1,0:T(8,128)(2,1)S(1)} %get-tuple-element.77), channel_id=1, source_target_pairs={{0,20},{4,16},{8,28},{12,24},{16,4},{20,0},{24,12},{28,8},{1,21},{... | collective-permute-start | bytes 196616 | tf_op jit(solution)/shard_map/ppermute | solution.py:309
  72.1 9.0 %collective-permute-start.25 = (bf16[32,1024]{1,0:T(8,128)(2,1)S(1)}, bf16[32,1024]{1,0:T(8,128)(2,1)S(1)}, u32[]{:S(2)}, u32[]{:S(2)}) collective-permute-start(bf16[32,1024]{1,0:T(8,128)(2,1)S(1)} %get-tuple-element.79), channel_id=1, source_target_pairs={{0,28},{4,24},{8,20},{12,16},{16,12},{20,8},{24,4},{28,0},{1,29},{... | collective-permute-start | bytes 196616 | tf_op jit(solution)/shard_map/ppermute | solution.py:309
  75.6 7.5 %collective-permute-start.18 = (bf16[32,1024]{1,0:T(8,128)(2,1)S(1)}, bf16[32,1024]{1,0:T(8,128)(2,1)S(1)}, u32[]{:S(2)}, u32[]{:S(2)}) collective-permute-start(bf16[32,1024]{1,0:T(8,128)(2,1)S(1)} %get-tuple-element.72), channel_id=1, source_target_pairs={{0,4},{4,0},{8,12},{12,8},{16,20},{20,16},{24,28},{28,24},{1,5},{5... | collective-permute-start | bytes 196616 | tf_op jit(solution)/shard_map/ppermute | solution.py:309
  77.4 5.6 %collective-permute-start.20 = (bf16[32,1024]{1,0:T(8,128)(2,1)S(1)}, bf16[32,1024]{1,0:T(8,128)(2,1)S(1)}, u32[]{:S(2)}, u32[]{:S(2)}) collective-permute-start(bf16[32,1024]{1,0:T(8,128)(2,1)S(1)} %get-tuple-element.74), channel_id=1, source_target_pairs={{0,12},{4,8},{8,4},{12,0},{16,28},{20,24},{24,20},{28,16},{1,13},{... | collective-permute-start | bytes 196616 | tf_op jit(solution)/shard_map/ppermute | solution.py:309
  77.4 5.6 %collective-permute-start.19 = (bf16[32,1024]{1,0:T(8,128)(2,1)S(1)}, bf16[32,1024]{1,0:T(8,128)(2,1)S(1)}, u32[]{:S(2)}, u32[]{:S(2)}) collective-permute-start(bf16[32,1024]{1,0:T(8,128)(2,1)S(1)} %get-tuple-element.73), channel_id=1, source_target_pairs={{0,8},{4,12},{8,0},{12,4},{16,24},{20,28},{24,16},{28,20},{1,9},{5... | collective-permute-start | bytes 196616 | tf_op jit(solution)/shard_map/ppermute | solution.py:309
  81.0 5.3 %collective-permute-start.21 = (bf16[32,1024]{1,0:T(8,128)(2,1)S(1)}, bf16[32,1024]{1,0:T(8,128)(2,1)S(1)}, u32[]{:S(2)}, u32[]{:S(2)}) collective-permute-start(bf16[32,1024]{1,0:T(8,128)(2,1)S(1)} %get-tuple-element.75), channel_id=1, source_target_pairs={{0,16},{4,20},{8,24},{12,28},{16,0},{20,4},{24,8},{28,12},{1,17},{... | collective-permute-start | bytes 196616 | tf_op jit(solution)/shard_map/ppermute | solution.py:309
  81.0 6.1 %collective-permute-start.24 = (bf16[32,1024]{1,0:T(8,128)(2,1)S(1)}, bf16[32,1024]{1,0:T(8,128)(2,1)S(1)}, u32[]{:S(2)}, u32[]{:S(2)}) collective-permute-start(bf16[32,1024]{1,0:T(8,128)(2,1)S(1)} %get-tuple-element.78), channel_id=1, source_target_pairs={{0,24},{4,28},{8,16},{12,20},{16,8},{20,12},{24,0},{28,4},{1,25},{... | collective-permute-start | bytes 196616 | tf_op jit(solution)/shard_map/ppermute | solution.py:309

commit v4 on v3

--- a/solution.py
+++ b/solution.py
@@ -134,20 +134,8 @@
         row += out_ref.shape[0]
 
 
-def finish_kernel(nz, nx, cap, wide, high_ref, low_ref, *refs):
-    blocks, refs = refs[: nz * nx], refs[nz * nx :]
-    *refs, held, out_s, sems = refs
-    copies = []
-    if wide:
-        *heads, out_ref, attended_ref = refs
-        z = where_am_i(nx)[0]
-        for k in range(nz):
-            columns = pl.ds(pl.multiple_of((z ^ k) * wide, wide), wide)
-            copies.append(pltpu.make_async_copy(heads[k], attended_ref.at[:, columns], sems.at[k]))
-    else:
-        (out_ref,) = refs
-    for copy in copies:
-        copy.start()
+def combine_kernel(cap, high_ref, low_ref, *refs):
+    *blocks, out_ref, held, out_s, sem = refs
     for j, ref in enumerate(blocks):
         held[j * cap : (j + 1) * cap, :] = ref[...]
     returned = held[...]
@@ -155,8 +143,21 @@
     out_s[...] = (
         dot(high_ref[...], returned, rows) + dot(low_ref[...], returned, rows)
     ).astype(jnp.bfloat16)
-    copies.append(pltpu.make_async_copy(out_s, out_ref, sems.at[nz]))
-    copies[-1].start()
+    copy = pltpu.make_async_copy(out_s, out_ref, sem)
+    copy.start()
+    copy.wait()
+
+
+def join_kernel(nz, nx, *refs):
+    *head_refs, out_ref, sems = refs
+    z = where_am_i(nx)[0]
+    wide = head_refs[0].shape[1]
+    copies = []
+    for k in range(nz):
+        columns = pl.ds(pl.multiple_of((z ^ k) * wide, wide), wide)
+        copies.append(pltpu.make_async_copy(head_refs[k], out_ref.at[:, columns], sems.at[k]))
+    for copy in copies:
+        copy.start()
     for copy in copies:
         copy.wait()
 
@@ -360,7 +361,6 @@
 
     packs = [shift(pack, "ep", k * nx) for k, pack in enumerate(packs)]
 
-    attended = None
     if wide:
         swaps = [[0], [nz // 2], [k for k in range(1, nz) if k != nz // 2]]
         swapped = []
@@ -382,6 +382,13 @@
             mib=16,
         )
         outs = [shift(outs[k], "ep", k * nx) for k in range(nz)]
+        attended = kernel(
+            functools.partial(join_kernel, nz, nx),
+            outs,
+            struct((rows_a, nz * wide)),
+            out_specs=HBM,
+            scratch=[pltpu.SemaphoreType.DMA((nz,))],
+        )
     else:
         attended = gathered_attention(queries, key_rows, values, lambdas, head_gain)
 
@@ -432,24 +439,18 @@
         [struct((slots, rows_b))] * 2,
         cost=pl.CostEstimate(flops=20_000_000_000, bytes_accessed=100_000, transcendentals=0),
     )
-    shapes = [struct((rows_b, width))] + [struct((rows_a, nz * wide))] * (wide > 0)
-    out, *held = kernel(
-        functools.partial(finish_kernel, nz, nx, cap, wide),
-        (
-            high,
-            low,
-            *[returned[k, m] for k in range(nz) for m in range(nx)],
-            *(outs if wide else ()),
-        ),
-        shapes,
-        out_specs=[HBM] * len(shapes),
+    out = kernel(
+        functools.partial(combine_kernel, cap),
+        (high, low, *[returned[k, m] for k in range(nz) for m in range(nx)]),
+        struct((rows_b, width)),
+        out_specs=HBM,
         scratch=[
             pltpu.VMEM((slots, width), jnp.bfloat16),
             pltpu.VMEM((rows_b, width), jnp.bfloat16),
-            pltpu.SemaphoreType.DMA((nz + 1,)),
+            pltpu.SemaphoreType.DMA,
         ],
     )
-    return held[0] if wide else attended, out
+    return attended, out
 
 
 def solution(mesh):

time: 88.4 us -> 84 us (0.950)
  waiting for transfers between devices: 29.4 us -> 26.3 us
  starting transfers between devices: 43 us -> 41.1 us
    ppermute x35, waiting for transfers between devices: 29.4 us -> 26.3 us  [shift(): return lax.ppermute(v, axis, [(i, i ^ mask) for i in range(n)])]
    ppermute x35, starting transfers between devices: 43 us -> 41.1 us  [shift(): return lax.ppermute(v, axis, [(i, i ^ mask) for i in range(n)])]
    pallas_call x13 -> x14, Pallas kernels: 10.2 us -> 10.9 us  [kernel(): pl.pallas_call(body, out_shape=outs, in_specs=in_specs or [VMEM] * len(in...]
  transfers between devices with their start and end apart: 35 -> 35, of which waited for: 10 -> 11; matrix products, arithmetic and copies ran while one was open for 0% -> 0% of each run, Pallas kernels for 8% -> 10%
where the time goes in v4:
time: 84 us; the launch traced here: 83.8 us
  starting transfers between devices  41.1 us (49%)
  waiting for transfers between devices  26.3 us (31%)
  Pallas kernels  10.9 us (13%)
  local copies, waits for them, and re-layouts  4.51 us (5%)
  between operations  0.96 us (1%)
    ppermute x35, starting transfers between devices, shift(): return lax.ppermute(v, axis, [(i, i ^ mask) for i in range(n)])  41.1 us
    ppermute x35, waiting for transfers between devices, shift(): return lax.ppermute(v, axis, [(i, i ^ mask) for i in range(n)])  26.3 us
    pallas_call x14, Pallas kernels, kernel(): pl.pallas_call(body, out_shape=outs, in_specs=in_specs or [VMEM] * len(in...  10.9 us
    unnamed x17, local copies, waits for them, and re-layouts  4.44 us
  transfers between devices with their start and end apart: 35, of which 11 were waited for; matrix products, arithmetic and copies ran while one was open for 0% of the time, Pallas kernels for 10%

profile of v4, /device:TPU:0, one launch (start us, length us, event | category | flops | bytes accessed | tf_op | source)
XLA Modules:
  0.0 83.8 jit_solution(2558096740886909048)
XLA Ops:
  0.6 1.9 %shard_map.132 = (bf16[64,1024]{1,0:T(8,128)(2,1)S(1)}, bf16[64,1024]{1,0:T(8,128)(2,1)S(1)}, bf16[64,1024]{1,0:T(8,128)(2,1)S(1)}, bf16[64,1024]{1,0:T(8,128)(2...) custom-call(bf16[64,4096]{1,0:T(8,128)(2,1)} %tokens_ref.1, ...), custom_call_target="tpu_custom_call" | custom-call | tf_op jit(solution)/shard_map/pallas_call | solution.py:318
  2.6 5.1 %collective-permute-start.11 = (bf16[32,1024]{1,0:T(8,128)(2,1)S(1)}, bf16[32,1024]{1,0:T(8,128)(2,1)S(1)}, u32[]{:S(2)}, u32[]{:S(2)}) collective-permute-start(bf16[32,1024]{1,0:T(8,128)(2,1)S(1)} %get-tuple-element.59), channel_id=1, source_target_pairs={{0,24},{4,28},{8,16},{12,20},{16,8},{20,12},{24,0},{28,4},{1,25},{... | collective-permute-start | bytes 196616 | tf_op jit(solution)/shard_map/ppermute | solution.py:310
  7.7 0.0 collective-permute-start.10
  7.7 1.5 %collective-permute-start.14 = (bf16[64,1024]{1,0:T(8,128)(2,1)S(1)}, bf16[64,1024]{1,0:T(8,128)(2,1)S(1)}, u32[]{:S(2)}, u32[]{:S(2)}) collective-permute-start(bf16[64,1024]{1,0:T(8,128)(2,1)S(1)} %get-tuple-element.60), channel_id=1, source_target_pairs={{0,4},{4,0},{8,12},{12,8},{16,20},{20,16},{24,28},{28,24},{1,5},{5... | collective-permute-start | bytes 393224 | tf_op jit(solution)/shard_map/ppermute | solution.py:310
  9.2 0.6 collective-permute-start.15
  9.8 2.8 %collective-permute-start.16 = (bf16[32,1024]{1,0:T(8,128)(2,1)S(1)}, bf16[32,1024]{1,0:T(8,128)(2,1)S(1)}, u32[]{:S(2)}, u32[]{:S(2)}) collective-permute-start(bf16[32,1024]{1,0:T(8,128)(2,1)S(1)} %get-tuple-element.62), channel_id=1, source_target_pairs={{0,20},{4,16},{8,28},{12,24},{16,4},{20,0},{24,12},{28,8},{1,21},{... | collective-permute-start | bytes 196616 | tf_op jit(solution)/shard_map/ppermute | solution.py:310
  12.6 2.8 %collective-permute-start.17 = (bf16[32,1024]{1,0:T(8,128)(2,1)S(1)}, bf16[32,1024]{1,0:T(8,128)(2,1)S(1)}, u32[]{:S(2)}, u32[]{:S(2)}) collective-permute-start(bf16[32,1024]{1,0:T(8,128)(2,1)S(1)} %get-tuple-element.63), channel_id=1, source_target_pairs={{0,28},{4,24},{8,20},{12,16},{16,12},{20,8},{24,4},{28,0},{1,29},{... | collective-permute-start | bytes 196616 | tf_op jit(solution)/shard_map/ppermute | solution.py:310
  15.4 0.0 collective-permute-done.10
  15.4 0.0 collective-permute-start.9
  15.4 0.6 collective-permute-done.14
  16.0 1.1 %collective-permute-start.12 = (bf16[64,1024]{1,0:T(8,128)(2,1)S(1)}, bf16[64,1024]{1,0:T(8,128)(2,1)S(1)}, u32[]{:S(2)}, u32[]{:S(2)}) collective-permute-start(bf16[64,1024]{1,0:T(8,128)(2,1)S(1)} %pad_maximum_fusion.3), channel_id=1, source_target_pairs={{0,2},{1,3},{2,0},{3,1},{4,6},{5,7},{6,4},{7,5},{8,10},{9,11},{10,... | collective-permute-start | bytes 393224 | tf_op jit(solution)/shard_map/ppermute | solution.py:310
  17.1 1.9 %collective-permute-done.15 = bf16[64,1024]{1,0:T(8,128)(2,1)S(1)} collective-permute-done((bf16[64,1024]{1,0:T(8,128)(2,1)S(1)}, bf16[64,1024]{1,0:T(8,128)(2,1)S(1)}, u32[]{:S(2)}, u32[]{:S(2)}) %collective-permute-start.15) | collective-permute-done | bytes 131104 | tf_op jit(solution)/shard_map/ppermute | solution.py:310
  19.0 0.0 collective-permute-done.16
  19.1 2.2 %collective-permute-done.17 = bf16[32,1024]{1,0:T(8,128)(2,1)S(1)} collective-permute-done((bf16[32,1024]{1,0:T(8,128)(2,1)S(1)}, bf16[32,1024]{1,0:T(8,128)(2,1)S(1)}, u32[]{:S(2)}, u32[]{:S(2)}) %collective-permute-start.17) | collective-permute-done | bytes 65568 | tf_op jit(solution)/shard_map/ppermute | solution.py:310
  21.3 0.1 collective-permute-start.18
  21.4 1.5 %collective-permute-start.22 = (bf16[64,1024]{1,0:T(8,128)(2,1)S(1)}, bf16[64,1024]{1,0:T(8,128)(2,1)S(1)}, u32[]{:S(2)}, u32[]{:S(2)}) collective-permute-start(bf16[64,1024]{1,0:T(8,128)(2,1)S(1)} %pad_maximum_fusion.4), channel_id=1, source_target_pairs={{0,2},{1,3},{2,0},{3,1},{4,6},{5,7},{6,4},{7,5},{8,10},{9,11},{10,... | collective-permute-start | bytes 393224 | tf_op jit(solution)/shard_map/ppermute | solution.py:310
  22.9 0.0 collective-permute-done.12
  22.9 0.3 collective-permute-start.13
  23.2 4.2 %collective-permute-done.22 = bf16[64,1024]{1,0:T(8,128)(2,1)S(1)} collective-permute-done((bf16[64,1024]{1,0:T(8,128)(2,1)S(1)}, bf16[64,1024]{1,0:T(8,128)(2,1)S(1)}, u32[]{:S(2)}, u32[]{:S(2)}) %collective-permute-start.22) | collective-permute-done | bytes 131104 | tf_op jit(solution)/shard_map/ppermute | solution.py:310
  27.4 0.1 collective-permute-start.23
  27.5 2.1 %collective-permute-start.2 = (bf16[384,256]{1,0:T(8,128)(2,1)S(1)}, bf16[384,256]{1,0:T(8,128)(2,1)S(1)}, u32[]{:S(2)}, u32[]{:S(2)}) collective-permute-start(bf16[384,256]{1,0:T(8,128)(2,1)S(1)} %get-tuple-element.47), channel_id=1, source_target_pairs={{0,24},{4,28},{8,16},{12,20},{16,8},{20,12},{24,0},{28,4},{1,25},{... | collective-permute-start | bytes 589832 | tf_op jit(solution)/shard_map/ppermute | solution.py:310
  29.6 0.0 copy-start.1
  29.6 2.2 %copy-done.1 = bf16[1,4096,512]{2,1,0:T(8,128)(2,1)S(1)} copy-done((bf16[1,4096,512]{2,1,0:T(8,128)(2,1)S(1)}, bf16[1,4096,512]{2,1,0:T(8,128)(2,1)}, u32[]{:S(2)}) %copy-start.1) | copy-done | bytes 4194328
  31.8 1.2 %shard_map.136 = (f32[128,512]{1,0:T(8,128)S(1)}, f32[128,512]{1,0:T(8,128)S(1)}, f32[128,512]{1,0:T(8,128)S(1)}, f32[128,512]{1,0:T(8,128)S(1)}) custom-call(bf16[256,1024]{1,0:T(8,128)(2,1)S(1)} %constant_dynamic-update-slice_fusion.first_ref, bf16[256,1024]{1,0:T(8,128)(2,1)S(1)} %collective-permute-done.18.second_ref, bf16[4096,512]{1,0:T(8,128)(2,1)S(1)} %bitcast.7, ...), custom_call_target="tpu_custom_call" | custom-call | tf_op jit(solution)/shard_map/pallas_call | solution.py:318
  33.1 0.9 %copy-done.2 = bf16[1,4096,512]{2,1,0:T(8,128)(2,1)S(1)} copy-done((bf16[1,4096,512]{2,1,0:T(8,128)(2,1)S(1)}, bf16[1,4096,512]{2,1,0:T(8,128)(2,1)}, u32[]{:S(2)}) %copy-start.2) | copy-done | bytes 4194328
  34.0 1.3 %copy-done.3 = bf16[1,512,4096]{2,1,0:T(8,128)(2,1)S(1)} copy-done((bf16[1,512,4096]{2,1,0:T(8,128)(2,1)S(1)}, bf16[1,512,4096]{2,1,0:T(8,128)(2,1)}, u32[]{:S(2)}) %copy-start.3) | copy-done | bytes 4194328
  35.3 1.4 %shard_map.137 = (bf16[128,1024]{1,0:T(8,128)(2,1)S(1)}, bf16[128,1024]{1,0:T(8,128)(2,1)S(1)}, bf16[128,1024]{1,0:T(8,128)(2,1)S(1)}, bf16[128,1024]{1,0:T(8,128)(2,1)S(1)}) custom-call(bf16[128,1024]{1,0:T(8,128)(2,1)S(1)} %pad_maximum_fusion.1.refs_0_, bf16[128,1024]{1,0:T(8,128)(2,1)S(1)} %collective-permute-done.13.refs_1_, ...), custom_call_target="tpu_custom_call" | custom-call | tf_op jit(solution)/shard_map/pallas_call | solution.py:318
  36.7 0.2 collective-permute-start.19
  36.9 1.4 %shard_map.140 = (bf16[128,1024]{1,0:T(8,128)(2,1)S(1)}, bf16[128,1024]{1,0:T(8,128)(2,1)S(1)}, bf16[128,1024]{1,0:T(8,128)(2,1)S(1)}, bf16[128,1024]{1,0:T(8,128)(2,1)S(1)}) custom-call(bf16[128,1024]{1,0:T(8,128)(2,1)S(1)} %pad_maximum_fusion.2.refs_0_, bf16[128,1024]{1,0:T(8,128)(2,1)S(1)} %collective-permute-done.23.refs_1_, ...), custom_call_target="tpu_custom_call" | custom-call | tf_op jit(solution)/shard_map/pallas_call | solution.py:318
  38.3 0.4 collective-permute-start.24
  38.7 2.3 %collective-permute-start.1 = (bf16[384,256]{1,0:T(8,128)(2,1)S(1)}, bf16[384,256]{1,0:T(8,128)(2,1)S(1)}, u32[]{:S(2)}, u32[]{:S(2)}) collective-permute-start(bf16[384,256]{1,0:T(8,128)(2,1)S(1)} %get-tuple-element.46), channel_id=1, source_target_pairs={{0,16},{4,20},{8,24},{12,28},{16,0},{20,4},{24,8},{28,12},{1,17},{... | collective-permute-start | bytes 589832 | tf_op jit(solution)/shard_map/ppermute | solution.py:310
  41.0 1.1 %collective-permute-start.3 = (bf16[256,256]{1,0:T(8,128)(2,1)S(1)}, bf16[256,256]{1,0:T(8,128)(2,1)S(1)}, u32[]{:S(2)}, u32[]{:S(2)}) collective-permute-start(bf16[256,256]{1,0:T(8,128)(2,1)S(1)} %slice.36), channel_id=1, source_target_pairs={{0,4},{4,0},{8,12},{12,8},{16,20},{20,16},{24,28},{28,24},{1,5},{5... | collective-permute-start | bytes 393224 | tf_op jit(solution)/shard_map/ppermute | solution.py:310
  42.2 1.1 %collective-permute-start.5 = (bf16[512,256]{1,0:T(8,128)(2,1)S(1)}, bf16[512,256]{1,0:T(8,128)(2,1)S(1)}, u32[]{:S(2)}, u32[]{:S(2)}) collective-permute-start(bf16[512,256]{1,0:T(8,128)(2,1)S(1)} %pad_maximum_fusion), channel_id=1, source_target_pairs={{0,4},{4,0},{8,12},{12,8},{16,20},{20,16},{24,28},{28,24},{1,5},{5... | collective-permute-start | bytes 786440 | tf_op jit(solution)/shard_map/ppermute | solution.py:310
  43.3 7.5 %collective-permute-done.1.refs_2_ = bf16[384,256]{1,0:T(8,128)(2,1)S(1)} collective-permute-done((bf16[384,256]{1,0:T(8,128)(2,1)S(1)}, bf16[384,256]{1,0:T(8,128)(2,1)S(1)}, u32[]{:S(2)}, u32[]{:S(2)}) %collective-permute-start.1) | collective-permute-done | bytes 196640 | tf_op jit(solution)/shard_map/ppermute | solution.py:310
  50.8 0.1 collective-permute-start.26
  50.9 1.0 %collective-permute-start.4 = (bf16[256,256]{1,0:T(8,128)(2,1)S(1)}, bf16[256,256]{1,0:T(8,128)(2,1)S(1)}, u32[]{:S(2)}, u32[]{:S(2)}) collective-permute-start(bf16[256,256]{1,0:T(8,128)(2,1)S(1)} %slice.48), channel_id=1, source_target_pairs={{0,4},{4,0},{8,12},{12,8},{16,20},{20,16},{24,28},{28,24},{1,5},{5... | collective-permute-start | bytes 393224 | tf_op jit(solution)/shard_map/ppermute | solution.py:310
  51.9 0.1 collective-permute-start.21
  52.0 0.1 shard_map.138
  52.1 1.6 %collective-permute-start.20 = (bf16[128,1024]{1,0:T(8,128)(2,1)S(1)}, bf16[128,1024]{1,0:T(8,128)(2,1)S(1)}, u32[]{:S(2)}, u32[]{:S(2)}) collective-permute-start(bf16[128,1024]{1,0:T(8,128)(2,1)S(1)} %shard_map.138), channel_id=1, source_target_pairs={{0,2},{1,3},{2,0},{3,1},{4,6},{5,7},{6,4},{7,5},{8,10},{9,11},{10,... | collective-permute-start | bytes 786440 | tf_op jit(solution)/shard_map/ppermute | solution.py:310
  53.7 0.1 shard_map.141
  53.8 3.0 %collective-permute-done.4.refs_5_ = bf16[256,256]{1,0:T(8,128)(2,1)S(1)} collective-permute-done((bf16[256,256]{1,0:T(8,128)(2,1)S(1)}, bf16[256,256]{1,0:T(8,128)(2,1)S(1)}, u32[]{:S(2)}, u32[]{:S(2)}) %collective-permute-start.4) | collective-permute-done | bytes 131104 | tf_op jit(solution)/shard_map/ppermute | solution.py:310
  56.8 1.5 %collective-permute-start.25 = (bf16[64,1024]{1,0:T(8,128)(2,1)S(1)}, bf16[64,1024]{1,0:T(8,128)(2,1)S(1)}, u32[]{:S(2)}, u32[]{:S(2)}) collective-permute-start(bf16[64,1024]{1,0:T(8,128)(2,1)S(1)} %get-tuple-element.75), channel_id=1, source_target_pairs={{0,2},{1,3},{2,0},{3,1},{4,6},{5,7},{6,4},{7,5},{8,10},{9,11},{10,... | collective-permute-start | bytes 393224 | tf_op jit(solution)/shard_map/ppermute | solution.py:310
  58.3 0.5 collective-permute-start.31
  58.8 2.7 %shard_map.133 = (bf16[128,256]{1,0:T(8,128)(2,1)S(1)}, bf16[128,256]{1,0:T(8,128)(2,1)S(1)}, bf16[128,256]{1,0:T(8,128)(2,1)S(1)}, bf16[128,256]{1,0:T(8,128)(2,1)S(1)}) custom-call(f32[4]{0:T(128)S(1)} %copy-done.5, f32[1,256]{1,0:T(1,128)S(1)} %shard_map.131.gain_ref, bf16[384,256]{1,0:T(8,128)(2,1)S(1)} %get-tuple-element.44.refs_0_, ...), custom_call_target="tpu_custom_call" | custom-call | tf_op jit(solution)/shard_map/pallas_call | solution.py:318
  61.6 0.1 collective-permute-start.6
  61.7 2.5 %collective-permute-done.25.refs_0_ = bf16[64,1024]{1,0:T(8,128)(2,1)S(1)} collective-permute-done((bf16[64,1024]{1,0:T(8,128)(2,1)S(1)}, bf16[64,1024]{1,0:T(8,128)(2,1)S(1)}, u32[]{:S(2)}, u32[]{:S(2)}) %collective-permute-start.25) | collective-permute-done | bytes 131104 | tf_op jit(solution)/shard_map/ppermute | solution.py:310
  64.2 0.1 shard_map.142
  64.2 1.9 %collective-permute-start.8 = (bf16[128,256]{1,0:T(8,128)(2,1)S(1)}, bf16[128,256]{1,0:T(8,128)(2,1)S(1)}, u32[]{:S(2)}, u32[]{:S(2)}) collective-permute-start(bf16[128,256]{1,0:T(8,128)(2,1)S(1)} %get-tuple-element.51), channel_id=1, source_target_pairs={{0,24},{4,28},{8,16},{12,20},{16,8},{20,12},{24,0},{28,4},{1,25},{... | collective-permute-start | bytes 196616 | tf_op jit(solution)/shard_map/ppermute | solution.py:310
  66.2 0.2 collective-permute-done.31.refs_0_
  66.4 1.1 %collective-permute-start.27 = (bf16[32,1024]{1,0:T(8,128)(2,1)S(1)}, bf16[32,1024]{1,0:T(8,128)(2,1)S(1)}, u32[]{:S(2)}, u32[]{:S(2)}) collective-permute-start(bf16[32,1024]{1,0:T(8,128)(2,1)S(1)} %get-tuple-element.78), channel_id=1, source_target_pairs={{0,4},{4,0},{8,12},{12,8},{16,20},{20,16},{24,28},{28,24},{1,5},{5... | collective-permute-start | bytes 196616 | tf_op jit(solution)/shard_map/ppermute | solution.py:310
  67.5 1.8 %collective-permute-start.29 = (bf16[32,1024]{1,0:T(8,128)(2,1)S(1)}, bf16[32,1024]{1,0:T(8,128)(2,1)S(1)}, u32[]{:S(2)}, u32[]{:S(2)}) collective-permute-start(bf16[32,1024]{1,0:T(8,128)(2,1)S(1)} %get-tuple-element.80), channel_id=1, source_target_pairs={{0,12},{4,8},{8,4},{12,0},{16,28},{20,24},{24,20},{28,16},{1,13},{... | collective-permute-start | bytes 196616 | tf_op jit(solution)/shard_map/ppermute | solution.py:310
  69.3 0.1 shard_map.143
  69.3 0.1 shard_map.139
  69.4 1.5 %collective-permute-start.32 = (bf16[32,1024]{1,0:T(8,128)(2,1)S(1)}, bf16[32,1024]{1,0:T(8,128)(2,1)S(1)}, u32[]{:S(2)}, u32[]{:S(2)}) collective-permute-start(bf16[32,1024]{1,0:T(8,128)(2,1)S(1)} %get-tuple-element.83), channel_id=1, source_target_pairs={{0,20},{4,16},{8,28},{12,24},{16,4},{20,0},{24,12},{28,8},{1,21},{... | collective-permute-start | bytes 196616 | tf_op jit(solution)/shard_map/ppermute | solution.py:310
  70.9 2.5 %collective-permute-start.34 = (bf16[32,1024]{1,0:T(8,128)(2,1)S(1)}, bf16[32,1024]{1,0:T(8,128)(2,1)S(1)}, u32[]{:S(2)}, u32[]{:S(2)}) collective-permute-start(bf16[32,1024]{1,0:T(8,128)(2,1)S(1)} %get-tuple-element.85), channel_id=1, source_target_pairs={{0,28},{4,24},{8,20},{12,16},{16,12},{20,8},{24,4},{28,0},{1,29},{... | collective-permute-start | bytes 196616 | tf_op jit(solution)/shard_map/ppermute | solution.py:310
  73.4 0.5 collective-permute-start.28
  73.9 1.9 %collective-permute-start.30 = (bf16[32,1024]{1,0:T(8,128)(2,1)S(1)}, bf16[32,1024]{1,0:T(8,128)(2,1)S(1)}, u32[]{:S(2)}, u32[]{:S(2)}) collective-permute-start(bf16[32,1024]{1,0:T(8,128)(2,1)S(1)} %get-tuple-element.81), channel_id=1, source_target_pairs={{0,16},{4,20},{8,24},{12,28},{16,0},{20,4},{24,8},{28,12},{1,17},{... | collective-permute-start | bytes 196616 | tf_op jit(solution)/shard_map/ppermute | solution.py:310
  75.8 2.0 %collective-permute-start.33 = (bf16[32,1024]{1,0:T(8,128)(2,1)S(1)}, bf16[32,1024]{1,0:T(8,128)(2,1)S(1)}, u32[]{:S(2)}, u32[]{:S(2)}) collective-permute-start(bf16[32,1024]{1,0:T(8,128)(2,1)S(1)} %get-tuple-element.84), channel_id=1, source_target_pairs={{0,24},{4,28},{8,16},{12,20},{16,8},{20,12},{24,0},{28,4},{1,25},{... | collective-permute-start | bytes 196616 | tf_op jit(solution)/shard_map/ppermute | solution.py:310
  77.8 0.2 shard_map.135
  77.9 0.7 shard_map.134
  78.7 0.8 collective-permute-done.32.refs_5_
  79.5 0.1 collective-permute-done.28.refs_2_
  79.6 3.3 %collective-permute-done.30.refs_4_ = bf16[32,1024]{1,0:T(8,128)(2,1)S(1)} collective-permute-done((bf16[32,1024]{1,0:T(8,128)(2,1)S(1)}, bf16[32,1024]{1,0:T(8,128)(2,1)S(1)}, u32[]{:S(2)}, u32[]{:S(2)}) %collective-permute-start.30) | collective-permute-done | bytes 65568 | tf_op jit(solution)/shard_map/ppermute | solution.py:310
  82.9 1.0 %shard_map.144 = bf16[64,1024]{1,0:T(8,128)(2,1)} custom-call(bf16[256,64]{1,0:T(8,128)(2,1)S(1)} %get-tuple-element.54.high_ref, bf16[256,64]{1,0:T(8,128)(2,1)S(1)} %get-tuple-element.55.low_ref, bf16[32,1024]{1,0:T(8,128)(2,1)S(1)} %get-tuple-element.70.refs_0_, bf16[32,1024]{1,0:T(8,128)(2,1)S(1)} %collective-permute-done.27.refs_1_, ...), custom_call_target="tpu_custom_call" | custom-call | tf_op jit(solution)/shard_map/pallas_call | solution.py:318
  (49 shorter events, 0.3 us)
Async XLA Ops:
  0.6 29.0 %copy-start = (bf16[1,4096,512]{2,1,0:T(8,128)(2,1)S(1)}, bf16[1,4096,512]{2,1,0:T(8,128)(2,1)}, u32[]{:S(2)}) copy-start(bf16[1,4096,512]{2,1,0:T(8,128)(2,1)} %param.21) | copy-start | bytes 12582916
  2.6 10.0 %collective-permute-start.11 = (bf16[32,1024]{1,0:T(8,128)(2,1)S(1)}, bf16[32,1024]{1,0:T(8,128)(2,1)S(1)}, u32[]{:S(2)}, u32[]{:S(2)}) collective-permute-start(bf16[32,1024]{1,0:T(8,128)(2,1)S(1)} %get-tuple-element.59), channel_id=1, source_target_pairs={{0,24},{4,28},{8,16},{12,20},{16,8},{20,12},{24,0},{28,4},{1,25},{... | collective-permute-start | bytes 196616 | tf_op jit(solution)/shard_map/ppermute | solution.py:310
  7.7 7.7 %collective-permute-start.10 = (bf16[32,1024]{1,0:T(8,128)(2,1)S(1)}, bf16[32,1024]{1,0:T(8,128)(2,1)S(1)}, u32[]{:S(2)}, u32[]{:S(2)}) collective-permute-start(bf16[32,1024]{1,0:T(8,128)(2,1)S(1)} %get-tuple-element.58), channel_id=1, source_target_pairs={{0,16},{4,20},{8,24},{12,28},{16,0},{20,4},{24,8},{28,12},{1,17},{... | collective-permute-start | bytes 196616 | tf_op jit(solution)/shard_map/ppermute | solution.py:310
  7.7 8.3 %collective-permute-start.14 = (bf16[64,1024]{1,0:T(8,128)(2,1)S(1)}, bf16[64,1024]{1,0:T(8,128)(2,1)S(1)}, u32[]{:S(2)}, u32[]{:S(2)}) collective-permute-start(bf16[64,1024]{1,0:T(8,128)(2,1)S(1)} %get-tuple-element.60), channel_id=1, source_target_pairs={{0,4},{4,0},{8,12},{12,8},{16,20},{20,16},{24,28},{28,24},{1,5},{5... | collective-permute-start | bytes 393224 | tf_op jit(solution)/shard_map/ppermute | solution.py:310
  9.2 9.8 %collective-permute-start.15 = (bf16[64,1024]{1,0:T(8,128)(2,1)S(1)}, bf16[64,1024]{1,0:T(8,128)(2,1)S(1)}, u32[]{:S(2)}, u32[]{:S(2)}) collective-permute-start(bf16[64,1024]{1,0:T(8,128)(2,1)S(1)} %get-tuple-element.61), channel_id=1, source_target_pairs={{0,12},{4,8},{8,4},{12,0},{16,28},{20,24},{24,20},{28,16},{1,13},{... | collective-permute-start | bytes 393224 | tf_op jit(solution)/shard_map/ppermute | solution.py:310
  9.8 9.2 %collective-permute-start.16 = (bf16[32,1024]{1,0:T(8,128)(2,1)S(1)}, bf16[32,1024]{1,0:T(8,128)(2,1)S(1)}, u32[]{:S(2)}, u32[]{:S(2)}) collective-permute-start(bf16[32,1024]{1,0:T(8,128)(2,1)S(1)} %get-tuple-element.62), channel_id=1, source_target_pairs={{0,20},{4,16},{8,28},{12,24},{16,4},{20,0},{24,12},{28,8},{1,21},{... | collective-permute-start | bytes 196616 | tf_op jit(solution)/shard_map/ppermute | solution.py:310
  12.6 8.6 %collective-permute-start.17 = (bf16[32,1024]{1,0:T(8,128)(2,1)S(1)}, bf16[32,1024]{1,0:T(8,128)(2,1)S(1)}, u32[]{:S(2)}, u32[]{:S(2)}) collective-permute-start(bf16[32,1024]{1,0:T(8,128)(2,1)S(1)} %get-tuple-element.63), channel_id=1, source_target_pairs={{0,28},{4,24},{8,20},{12,16},{16,12},{20,8},{24,4},{28,0},{1,29},{... | collective-permute-start | bytes 196616 | tf_op jit(solution)/shard_map/ppermute | solution.py:310
  15.4 5.8 %collective-permute-start.9 = (bf16[64,1024]{1,0:T(8,128)(2,1)S(1)}, bf16[64,1024]{1,0:T(8,128)(2,1)S(1)}, u32[]{:S(2)}, u32[]{:S(2)}) collective-permute-start(bf16[64,1024]{1,0:T(8,128)(2,1)S(1)} %get-tuple-element.57), channel_id=1, source_target_pairs={{0,8},{4,12},{8,0},{12,4},{16,24},{20,28},{24,16},{28,20},{1,9},{5... | collective-permute-start | bytes 393224 | tf_op jit(solution)/shard_map/ppermute | solution.py:310
  16.0 6.9 %collective-permute-start.12 = (bf16[64,1024]{1,0:T(8,128)(2,1)S(1)}, bf16[64,1024]{1,0:T(8,128)(2,1)S(1)}, u32[]{:S(2)}, u32[]{:S(2)}) collective-permute-start(bf16[64,1024]{1,0:T(8,128)(2,1)S(1)} %pad_maximum_fusion.3), channel_id=1, source_target_pairs={{0,2},{1,3},{2,0},{3,1},{4,6},{5,7},{6,4},{7,5},{8,10},{9,11},{10,... | collective-permute-start | bytes 393224 | tf_op jit(solution)/shard_map/ppermute | solution.py:310
  21.3 8.3 %collective-permute-start.18 = (bf16[256,1024]{1,0:T(8,128)(2,1)S(1)}, bf16[256,1024]{1,0:T(8,128)(2,1)S(1)}, u32[]{:S(2)}, u32[]{:S(2)}) collective-permute-start(bf16[256,1024]{1,0:T(8,128)(2,1)S(1)} %constant_dynamic-update-slice_fusion.first_ref), channel_id=1, source_target_pairs={{0,1},{1,0},{2,3},{3,2},{4,5},{5,4},{6,7},{7,6},{8,9},{9,8},{10,11... | collective-permute-start | bytes 1572872 | tf_op jit(solution)/shard_map/ppermute | solution.py:310
  21.4 6.0 %collective-permute-start.22 = (bf16[64,1024]{1,0:T(8,128)(2,1)S(1)}, bf16[64,1024]{1,0:T(8,128)(2,1)S(1)}, u32[]{:S(2)}, u32[]{:S(2)}) collective-permute-start(bf16[64,1024]{1,0:T(8,128)(2,1)S(1)} %pad_maximum_fusion.4), channel_id=1, source_target_pairs={{0,2},{1,3},{2,0},{3,1},{4,6},{5,7},{6,4},{7,5},{8,10},{9,11},{10,... | collective-permute-start | bytes 393224 | tf_op jit(solution)/shard_map/ppermute | solution.py:310
  22.9 10.1 %collective-permute-start.13 = (bf16[128,1024]{1,0:T(8,128)(2,1)S(1)}, bf16[128,1024]{1,0:T(8,128)(2,1)S(1)}, u32[]{:S(2)}, u32[]{:S(2)}) collective-permute-start(bf16[128,1024]{1,0:T(8,128)(2,1)S(1)} %pad_maximum_fusion.1.refs_0_), channel_id=1, source_target_pairs={{0,1},{1,0},{2,3},{3,2},{4,5},{5,4},{6,7},{7,6},{8,9},{9,8},{10,11... | collective-permute-start | bytes 786440 | tf_op jit(solution)/shard_map/ppermute | solution.py:310
  27.4 9.5 %collective-permute-start.23 = (bf16[128,1024]{1,0:T(8,128)(2,1)S(1)}, bf16[128,1024]{1,0:T(8,128)(2,1)S(1)}, u32[]{:S(2)}, u32[]{:S(2)}) collective-permute-start(bf16[128,1024]{1,0:T(8,128)(2,1)S(1)} %pad_maximum_fusion.2.refs_0_), channel_id=1, source_target_pairs={{0,1},{1,0},{2,3},{3,2},{4,5},{5,4},{6,7},{7,6},{8,9},{9,8},{10,11... | collective-permute-start | bytes 786440 | tf_op jit(solution)/shard_map/ppermute | solution.py:310
  27.5 13.6 %collective-permute-start.2 = (bf16[384,256]{1,0:T(8,128)(2,1)S(1)}, bf16[384,256]{1,0:T(8,128)(2,1)S(1)}, u32[]{:S(2)}, u32[]{:S(2)}) collective-permute-start(bf16[384,256]{1,0:T(8,128)(2,1)S(1)} %get-tuple-element.47), channel_id=1, source_target_pairs={{0,24},{4,28},{8,16},{12,20},{16,8},{20,12},{24,0},{28,4},{1,25},{... | collective-permute-start | bytes 589832 | tf_op jit(solution)/shard_map/ppermute | solution.py:310
  29.6 12.6 %collective-permute-start = (bf16[384,256]{1,0:T(8,128)(2,1)S(1)}, bf16[384,256]{1,0:T(8,128)(2,1)S(1)}, u32[]{:S(2)}, u32[]{:S(2)}) collective-permute-start(bf16[384,256]{1,0:T(8,128)(2,1)S(1)} %get-tuple-element.45), channel_id=1, source_target_pairs={{0,8},{4,12},{8,0},{12,4},{16,24},{20,28},{24,16},{28,20},{1,9},{5... | collective-permute-start | bytes 589832 | tf_op jit(solution)/shard_map/ppermute | solution.py:310
  29.6 2.2 %copy-start.1 = (bf16[1,4096,512]{2,1,0:T(8,128)(2,1)S(1)}, bf16[1,4096,512]{2,1,0:T(8,128)(2,1)}, u32[]{:S(2)}) copy-start(bf16[1,4096,512]{2,1,0:T(8,128)(2,1)} %param.22) | copy-start | bytes 12582916
  31.8 2.2 %copy-start.2 = (bf16[1,4096,512]{2,1,0:T(8,128)(2,1)S(1)}, bf16[1,4096,512]{2,1,0:T(8,128)(2,1)}, u32[]{:S(2)}) copy-start(bf16[1,4096,512]{2,1,0:T(8,128)(2,1)} %param.22) | copy-start | bytes 12582916
  31.8 3.5 %copy-start.3 = (bf16[1,512,4096]{2,1,0:T(8,128)(2,1)S(1)}, bf16[1,512,4096]{2,1,0:T(8,128)(2,1)}, u32[]{:S(2)}) copy-start(bf16[1,512,4096]{2,1,0:T(8,128)(2,1)} %param.23) | copy-start | bytes 12582916
  36.7 15.2 %collective-permute-start.19 = (bf16[128,1024]{1,0:T(8,128)(2,1)S(1)}, bf16[128,1024]{1,0:T(8,128)(2,1)S(1)}, u32[]{:S(2)}, u32[]{:S(2)}) collective-permute-start(bf16[128,1024]{1,0:T(8,128)(2,1)S(1)} %get-tuple-element.67), channel_id=1, source_target_pairs={{0,1},{1,0},{2,3},{3,2},{4,5},{5,4},{6,7},{7,6},{8,9},{9,8},{10,11... | collective-permute-start | bytes 786440 | tf_op jit(solution)/shard_map/ppermute | solution.py:310
  36.9 21.9 %copy-start.4 = (f32[256]{0:T(256)S(1)}, f32[256]{0:T(256)}, u32[]{:S(2)}) copy-start(f32[256]{0:T(256)} %param.16) | copy-start | bytes 3076
  36.9 21.9 %copy-start.5 = (f32[4]{0:T(128)S(1)}, f32[4]{0:T(128)}, u32[]{:S(2)}) copy-start(f32[4]{0:T(128)} %lambda_ref.1) | copy-start | bytes 52
  38.3 13.8 %collective-permute-start.24 = (bf16[128,1024]{1,0:T(8,128)(2,1)S(1)}, bf16[128,1024]{1,0:T(8,128)(2,1)S(1)}, u32[]{:S(2)}, u32[]{:S(2)}) collective-permute-start(bf16[128,1024]{1,0:T(8,128)(2,1)S(1)} %get-tuple-element.74), channel_id=1, source_target_pairs={{0,1},{1,0},{2,3},{3,2},{4,5},{5,4},{6,7},{7,6},{8,9},{9,8},{10,11... | collective-permute-start | bytes 786440 | tf_op jit(solution)/shard_map/ppermute | solution.py:310
  38.7 12.1 %collective-permute-start.1 = (bf16[384,256]{1,0:T(8,128)(2,1)S(1)}, bf16[384,256]{1,0:T(8,128)(2,1)S(1)}, u32[]{:S(2)}, u32[]{:S(2)}) collective-permute-start(bf16[384,256]{1,0:T(8,128)(2,1)S(1)} %get-tuple-element.46), channel_id=1, source_target_pairs={{0,16},{4,20},{8,24},{12,28},{16,0},{20,4},{24,8},{28,12},{1,17},{... | collective-permute-start | bytes 589832 | tf_op jit(solution)/shard_map/ppermute | solution.py:310
  41.0 9.8 %collective-permute-start.3 = (bf16[256,256]{1,0:T(8,128)(2,1)S(1)}, bf16[256,256]{1,0:T(8,128)(2,1)S(1)}, u32[]{:S(2)}, u32[]{:S(2)}) collective-permute-start(bf16[256,256]{1,0:T(8,128)(2,1)S(1)} %slice.36), channel_id=1, source_target_pairs={{0,4},{4,0},{8,12},{12,8},{16,20},{20,16},{24,28},{28,24},{1,5},{5... | collective-permute-start | bytes 393224 | tf_op jit(solution)/shard_map/ppermute | solution.py:310
  42.2 16.1 %collective-permute-start.5 = (bf16[512,256]{1,0:T(8,128)(2,1)S(1)}, bf16[512,256]{1,0:T(8,128)(2,1)S(1)}, u32[]{:S(2)}, u32[]{:S(2)}) collective-permute-start(bf16[512,256]{1,0:T(8,128)(2,1)S(1)} %pad_maximum_fusion), channel_id=1, source_target_pairs={{0,4},{4,0},{8,12},{12,8},{16,20},{20,16},{24,28},{28,24},{1,5},{5... | collective-permute-start | bytes 786440 | tf_op jit(solution)/shard_map/ppermute | solution.py:310
  50.8 10.8 %collective-permute-start.26 = (bf16[128,1024]{1,0:T(8,128)(2,1)S(1)}, bf16[128,1024]{1,0:T(8,128)(2,1)S(1)}, u32[]{:S(2)}, u32[]{:S(2)}) collective-permute-start(bf16[128,1024]{1,0:T(8,128)(2,1)S(1)} %get-tuple-element.77), channel_id=1, source_target_pairs={{0,1},{1,0},{2,3},{3,2},{4,5},{5,4},{6,7},{7,6},{8,9},{9,8},{10,11... | collective-permute-start | bytes 786440 | tf_op jit(solution)/shard_map/ppermute | solution.py:310
  50.9 5.9 %collective-permute-start.4 = (bf16[256,256]{1,0:T(8,128)(2,1)S(1)}, bf16[256,256]{1,0:T(8,128)(2,1)S(1)}, u32[]{:S(2)}, u32[]{:S(2)}) collective-permute-start(bf16[256,256]{1,0:T(8,128)(2,1)S(1)} %slice.48), channel_id=1, source_target_pairs={{0,4},{4,0},{8,12},{12,8},{16,20},{20,16},{24,28},{28,24},{1,5},{5... | collective-permute-start | bytes 393224 | tf_op jit(solution)/shard_map/ppermute | solution.py:310
  51.9 12.3 %collective-permute-start.21 = (bf16[128,1024]{1,0:T(8,128)(2,1)S(1)}, bf16[128,1024]{1,0:T(8,128)(2,1)S(1)}, u32[]{:S(2)}, u32[]{:S(2)}) collective-permute-start(bf16[128,1024]{1,0:T(8,128)(2,1)S(1)} %get-tuple-element.69), channel_id=1, source_target_pairs={{0,1},{1,0},{2,3},{3,2},{4,5},{5,4},{6,7},{7,6},{8,9},{9,8},{10,11... | collective-permute-start | bytes 786440 | tf_op jit(solution)/shard_map/ppermute | solution.py:310
  52.1 15.3 %collective-permute-start.20 = (bf16[128,1024]{1,0:T(8,128)(2,1)S(1)}, bf16[128,1024]{1,0:T(8,128)(2,1)S(1)}, u32[]{:S(2)}, u32[]{:S(2)}) collective-permute-start(bf16[128,1024]{1,0:T(8,128)(2,1)S(1)} %shard_map.138), channel_id=1, source_target_pairs={{0,2},{1,3},{2,0},{3,1},{4,6},{5,7},{6,4},{7,5},{8,10},{9,11},{10,... | collective-permute-start | bytes 786440 | tf_op jit(solution)/shard_map/ppermute | solution.py:310
  56.8 7.4 %collective-permute-start.25 = (bf16[64,1024]{1,0:T(8,128)(2,1)S(1)}, bf16[64,1024]{1,0:T(8,128)(2,1)S(1)}, u32[]{:S(2)}, u32[]{:S(2)}) collective-permute-start(bf16[64,1024]{1,0:T(8,128)(2,1)S(1)} %get-tuple-element.75), channel_id=1, source_target_pairs={{0,2},{1,3},{2,0},{3,1},{4,6},{5,7},{6,4},{7,5},{8,10},{9,11},{10,... | collective-permute-start | bytes 393224 | tf_op jit(solution)/shard_map/ppermute | solution.py:310
  58.3 8.1 %collective-permute-start.31 = (bf16[64,1024]{1,0:T(8,128)(2,1)S(1)}, bf16[64,1024]{1,0:T(8,128)(2,1)S(1)}, u32[]{:S(2)}, u32[]{:S(2)}) collective-permute-start(bf16[64,1024]{1,0:T(8,128)(2,1)S(1)} %get-tuple-element.82), channel_id=1, source_target_pairs={{0,2},{1,3},{2,0},{3,1},{4,6},{5,7},{6,4},{7,5},{8,10},{9,11},{10,... | collective-permute-start | bytes 393224 | tf_op jit(solution)/shard_map/ppermute | solution.py:310
  61.6 7.8 %collective-permute-start.6 = (bf16[128,256]{1,0:T(8,128)(2,1)S(1)}, bf16[128,256]{1,0:T(8,128)(2,1)S(1)}, u32[]{:S(2)}, u32[]{:S(2)}) collective-permute-start(bf16[128,256]{1,0:T(8,128)(2,1)S(1)} %get-tuple-element.49), channel_id=1, source_target_pairs={{0,8},{4,12},{8,0},{12,4},{16,24},{20,28},{24,16},{28,20},{1,9},{5... | collective-permute-start | bytes 196616 | tf_op jit(solution)/shard_map/ppermute | solution.py:310
  64.2 6.7 %collective-permute-start.7 = (bf16[128,256]{1,0:T(8,128)(2,1)S(1)}, bf16[128,256]{1,0:T(8,128)(2,1)S(1)}, u32[]{:S(2)}, u32[]{:S(2)}) collective-permute-start(bf16[128,256]{1,0:T(8,128)(2,1)S(1)} %get-tuple-element.50), channel_id=1, source_target_pairs={{0,16},{4,20},{8,24},{12,28},{16,0},{20,4},{24,8},{28,12},{1,17},{... | collective-permute-start | bytes 196616 | tf_op jit(solution)/shard_map/ppermute | solution.py:310
  64.2 9.1 %collective-permute-start.8 = (bf16[128,256]{1,0:T(8,128)(2,1)S(1)}, bf16[128,256]{1,0:T(8,128)(2,1)S(1)}, u32[]{:S(2)}, u32[]{:S(2)}) collective-permute-start(bf16[128,256]{1,0:T(8,128)(2,1)S(1)} %get-tuple-element.51), channel_id=1, source_target_pairs={{0,24},{4,28},{8,16},{12,20},{16,8},{20,12},{24,0},{28,4},{1,25},{... | collective-permute-start | bytes 196616 | tf_op jit(solution)/shard_map/ppermute | solution.py:310
  66.4 7.5 %collective-permute-start.27 = (bf16[32,1024]{1,0:T(8,128)(2,1)S(1)}, bf16[32,1024]{1,0:T(8,128)(2,1)S(1)}, u32[]{:S(2)}, u32[]{:S(2)}) collective-permute-start(bf16[32,1024]{1,0:T(8,128)(2,1)S(1)} %get-tuple-element.78), channel_id=1, source_target_pairs={{0,4},{4,0},{8,12},{12,8},{16,20},{20,16},{24,28},{28,24},{1,5},{5... | collective-permute-start | bytes 196616 | tf_op jit(solution)/shard_map/ppermute | solution.py:310
  67.5 8.3 %collective-permute-start.29 = (bf16[32,1024]{1,0:T(8,128)(2,1)S(1)}, bf16[32,1024]{1,0:T(8,128)(2,1)S(1)}, u32[]{:S(2)}, u32[]{:S(2)}) collective-permute-start(bf16[32,1024]{1,0:T(8,128)(2,1)S(1)} %get-tuple-element.80), channel_id=1, source_target_pairs={{0,12},{4,8},{8,4},{12,0},{16,28},{20,24},{24,20},{28,16},{1,13},{... | collective-permute-start | bytes 196616 | tf_op jit(solution)/shard_map/ppermute | solution.py:310
  69.4 10.0 %collective-permute-start.32 = (bf16[32,1024]{1,0:T(8,128)(2,1)S(1)}, bf16[32,1024]{1,0:T(8,128)(2,1)S(1)}, u32[]{:S(2)}, u32[]{:S(2)}) collective-permute-start(bf16[32,1024]{1,0:T(8,128)(2,1)S(1)} %get-tuple-element.83), channel_id=1, source_target_pairs={{0,20},{4,16},{8,28},{12,24},{16,4},{20,0},{24,12},{28,8},{1,21},{... | collective-permute-start | bytes 196616 | tf_op jit(solution)/shard_map/ppermute | solution.py:310
  70.9 8.6 %collective-permute-start.34 = (bf16[32,1024]{1,0:T(8,128)(2,1)S(1)}, bf16[32,1024]{1,0:T(8,128)(2,1)S(1)}, u32[]{:S(2)}, u32[]{:S(2)}) collective-permute-start(bf16[32,1024]{1,0:T(8,128)(2,1)S(1)} %get-tuple-element.85), channel_id=1, source_target_pairs={{0,28},{4,24},{8,20},{12,16},{16,12},{20,8},{24,4},{28,0},{1,29},{... | collective-permute-start | bytes 196616 | tf_op jit(solution)/shard_map/ppermute | solution.py:310
  73.4 6.2 %collective-permute-start.28 = (bf16[32,1024]{1,0:T(8,128)(2,1)S(1)}, bf16[32,1024]{1,0:T(8,128)(2,1)S(1)}, u32[]{:S(2)}, u32[]{:S(2)}) collective-permute-start(bf16[32,1024]{1,0:T(8,128)(2,1)S(1)} %get-tuple-element.79), channel_id=1, source_target_pairs={{0,8},{4,12},{8,0},{12,4},{16,24},{20,28},{24,16},{28,20},{1,9},{5... | collective-permute-start | bytes 196616 | tf_op jit(solution)/shard_map/ppermute | solution.py:310
  73.9 9.0 %collective-permute-start.30 = (bf16[32,1024]{1,0:T(8,128)(2,1)S(1)}, bf16[32,1024]{1,0:T(8,128)(2,1)S(1)}, u32[]{:S(2)}, u32[]{:S(2)}) collective-permute-start(bf16[32,1024]{1,0:T(8,128)(2,1)S(1)} %get-tuple-element.81), channel_id=1, source_target_pairs={{0,16},{4,20},{8,24},{12,28},{16,0},{20,4},{24,8},{28,12},{1,17},{... | collective-permute-start | bytes 196616 | tf_op jit(solution)/shard_map/ppermute | solution.py:310
  75.8 7.1 %collective-permute-start.33 = (bf16[32,1024]{1,0:T(8,128)(2,1)S(1)}, bf16[32,1024]{1,0:T(8,128)(2,1)S(1)}, u32[]{:S(2)}, u32[]{:S(2)}) collective-permute-start(bf16[32,1024]{1,0:T(8,128)(2,1)S(1)} %get-tuple-element.84), channel_id=1, source_target_pairs={{0,24},{4,28},{8,16},{12,20},{16,8},{20,12},{24,0},{28,4},{1,25},{... | collective-permute-start | bytes 196616 | tf_op jit(solution)/shard_map/ppermute | solution.py:310
